TPU v7x, 512 devices: a whole 4x8x8 slice. The times are simulated.
512 devices in a mesh: ep: 128 (over z, y, core), tp: 4 (over x).
Axes of the slice: x: 4, y: 8, z: 8, core: 2. Of those that a mesh axis runs over, the one named last changes fastest.
Arguments:
- tokens: bfloat16 [2048, 1024], P('ep', 'tp'), may hold values from -75 to 75
- gain_mix: float32 [1024], replicated, may hold values from 0.1 to 1.9
- w_query: bfloat16 [1024, 512], P(None, 'tp'), may hold values from -0.1875 to 0.1875
- w_key: bfloat16 [1024, 512], P(None, 'tp'), may hold values from -0.1875 to 0.1875
- w_value: bfloat16 [1024, 512], P(None, 'tp'), may hold values from -0.1875 to 0.1875
- w_outgate: bfloat16 [1024, 512], P(None, 'tp'), may hold values from -0.1875 to 0.1875
- w_input_gate: bfloat16 [1024, 4], P(None, 'tp'), may hold values from -0.1875 to 0.1875
- w_forget_gate: bfloat16 [1024, 4], P(None, 'tp'), may hold values from -0.1875 to 0.1875
- w_mix_out: bfloat16 [512, 1024], P(None, 'tp'), may hold values from -0.25 to 0.25
- cell_state: float32 [2048, 4, 128, 128], P('ep', 'tp'), may hold values from -3 to 3
- norm_state: float32 [2048, 4, 128], P('ep', 'tp'), may hold values from -3 to 3
- max_state: float32 [2048, 4], P('ep', 'tp'), may hold values from -2 to 143
- gain_ffn: float32 [1024], replicated, may hold values from 0.1 to 1.9
- route_ids: int32 [2048, 2], P('ep'), may hold values from 0 to 127, all different within a row; in each aligned block of 16 rows (0 to 15, 16 to 31, ...) no two rows name the same one
- route_logits: float32 [2048, 2], P('ep'), may hold values from -5 to 5
- expert_gate: bfloat16 [128, 1024, 1408], P('ep', None, 'tp'), may hold values from -0.1875 to 0.1875
- expert_up: bfloat16 [128, 1024, 1408], P('ep', None, 'tp'), may hold values from -0.1875 to 0.1875
- expert_down: bfloat16 [128, 1408, 1024], P('ep', 'tp'), may hold values from -0.15625 to 0.15625
- dense_gate: bfloat16 [1024, 3072], P('tp', 'ep'), may hold values from -0.1875 to 0.1875
- dense_up: bfloat16 [1024, 3072], P('tp', 'ep'), may hold values from -0.1875 to 0.1875
- dense_down: bfloat16 [3072, 1024], P('ep', 'tp'), may hold values from -0.3125 to 0.3125
- dense_mix: bfloat16 [1024], P('tp'), may hold values from -0.1875 to 0.1875
Outputs:
- layer_out: bfloat16 [2048, 1024], P('ep', 'tp')
Inputs may be any that keep to these rules, and one draw needn't show every extreme that they name: `route_ids`: each row names 2 different experts. Among the 16 tokens of one index of ep no expert is named more than 1 times, and in every draw some expert is named exactly 1 times by the tokens of one index of ep.
All inputs are finite; a program needn't handle non-finite values.
Results may differ from a plain program's by a relative error of at most 0.013.
Values may be sent and summed in bfloat16 or wider, within the bound.
No kernel may reach another device: no remote copies, remote signals or barrier semaphores. Data moves between devices by JAX's collectives and lax.ppermute only.
A program may use at most 64 MiB of HBM per device.

v0:
```python
import jax
import jax.numpy as jnp
from jax import lax
from jax.sharding import PartitionSpec as P

HEAD = 128
TOP = 2


epsilon = 1e-06
highest = lax.Precision.HIGHEST


def sent_to_all(shard, axis):
    size = lax.axis_size(axis)
    return lax.all_to_all(
        jnp.broadcast_to(shard[None], (size, *shard.shape)), axis, 0, 0, tiled=True
    )


def joined_along(blocks, dim):
    dims = list(blocks.shape[1:])
    dims[dim] *= blocks.shape[0]
    return jnp.moveaxis(blocks, 0, dim).reshape(dims)


def collect(shard, axis, dim):
    blocks = sent_to_all(shard, axis)
    return joined_along(blocks, dim)


def cut_along(shard, dim, size):
    dims = shard.shape
    blocks = shard.reshape(*dims[:dim], size, dims[dim] // size, *dims[dim + 1 :])
    return jnp.moveaxis(blocks, dim, 0)


def sent_and_summed(shard, axis, dim):
    blocks = cut_along(shard, dim, lax.axis_size(axis))
    arrived = lax.all_to_all(blocks, axis, split_axis=0, concat_axis=0, tiled=True)
    return arrived.astype(jnp.float32).sum(axis=0)


def turned_gather(arrays, axis, dims):
    turned = [jnp.moveaxis(a, dim, 0) for a, dim in zip(arrays, dims)]
    widths = [t[0].size for t in turned]
    both = jnp.concatenate([t.reshape(-1, w) for t, w in zip(turned, widths)], axis=1)
    result = lax.all_gather(both, axis, axis=0, tiled=True)
    blocks = jnp.split(result, [sum(widths[:k]) for k in range(1, len(widths))], axis=1)
    return tuple(
        (
            jnp.moveaxis(b.reshape(-1, *t.shape[1:]), 0, dim)
            for b, t, dim in zip(blocks, turned, dims)
        )
    )


def of_everyone(shard, axis):
    return sent_to_all(shard, axis).astype(jnp.float32).sum(axis=0)


def rms_norm(rows, gain):
    values = rows.astype(jnp.float32)
    scale = lax.rsqrt(jnp.mean(values * values, axis=-1, keepdims=True) + epsilon)
    return (values * scale * gain).astype(jnp.bfloat16)


def local(
    tokens,
    gain_mix,
    w_query,
    w_key,
    w_value,
    w_outgate,
    w_input_gate,
    w_forget_gate,
    w_mix_out,
    cell_state,
    norm_state,
    max_state,
    gain_ffn,
    route_ids,
    route_logits,
    expert_gate,
    expert_up,
    expert_down,
    dense_gate,
    dense_up,
    dense_down,
    dense_mix,
):
    seq_count, quarter = tokens.shape
    tp_rank = lax.axis_index("tp")
    full_tokens = collect(tokens, "tp", 1)
    normed_mix = rms_norm(full_tokens, gain_mix)

    def project(weight):
        return jnp.dot(normed_mix, weight, preferred_element_type=jnp.float32)

    query_rows = project(w_query).reshape(seq_count, -1, HEAD)
    key_rows = project(w_key).reshape(seq_count, -1, HEAD) * HEAD ** (-0.5)
    value_rows = project(w_value).reshape(seq_count, -1, HEAD)
    out_gate = project(w_outgate)
    input_gate = project(w_input_gate)
    carried = jax.nn.log_sigmoid(project(w_forget_gate)) + max_state
    stabilizer = jnp.maximum(carried, input_gate)
    weight_old = jnp.exp(carried - stabilizer)
    weight_new = jnp.exp(input_gate - stabilizer) * jnp.sum(query_rows * key_rows, axis=-1)
    cell_read = jnp.einsum("bhd,bhde->bhe", query_rows, cell_state, precision=highest)
    numerator = weight_old[..., None] * cell_read + weight_new[..., None] * value_rows
    denominator = weight_old * jnp.sum(query_rows * norm_state, axis=-1) + weight_new
    cell_out = numerator / jnp.maximum(jnp.abs(denominator), 1.0)[..., None]
    mixed = (jax.nn.sigmoid(out_gate) * cell_out.reshape(seq_count, -1)).astype(jnp.bfloat16)
    all_heads = collect(mixed, "tp", 1)
    resid = (
        tokens.astype(jnp.float32)
        + jnp.dot(all_heads, w_mix_out, preferred_element_type=jnp.float32)
    ).astype(jnp.bfloat16)
    whole_resid = collect(resid, "tp", 1)
    normed_full = rms_norm(whole_resid, gain_ffn)
    normed_part = lax.dynamic_slice_in_dim(normed_full, tp_rank * quarter, quarter, 1)
    experts = lax.axis_size("ep")
    slots = (2 * seq_count * TOP + experts - 1) // experts
    flat_ids = route_ids.reshape(-1)
    onehot = (flat_ids[:, None] == jnp.arange(experts, dtype=jnp.int32)[None, :]).astype(jnp.int32)
    earlier = jnp.cumsum(onehot, axis=0) - onehot
    slot_rank = jnp.sum(earlier * onehot, axis=1)
    target = flat_ids * slots + slot_rank
    select = (jnp.arange(experts * slots, dtype=jnp.int32)[:, None] == target[None, :]).astype(
        jnp.bfloat16
    )
    repeated = jnp.repeat(normed_full, TOP, axis=0)
    outgoing = jnp.dot(select, repeated, preferred_element_type=jnp.float32).astype(jnp.bfloat16)
    outgoing = outgoing.reshape(experts, slots, -1)
    received = lax.all_to_all(outgoing, "ep", split_axis=0, concat_axis=0, tiled=True)
    sources = received.shape[0]
    item_count = received.shape[1]
    flat_rows = received.reshape(sources * item_count, -1)
    gate_rows = jnp.dot(flat_rows, expert_gate[0], preferred_element_type=jnp.float32)
    up_rows = jnp.dot(flat_rows, expert_up[0], preferred_element_type=jnp.float32)
    hidden = (jax.nn.silu(gate_rows) * up_rows).astype(jnp.bfloat16)
    partial_value = jnp.dot(hidden, expert_down[0], preferred_element_type=jnp.float32)
    summed = sent_and_summed(partial_value.astype(jnp.bfloat16), "tp", 1).astype(jnp.bfloat16)
    returned = lax.all_to_all(
        summed.reshape(sources, item_count, -1), "ep", split_axis=0, concat_axis=0, tiled=True
    )
    picked = lax.dot_general(
        select,
        returned.reshape(experts * slots, -1),
        (((0,), (0,)), ((), ())),
        preferred_element_type=jnp.float32,
    ).reshape(seq_count, TOP, -1)
    route_weight = jax.nn.sigmoid(route_logits - route_logits[:, ::-1])
    moe = jnp.sum(route_weight[..., None] * picked, axis=1)
    mix_part = jnp.dot(normed_part, dense_mix, preferred_element_type=jnp.float32)
    pieces = turned_gather((dense_gate, dense_up), "ep", (1, 1))
    gate_cols = jnp.dot(normed_part, pieces[0], preferred_element_type=jnp.float32)
    up_cols = jnp.dot(normed_part, pieces[1], preferred_element_type=jnp.float32)
    gate_sum, up_sum, mix_logit = (
        of_everyone(gate_cols.astype(jnp.bfloat16), "tp").astype(jnp.float32),
        of_everyone(up_cols.astype(jnp.bfloat16), "tp").astype(jnp.float32),
        of_everyone(mix_part.astype(jnp.bfloat16), "tp").astype(jnp.float32),
    )
    dense_hidden = (jax.nn.silu(gate_sum) * up_sum).astype(jnp.bfloat16)
    dense_out = jnp.dot(
        dense_hidden,
        lax.all_gather(dense_down, "ep", axis=0, tiled=True),
        preferred_element_type=jnp.float32,
    )
    mix_gate = jax.nn.sigmoid(mix_logit)
    total = resid.astype(jnp.float32) + moe + mix_gate[:, None] * dense_out
    return total.astype(jnp.bfloat16)


def solution(mesh):
    return jax.shard_map(
        local,
        mesh=mesh,
        in_specs=(
            P("ep", "tp"),
            P(),
            P(None, "tp"),
            P(None, "tp"),
            P(None, "tp"),
            P(None, "tp"),
            P(None, "tp"),
            P(None, "tp"),
            P(None, "tp"),
            P("ep", "tp", None, None),
            P("ep", "tp", None),
            P("ep", "tp"),
            P(),
            P("ep", None),
            P("ep", None),
            P("ep", None, "tp"),
            P("ep", None, "tp"),
            P("ep", "tp", None),
            P("tp", "ep"),
            P("tp", "ep"),
            P("ep", "tp"),
            P("tp"),
        ),
        out_specs=P("ep", "tp"),
        check_vma=False,
    )
```

profile of v0, /device:TPU:1, one launch (start us, length us, event | category | flops | bytes accessed | tf_op | source)
XLA Modules:
  0.0 192.4 jit_solution(7491865044756722748)
XLA Ops:
  6.5 0.0 all-gather.3.cloned.1.call-start
  6.6 1.4 pad_maximum_fusion
  8.0 1.3 broadcast_in_dim.14
  9.3 4.8 %all-to-all-start = ((bf16[4,16,256]{2,1,0:T(8,128)(2,1)}), bf16[4,16,256]{2,1,0:T(8,128)(2,1)S(1)}, u32[]{:S(2)}, u32[]{:S(2)}) async-start(bf16[4,16,256]{2,1,0:T(8,128)(2,1)} %broadcast_in_dim.14), calls=%async_computation | async-start | bytes 65536 | tf_op jit(solution)/shard_map/all_to_all | solution.py:16
  14.2 0.7 all-gather.5.cloned.1.call-update
  14.9 0.7 mul.148
  15.6 0.8 copy.72
  16.4 0.1 reshape.174
  16.5 2.0 %all-to-all-done = bf16[4,16,256]{2,1,0:T(8,128)(2,1)S(1)} async-done(((bf16[4,16,256]{2,1,0:T(8,128)(2,1)}), bf16[4,16,256]{2,1,0:T(8,128)(2,1)S(1)}, u32[]{:S(2)}, u32[]{:S(2)}) %all-to-all-start) | async-done | bytes 32800 | tf_op jit(solution)/shard_map/all_to_all | solution.py:16
  18.5 0.1 fusion.40
  18.6 0.8 multiply_convert_fusion.3
  19.4 0.1 fusion.45
  19.5 1.1 fusion.14
  20.6 1.2 fusion.51
  21.8 1.2 fusion.16
  23.1 1.0 fusion.19
  24.0 0.1 bitcast_add_fusion
  24.2 0.1 maximum_bitcast_fusion
  24.3 0.2 fusion.15
  24.5 0.6 broadcast_in_dim.15
  25.1 3.2 %all-to-all-start.1 = ((bf16[4,16,128]{2,1,0:T(8,128)(2,1)}), bf16[4,16,128]{2,1,0:T(8,128)(2,1)S(1)}, u32[]{:S(2)}, u32[]{:S(2)}) async-start(bf16[4,16,128]{2,1,0:T(8,128)(2,1)} %broadcast_in_dim.15), calls=%async_computation.1 | async-start | bytes 32768 | tf_op jit(solution)/shard_map/all_to_all | solution.py:16
  28.4 0.1 fusion.49
  28.4 0.1 reduce_window_sum.11
  28.5 4.0 %all-to-all-done.1 = bf16[4,16,128]{2,1,0:T(8,128)(2,1)S(1)} async-done(((bf16[4,16,128]{2,1,0:T(8,128)(2,1)}), bf16[4,16,128]{2,1,0:T(8,128)(2,1)S(1)}, u32[]{:S(2)}, u32[]{:S(2)}) %all-to-all-start.1) | async-done | bytes 16416 | tf_op jit(solution)/shard_map/all_to_all | solution.py:16
  32.5 0.1 fusion.6
  32.7 0.6 broadcast_in_dim.16
  33.3 3.3 %all-to-all-start.2 = ((bf16[4,16,256]{2,1,0:T(8,128)(2,1)}), bf16[4,16,256]{2,1,0:T(8,128)(2,1)S(1)}, u32[]{:S(2)}, u32[]{:S(2)}) async-start(bf16[4,16,256]{2,1,0:T(8,128)(2,1)} %broadcast_in_dim.16), calls=%async_computation.2 | async-start | bytes 65536 | tf_op jit(solution)/shard_map/all_to_all | solution.py:16
  36.6 0.2 select_reduce_fusion
  36.8 4.1 %all-to-all-done.2 = bf16[4,16,256]{2,1,0:T(8,128)(2,1)S(1)} async-done(((bf16[4,16,256]{2,1,0:T(8,128)(2,1)}), bf16[4,16,256]{2,1,0:T(8,128)(2,1)S(1)}, u32[]{:S(2)}, u32[]{:S(2)}) %all-to-all-start.2) | async-done | bytes 32800 | tf_op jit(solution)/shard_map/all_to_all | solution.py:16
  40.8 0.1 fusion.39
  41.0 0.1 multiply_convert_fusion.2
  41.2 0.2 fusion.2
  41.4 0.5 broadcast.120
  41.9 0.7 reduce.9
  42.6 0.9 reshape.195
  43.5 21.3 %all-to-all-start.3 = ((bf16[128,2,512]{2,1,0:T(2,128)(2,1)}), bf16[128,2,512]{2,1,0:T(2,128)(2,1)S(1)}, u32[]{:S(2)}, u32[]{:S(2)}) async-start(bf16[128,2,512]{2,1,0:T(2,128)(2,1)} %reshape.195), calls=%async_computation.3 | async-start | bytes 524288 | tf_op jit(solution)/shard_map/all_to_all | solution.py:135
  64.8 0.1 iota_compare_fusion.3
  65.0 15.1 %all-to-all-done.3 = bf16[128,2,512]{2,1,0:T(2,128)(2,1)S(1)} async-done(((bf16[128,2,512]{2,1,0:T(2,128)(2,1)}), bf16[128,2,512]{2,1,0:T(2,128)(2,1)S(1)}, u32[]{:S(2)}, u32[]{:S(2)}) %all-to-all-start.3) | async-done | bytes 262176 | tf_op jit(solution)/shard_map/all_to_all | solution.py:135
  80.0 0.2 reshape.196
  80.3 0.4 fusion.24
  80.7 2.0 %convolution_convert_fusion.3 = bf16[128,1024]{1,0:T(8,128)(2,1)S(1)} fusion(bf16[1,352,1024]{2,1,0:T(8,128)(2,1)S(1)} %copy-done.6, bf16[1,1024,352]{1,2,0:T(8,128)(2,1)} %param.38, f32[128,352]{0,1:T(8,128)S(1)} %fusion.24, bf16[128,1,1024]{2,1,0:T(2,128)(2,1)S(1)} %reshape.196), kind=kOutput, calls=%fused_computation.5 | convolution fusion | flops 184950784 | bytes 2146304 | tf_op jit(solution)/shard_map/dot_general | solution.py:142
  82.7 0.7 copy.109
  83.4 3.4 %all-to-all-start.4 = ((bf16[4,128,256]{2,1,0:T(8,128)(2,1)}), bf16[4,128,256]{2,1,0:T(8,128)(2,1)S(1)}, u32[]{:S(2)}, u32[]{:S(2)}) async-start(bf16[4,128,256]{2,1,0:T(8,128)(2,1)} %bitcast.113), calls=%async_computation.4 | async-start | bytes 524288 | tf_op jit(solution)/shard_map/all_to_all | solution.py:40
  86.8 0.1 fusion.17
  87.0 6.0 %all-to-all-done.4 = bf16[4,128,256]{2,1,0:T(8,128)(2,1)S(1)} async-done(((bf16[4,128,256]{2,1,0:T(8,128)(2,1)}), bf16[4,128,256]{2,1,0:T(8,128)(2,1)S(1)}, u32[]{:S(2)}, u32[]{:S(2)}) %all-to-all-start.4) | async-done | bytes 262176 | tf_op jit(solution)/shard_map/all_to_all | solution.py:40
  92.9 0.6 broadcast_in_dim.18
  93.5 3.2 %all-to-all-start.6 = ((bf16[4,1,16]{2,1,0:T(2,128)(2,1)}), bf16[4,1,16]{2,1,0:T(2,128)(2,1)S(1)}, u32[]{:S(2)}, u32[]{:S(2)}) async-start(bf16[4,1,16]{2,1,0:T(2,128)(2,1)} %broadcast_in_dim.18), calls=%async_computation.6 | async-start | bytes 4096 | tf_op jit(solution)/shard_map/all_to_all | solution.py:16
  96.8 0.6 reduce.10
  97.4 0.6 reshape.197
  98.0 2.8 %all-to-all-done.6 = bf16[4,1,16]{2,1,0:T(2,128)(2,1)S(1)} async-done(((bf16[4,1,16]{2,1,0:T(2,128)(2,1)}), bf16[4,1,16]{2,1,0:T(2,128)(2,1)S(1)}, u32[]{:S(2)}, u32[]{:S(2)}) %all-to-all-start.6) | async-done | bytes 160 | tf_op jit(solution)/shard_map/all_to_all | solution.py:16
  100.7 7.7 %all-to-all-start.5 = ((bf16[128,2,128]{2,1,0:T(2,128)(2,1)}), bf16[128,2,128]{2,1,0:T(2,128)(2,1)S(1)}, u32[]{:S(2)}, u32[]{:S(2)}) async-start(bf16[128,2,128]{2,1,0:T(2,128)(2,1)} %reshape.197), calls=%async_computation.5 | async-start | bytes 131072 | tf_op jit(solution)/shard_map/all_to_all | solution.py:144
  108.5 1.9 convolution_convert_fusion.1
  110.4 9.6 %all-to-all-done.5 = bf16[128,2,128]{2,1,0:T(2,128)(2,1)S(1)} async-done(((bf16[128,2,128]{2,1,0:T(2,128)(2,1)}), bf16[128,2,128]{2,1,0:T(2,128)(2,1)S(1)}, u32[]{:S(2)}, u32[]{:S(2)}) %all-to-all-start.5) | async-done | bytes 65568 | tf_op jit(solution)/shard_map/all_to_all | solution.py:144
  120.0 0.8 broadcast_in_dim.19
  120.8 3.5 %all-to-all-start.7 = ((bf16[4,16,3072]{2,1,0:T(8,128)(2,1)}), bf16[4,16,3072]{2,1,0:T(8,128)(2,1)S(1)}, u32[]{:S(2)}, u32[]{:S(2)}) async-start(bf16[4,16,3072]{2,1,0:T(8,128)(2,1)} %broadcast_in_dim.19), calls=%async_computation.7 | async-start | bytes 786432 | tf_op jit(solution)/shard_map/all_to_all | solution.py:16
  124.3 1.9 convolution_convert_fusion
  126.2 5.6 %all-to-all-done.7 = bf16[4,16,3072]{2,1,0:T(8,128)(2,1)S(1)} async-done(((bf16[4,16,3072]{2,1,0:T(8,128)(2,1)}), bf16[4,16,3072]{2,1,0:T(8,128)(2,1)S(1)}, u32[]{:S(2)}, u32[]{:S(2)}) %all-to-all-start.7) | async-done | bytes 393248 | tf_op jit(solution)/shard_map/all_to_all | solution.py:16
  131.9 0.8 broadcast_in_dim.20
  132.6 3.5 %all-to-all-start.8 = ((bf16[4,16,3072]{2,1,0:T(8,128)(2,1)}), bf16[4,16,3072]{2,1,0:T(8,128)(2,1)S(1)}, u32[]{:S(2)}, u32[]{:S(2)}) async-start(bf16[4,16,3072]{2,1,0:T(8,128)(2,1)} %broadcast_in_dim.20), calls=%async_computation.8 | async-start | bytes 786432 | tf_op jit(solution)/shard_map/all_to_all | solution.py:16
  136.1 0.1 fusion.4
  136.2 0.1 convert_reduce_fusion.1
  136.3 6.2 %all-to-all-done.8 = bf16[4,16,3072]{2,1,0:T(8,128)(2,1)S(1)} async-done(((bf16[4,16,3072]{2,1,0:T(8,128)(2,1)}), bf16[4,16,3072]{2,1,0:T(8,128)(2,1)S(1)}, u32[]{:S(2)}, u32[]{:S(2)}) %all-to-all-start.8) | async-done | bytes 393248 | tf_op jit(solution)/shard_map/all_to_all | solution.py:16
  142.6 40.6 %all-gather.5.cloned.1.call-done = bf16[3072,256]{1,0:T(8,128)(2,1)} async-done(((bf16[24,256]{1,0:T(8,128)(2,1)}), bf16[3072,256]{1,0:T(8,128)(2,1)}) %all-gather.5.cloned.1.call-update) | async-done | bytes 1572880 | tf_op jit(solution)/shard_map/all_gather | solution.py:167
  183.3 2.3 %fusion.7 = bf16[16,256]{1,0:T(8,128)(2,1)} fusion(bf16[3072,256]{1,0:T(8,128)(2,1)} %all-gather.5.cloned.1.call-done, f32[16,3072]{1,0:T(8,128)S(1)} %convert_reduce_fusion, f32[16,3072]{1,0:T(8,128)S(1)} %convert_reduce_fusion.1, f32[16,256]{1,0:T(8,128)S(1)} %fusion.4, bf16[16,256]{1,0:T(8,128)(2,1)S(1)} %fusion.6, f32[16]{0:T(128)S(1)} %add_divide_fusion.1), kind=kOutput, calls=%fused_computation.15 | convolution fusion | flops 25481216 | bytes 1998912 | tf_op jit(solution)/shard_map/dot_general | solution.py:165
  (46 shorter events, 0.4 us)
Async XLA Ops:
  6.5 16.5 %copy-start = (f32[16,1,128,128]{3,2,1,0:T(8,128)S(1)}, f32[16,1,128,128]{3,2,1,0:T(8,128)}, u32[]{:S(2)}) copy-start(f32[16,1,128,128]{3,2,1,0:T(8,128)} %param.31) | copy-start | bytes 3145732
  6.5 17.5 %copy-start.8 = (bf16[1024,1]{0,1:T(2,128)(2,1)S(1)}, bf16[1024,1]{0,1:T(2,128)(2,1)}, u32[]{:S(2)}) copy-start(bf16[1024,1]{0,1:T(2,128)(2,1)} %param.29) | copy-start | bytes 6148
  6.5 17.5 %copy-start.10 = (f32[16,1]{0,1:T(1,128)S(1)}, f32[16,1]{0,1:T(1,128)}, u32[]{:S(2)}) copy-start(f32[16,1]{0,1:T(1,128)} %param.33) | copy-start | bytes 196
  6.5 17.6 %copy-start.9 = (bf16[1024,1]{0,1:T(2,128)(2,1)S(1)}, bf16[1024,1]{0,1:T(2,128)(2,1)}, u32[]{:S(2)}) copy-start(bf16[1024,1]{0,1:T(2,128)(2,1)} %param.28) | copy-start | bytes 6148
  6.5 17.8 %copy-start.7 = (bf16[1024,128]{1,0:T(8,128)(2,1)S(1)}, bf16[1024,128]{1,0:T(8,128)(2,1)}, u32[]{:S(2)}) copy-start(bf16[1024,128]{1,0:T(8,128)(2,1)} %param.26) | copy-start | bytes 786436
  6.5 101.9 %all-gather.3.cloned.1.call-start = ((), (), s32[]{:S(2)}) async-start(), calls=%async_computation.9 | async-start | bytes 3170304 | tf_op jit(solution)/shard_map/all_gather | solution.py:48
  9.3 9.1 %all-to-all-start = ((bf16[4,16,256]{2,1,0:T(8,128)(2,1)}), bf16[4,16,256]{2,1,0:T(8,128)(2,1)S(1)}, u32[]{:S(2)}, u32[]{:S(2)}) async-start(bf16[4,16,256]{2,1,0:T(8,128)(2,1)} %broadcast_in_dim.14), calls=%async_computation | async-start | bytes 65536 | tf_op jit(solution)/shard_map/all_to_all | solution.py:16
  14.2 18.4 %copy-start.2 = (bf16[512,256]{1,0:T(8,128)(2,1)S(1)}, bf16[512,256]{1,0:T(8,128)(2,1)}, u32[]{:S(2)}) copy-start(bf16[512,256]{1,0:T(8,128)(2,1)} %param.30) | copy-start | bytes 786436
  14.2 18.4 %copy-start.3 = (bf16[16,256]{1,0:T(8,128)(2,1)S(1)}, bf16[16,256]{1,0:T(8,128)(2,1)}, u32[]{:S(2)}) copy-start(bf16[16,256]{1,0:T(8,128)(2,1)} %param.22) | copy-start | bytes 24580
  14.2 169.1 %all-gather.5.cloned.1.call-start = ((), (), s32[]{:S(2)}) async-start(), calls=%async_computation.10 | async-start | bytes 1585152 | tf_op jit(solution)/shard_map/all_gather | solution.py:167
  19.5 21.5 %copy-start.4 = (f32[1024]{0:T(1024)S(1)}, f32[1024]{0:T(1024)}, u32[]{:S(2)}) copy-start(f32[1024]{0:T(1024)} %param.34) | copy-start | bytes 12292
  24.5 40.4 %copy-start.5 = (f32[16,2]{0,1:T(2,128)S(1)}, f32[16,2]{0,1:T(2,128)}, u32[]{:S(2)}) copy-start(f32[16,2]{0,1:T(2,128)} %param.36) | copy-start | bytes 388
  24.5 40.4 %copy-start.11 = (bf16[256]{0:T(256)(128)(2,1)S(1)}, bf16[256]{0:T(256)(128)(2,1)}, u32[]{:S(2)}) copy-start(bf16[256]{0:T(256)(128)(2,1)} %param.43) | copy-start | bytes 1540
  25.1 7.4 %all-to-all-start.1 = ((bf16[4,16,128]{2,1,0:T(8,128)(2,1)}), bf16[4,16,128]{2,1,0:T(8,128)(2,1)S(1)}, u32[]{:S(2)}, u32[]{:S(2)}) async-start(bf16[4,16,128]{2,1,0:T(8,128)(2,1)} %broadcast_in_dim.15), calls=%async_computation.1 | async-start | bytes 32768 | tf_op jit(solution)/shard_map/all_to_all | solution.py:16
  33.3 7.5 %all-to-all-start.2 = ((bf16[4,16,256]{2,1,0:T(8,128)(2,1)}), bf16[4,16,256]{2,1,0:T(8,128)(2,1)S(1)}, u32[]{:S(2)}, u32[]{:S(2)}) async-start(bf16[4,16,256]{2,1,0:T(8,128)(2,1)} %broadcast_in_dim.16), calls=%async_computation.2 | async-start | bytes 65536 | tf_op jit(solution)/shard_map/all_to_all | solution.py:16
  41.0 39.3 %copy-start.1 = (bf16[1,1024,352]{1,2,0:T(8,128)(2,1)S(1)}, bf16[1,1024,352]{1,2,0:T(8,128)(2,1)}, u32[]{:S(2)}) copy-start(bf16[1,1024,352]{1,2,0:T(8,128)(2,1)} %param.37) | copy-start | bytes 2162692
  42.6 38.1 %copy-start.6 = (bf16[1,352,1024]{2,1,0:T(8,128)(2,1)S(1)}, bf16[1,352,1024]{2,1,0:T(8,128)(2,1)}, u32[]{:S(2)}) copy-start(bf16[1,352,1024]{2,1,0:T(8,128)(2,1)} %param.39) | copy-start | bytes 2162692
  43.5 36.6 %all-to-all-start.3 = ((bf16[128,2,512]{2,1,0:T(2,128)(2,1)}), bf16[128,2,512]{2,1,0:T(2,128)(2,1)S(1)}, u32[]{:S(2)}, u32[]{:S(2)}) async-start(bf16[128,2,512]{2,1,0:T(2,128)(2,1)} %reshape.195), calls=%async_computation.3 | async-start | bytes 524288 | tf_op jit(solution)/shard_map/all_to_all | solution.py:135
  83.4 9.5 %all-to-all-start.4 = ((bf16[4,128,256]{2,1,0:T(8,128)(2,1)}), bf16[4,128,256]{2,1,0:T(8,128)(2,1)S(1)}, u32[]{:S(2)}, u32[]{:S(2)}) async-start(bf16[4,128,256]{2,1,0:T(8,128)(2,1)} %bitcast.113), calls=%async_computation.4 | async-start | bytes 524288 | tf_op jit(solution)/shard_map/all_to_all | solution.py:40
  93.5 7.3 %all-to-all-start.6 = ((bf16[4,1,16]{2,1,0:T(2,128)(2,1)}), bf16[4,1,16]{2,1,0:T(2,128)(2,1)S(1)}, u32[]{:S(2)}, u32[]{:S(2)}) async-start(bf16[4,1,16]{2,1,0:T(2,128)(2,1)} %broadcast_in_dim.18), calls=%async_computation.6 | async-start | bytes 4096 | tf_op jit(solution)/shard_map/all_to_all | solution.py:16
  100.7 19.3 %all-to-all-start.5 = ((bf16[128,2,128]{2,1,0:T(2,128)(2,1)}), bf16[128,2,128]{2,1,0:T(2,128)(2,1)S(1)}, u32[]{:S(2)}, u32[]{:S(2)}) async-start(bf16[128,2,128]{2,1,0:T(2,128)(2,1)} %reshape.197), calls=%async_computation.5 | async-start | bytes 131072 | tf_op jit(solution)/shard_map/all_to_all | solution.py:144
  120.8 11.0 %all-to-all-start.7 = ((bf16[4,16,3072]{2,1,0:T(8,128)(2,1)}), bf16[4,16,3072]{2,1,0:T(8,128)(2,1)S(1)}, u32[]{:S(2)}, u32[]{:S(2)}) async-start(bf16[4,16,3072]{2,1,0:T(8,128)(2,1)} %broadcast_in_dim.19), calls=%async_computation.7 | async-start | bytes 786432 | tf_op jit(solution)/shard_map/all_to_all | solution.py:16
  132.6 9.9 %all-to-all-start.8 = ((bf16[4,16,3072]{2,1,0:T(8,128)(2,1)}), bf16[4,16,3072]{2,1,0:T(8,128)(2,1)S(1)}, u32[]{:S(2)}, u32[]{:S(2)}) async-start(bf16[4,16,3072]{2,1,0:T(8,128)(2,1)} %broadcast_in_dim.20), calls=%async_computation.8 | async-start | bytes 786432 | tf_op jit(solution)/shard_map/all_to_all | solution.py:16
Sparse Core Ops, SparseCore 0:
  10.5 90.2 all-gather.2
  104.0 79.2 all-gather.4
where the time goes:
time: 193 us; the launch traced here: 192 us
  waiting for transfers between devices  96.8 us (50%)
  starting transfers between devices  54 us (28%)
  matrix products  14.1 us (7%)
  between operations  13.7 us (7%)
  local copies, waits for them, and re-layouts  9.37 us (5%)
  other arithmetic  4.49 us (2%)
    all_gather x1, waiting for transfers between devices, local(): lax.all_gather(dense_down, 'ep', axis=0, tiled=True)  40.6 us
    all_to_all x6, waiting for transfers between devices, sent_to_all(): lax.all_to_all(jnp.broadcast_to(shard[None], (size, *shard.shape)), axis,...  24.7 us
    all_to_all x6, starting transfers between devices, sent_to_all(): lax.all_to_all(jnp.broadcast_to(shard[None], (size, *shard.shape)), axis,...  21.5 us
    all_to_all x1, starting transfers between devices, local(): lax.all_to_all(outgoing, 'ep', split_axis=0, concat_axis=0, tiled=True)  21.3 us
    all_to_all x1, waiting for transfers between devices, local(): lax.all_to_all(outgoing, 'ep', split_axis=0, concat_axis=0, tiled=True)  15.1 us
    all_to_all x1, waiting for transfers between devices, local(): lax.all_to_all(summed.reshape(sources, item_count, -1), 'ep', split_axis=...  9.63 us
    all_to_all x1, starting transfers between devices, local(): lax.all_to_all(summed.reshape(sources, item_count, -1), 'ep', split_axis=...  7.71 us
    all_to_all x1, waiting for transfers between devices, sent_and_summed(): lax.all_to_all(blocks, axis, split_axis=0, concat_axis=0, tiled=True)  5.95 us
  transfers between devices with their start and end apart: 11, of which 10 were waited for; matrix products, arithmetic and copies ran while one was open for 13% of the time, Pallas kernels for 0%

commit v1 on v0

v1 whole, which is shorter than its diff:
```python
import jax
import jax.numpy as jnp
from jax import lax
from jax.sharding import Mesh, PartitionSpec as P

HEAD = 128
TOP = 2

epsilon = 1e-06
highest = lax.Precision.HIGHEST
f32 = jnp.float32
bf16 = jnp.bfloat16

FAR = ("zh", "yh")
NEAR = ("zl", "yl", "c")
EP = ("zh", "zl", "yh", "yl", "c")


def exchange(blocks, axis):
    return lax.all_to_all(blocks, axis, 0, 0, tiled=True)


def to_all(shard, size):
    return jnp.broadcast_to(shard[None], (size, *shard.shape))


def side_by_side(blocks):
    count, rows, columns = blocks.shape
    return jnp.moveaxis(blocks, 0, 1).reshape(rows, count * columns)


def rms_norm(rows, gain):
    values = rows.astype(f32)
    scale = lax.rsqrt(jnp.mean(values * values, axis=-1, keepdims=True) + epsilon)
    return (values * scale * gain).astype(bf16)


def dot(a, b):
    return jnp.dot(a, b, preferred_element_type=f32)


def local(
    tokens,
    gain_mix,
    w_query,
    w_key,
    w_value,
    w_outgate,
    w_input_gate,
    w_forget_gate,
    w_mix_out,
    cell_state,
    norm_state,
    max_state,
    gain_ffn,
    route_ids,
    route_logits,
    expert_gate,
    expert_up,
    expert_down,
    dense_gate,
    dense_up,
    dense_down,
    dense_mix,
):
    seqs, quarter = tokens.shape
    tp = lax.axis_size("x")
    far = lax.axis_size(FAR)
    near = lax.axis_size(NEAR)
    experts = lax.axis_size(EP)
    me = lax.axis_index("x")
    columns = dense_gate.shape[1]
    slim = columns // tp

    full_tokens = side_by_side(exchange(to_all(tokens, tp), "x"))

    extra = jnp.concatenate([dense_mix[None], jnp.zeros((7, quarter), bf16)], axis=0)
    mix_out = exchange(to_all(jnp.concatenate([w_mix_out, extra], axis=0), tp), "x")

    packed = jnp.stack([dense_gate.T, dense_up.T, dense_down]).reshape(3, tp, slim, quarter)
    packed = jnp.moveaxis(packed, 1, 0).reshape(tp, 3 * slim, quarter)
    dense = exchange(jnp.tile(packed, (far, 1, 1)), FAR + ("x",))
    dense = dense.reshape(far, tp, 3, slim, quarter)
    dense = jnp.transpose(dense, (2, 0, 3, 1, 4)).reshape(3, far * slim, tp * quarter)

    normed_mix = rms_norm(full_tokens, gain_mix)

    def project(weight):
        return dot(normed_mix, weight)

    query_rows = project(w_query).reshape(seqs, -1, HEAD)
    key_rows = project(w_key).reshape(seqs, -1, HEAD) * HEAD ** (-0.5)
    value_rows = project(w_value).reshape(seqs, -1, HEAD)
    out_gate = project(w_outgate)
    input_gate = project(w_input_gate)
    carried = jax.nn.log_sigmoid(project(w_forget_gate)) + max_state
    stabilizer = jnp.maximum(carried, input_gate)
    weight_old = jnp.exp(carried - stabilizer)
    weight_new = jnp.exp(input_gate - stabilizer) * jnp.sum(query_rows * key_rows, axis=-1)
    cell_read = jnp.einsum("bhd,bhde->bhe", query_rows, cell_state, precision=highest)
    numerator = weight_old[..., None] * cell_read + weight_new[..., None] * value_rows
    denominator = weight_old * jnp.sum(query_rows * norm_state, axis=-1) + weight_new
    cell_out = numerator / jnp.maximum(jnp.abs(denominator), 1.0)[..., None]
    mixed = (jax.nn.sigmoid(out_gate) * cell_out.reshape(seqs, -1)).astype(bf16)

    all_heads = side_by_side(exchange(to_all(mixed, tp), "x"))
    width = all_heads.shape[1]
    added = jnp.concatenate([dot(all_heads, mix_out[k, :width]) for k in range(tp)], axis=1)
    resid = (full_tokens.astype(f32) + added).astype(bf16)
    normed = rms_norm(resid, gain_ffn)
    own_resid = lax.dynamic_slice_in_dim(resid, me * quarter, quarter, 1)
    mix_row = mix_out[:, width, :].reshape(1, -1)
    mix_logit = jnp.sum(normed.astype(f32) * mix_row.astype(f32), axis=1, keepdims=True)

    flat_ids = route_ids.reshape(-1)
    picks = (flat_ids[:, None] == jnp.arange(experts, dtype=jnp.int32)[None, :]).astype(bf16)
    chosen = picks.reshape(seqs, TOP, experts).sum(axis=1)
    outgoing = lax.dot_general(chosen, normed, (((0,), (0,)), ((), ())), preferred_element_type=f32)
    received = exchange(outgoing.astype(bf16).reshape(experts, 4, -1), EP)

    group = exchange(to_all(normed, near), NEAR).reshape(near * seqs, -1)

    rows = received.reshape(experts, -1)
    hidden = (jax.nn.silu(dot(rows, expert_gate[0])) * dot(rows, expert_up[0])).astype(bf16)
    partial = dot(hidden, expert_down[0]).astype(bf16)
    returned = exchange(partial.reshape(experts * tp, 2, -1), EP + ("x",))

    transposed = (((1,), (1,)), ((), ()))
    gate_cols = lax.dot_general(group, dense[0], transposed, preferred_element_type=f32)
    up_cols = lax.dot_general(group, dense[1], transposed, preferred_element_type=f32)
    dense_hidden = (jax.nn.silu(gate_cols) * up_cols).astype(bf16)
    dense_part = dot(dense_hidden, dense[2]).astype(bf16)
    dense_part = jnp.transpose(dense_part.reshape(near, seqs, tp, quarter), (0, 2, 1, 3))
    dense_sum = exchange(dense_part.reshape(near * tp, seqs, quarter), NEAR + ("x",))
    dense_out = dense_sum.astype(f32).sum(axis=0)

    result = returned.reshape(experts, tp, quarter).astype(f32).sum(axis=1).astype(bf16)
    picked = dot(picks, result).reshape(seqs, TOP, quarter)
    route_weight = jax.nn.sigmoid(route_logits - route_logits[:, ::-1])
    moe = jnp.sum(route_weight[..., None] * picked, axis=1)
    total = own_resid.astype(f32) + moe + jax.nn.sigmoid(mix_logit) * dense_out
    return total.astype(bf16)


def solution(mesh):
    fine = Mesh(mesh.devices.reshape(4, 2, 4, 2, 2, 4), EP + ("x",))
    return jax.shard_map(
        local,
        mesh=fine,
        in_specs=(
            P(EP, "x"),
            P(),
            P(None, "x"),
            P(None, "x"),
            P(None, "x"),
            P(None, "x"),
            P(None, "x"),
            P(None, "x"),
            P(None, "x"),
            P(EP, "x", None, None),
            P(EP, "x", None),
            P(EP, "x"),
            P(),
            P(EP, None),
            P(EP, None),
            P(EP, None, "x"),
            P(EP, None, "x"),
            P(EP, "x", None),
            P("x", EP),
            P("x", EP),
            P(EP, "x"),
            P("x"),
        ),
        out_specs=P(EP, "x"),
        check_vma=False,
    )
```

time: 193 us -> 161 us (0.83)
  waiting for transfers between devices: 96.8 us -> 74.8 us
  between operations: 13.7 us -> 0.49 us
  starting transfers between devices: 54 us -> 57.9 us
  matrix products: 14.1 us -> 11.4 us
    all_gather x2 -> x0, waiting for transfers between devices: 40.7 us -> none  [the longest x1 40.6 us: local(): lax.all_gather(dense_down, 'ep', axis=0, tiled=True)]
    all_to_all x9 -> x8, waiting for transfers between devices: 55.4 us -> 74.8 us  [exchange(): return lax.all_to_all(blocks, axis, 0, 0, tiled=True)]
    all_to_all x9 -> x8, starting transfers between devices: 53.9 us -> 57.9 us  [exchange(): return lax.all_to_all(blocks, axis, 0, 0, tiled=True)]
    dot_general x15 -> x16, matrix products: 13.1 us -> 10.5 us  [the longest x14 9.05 us: dot(): return jnp.dot(a, b, preferred_element_type=f32)]
    unnamed x30 -> x43, local copies, waits for them, and re-layouts: 2.58 us -> 0.19 us
    broadcast_in_dim x7 -> x6, local copies, waits for them, and re-layouts: 4.68 us -> 4.47 us  [the longest x4 3.81 us: to_all(): return jnp.broadcast_to(shard[None], (size, *shard.shape))]
  transfers between devices with their start and end apart: 11 -> 8, of which waited for: 10 -> 8; matrix products, arithmetic and copies ran while one was open for 13% -> 9% of each run, Pallas kernels for 0% -> 0%
where the time goes in v1:
time: 161 us; the launch traced here: 160 us
  waiting for transfers between devices  74.8 us (46%)
  starting transfers between devices  57.9 us (36%)
  matrix products  11.4 us (7%)
  local copies, waits for them, and re-layouts  10.6 us (7%)
  other arithmetic  5.11 us (3%)
    all_to_all x8, waiting for transfers between devices, exchange(): return lax.all_to_all(blocks, axis, 0, 0, tiled=True)  74.8 us
    all_to_all x8, starting transfers between devices, exchange(): return lax.all_to_all(blocks, axis, 0, 0, tiled=True)  57.9 us
    dot_general x14, matrix products, dot(): return jnp.dot(a, b, preferred_element_type=f32)  9.05 us
    broadcast_in_dim x4, local copies, waits for them, and re-layouts, to_all(): return jnp.broadcast_to(shard[None], (size, *shard.shape))  3.81 us
  transfers between devices with their start and end apart: 8, of which 8 were waited for; matrix products, arithmetic and copies ran while one was open for 9% of the time, Pallas kernels for 0%

profile of v1, /device:TPU:1, one launch (start us, length us, event | category | flops | bytes accessed | tf_op | source)
XLA Modules:
  0.0 160.4 jit_solution(4343970267021643378)
XLA Ops:
  0.0 1.4 broadcast_in_dim.12
  1.4 4.8 %all-to-all-start = ((bf16[4,16,256]{2,1,0:T(8,128)(2,1)}), bf16[4,16,256]{2,1,0:T(8,128)(2,1)S(1)}, u32[]{:S(2)}, u32[]{:S(2)}) async-start(bf16[4,16,256]{2,1,0:T(8,128)(2,1)} %broadcast_in_dim.12), calls=%async_computation | async-start | bytes 65536 | tf_op jit(solution)/shard_map/all_to_all | solution.py:20
  6.2 0.7 mul.168
  6.9 0.7 broadcast_in_dim.14
  7.6 0.1 pad.13.clone
  7.7 2.9 %all-to-all-done = bf16[4,16,256]{2,1,0:T(8,128)(2,1)S(1)} async-done(((bf16[4,16,256]{2,1,0:T(8,128)(2,1)}), bf16[4,16,256]{2,1,0:T(8,128)(2,1)S(1)}, u32[]{:S(2)}, u32[]{:S(2)}) %all-to-all-start) | async-done | bytes 32800 | tf_op jit(solution)/shard_map/all_to_all | solution.py:20
  10.6 0.1 fusion.37
  10.7 0.8 multiply_convert_fusion.1
  11.5 0.1 fusion.47
  11.6 1.1 fusion.9
  12.8 1.3 fusion.59
  14.0 0.3 fusion.11
  14.3 1.0 fusion.13
  15.3 0.1 bitcast_add_fusion
  15.4 0.1 maximum_bitcast_fusion.1
  15.6 0.2 fusion.10
  15.7 0.6 broadcast_in_dim.13
  16.3 3.2 %all-to-all-start.1 = ((bf16[4,16,128]{2,1,0:T(8,128)(2,1)}), bf16[4,16,128]{2,1,0:T(8,128)(2,1)S(1)}, u32[]{:S(2)}, u32[]{:S(2)}) async-start(bf16[4,16,128]{2,1,0:T(8,128)(2,1)} %broadcast_in_dim.13), calls=%async_computation.1 | async-start | bytes 32768 | tf_op jit(solution)/shard_map/all_to_all | solution.py:20
  19.6 0.1 maximum_maximum_fusion
  19.7 4.0 %all-to-all-done.1 = bf16[4,16,128]{2,1,0:T(8,128)(2,1)S(1)} async-done(((bf16[4,16,128]{2,1,0:T(8,128)(2,1)}), bf16[4,16,128]{2,1,0:T(8,128)(2,1)S(1)}, u32[]{:S(2)}, u32[]{:S(2)}) %all-to-all-start.1) | async-done | bytes 16416 | tf_op jit(solution)/shard_map/all_to_all | solution.py:20
  23.8 1.1 broadcast_in_dim.16
  24.8 3.6 %all-to-all-start.2 = ((bf16[4,520,256]{2,1,0:T(8,128)(2,1)}), bf16[4,520,256]{2,1,0:T(8,128)(2,1)S(1)}, u32[]{:S(2)}, u32[]{:S(2)}) async-start(bf16[4,520,256]{2,1,0:T(8,128)(2,1)} %broadcast_in_dim.16), calls=%async_computation.2 | async-start | bytes 2129920 | tf_op jit(solution)/shard_map/all_to_all | solution.py:20
  28.6 9.6 %all-to-all-done.2 = bf16[4,520,256]{2,1,0:T(8,128)(2,1)S(1)} async-done(((bf16[4,520,256]{2,1,0:T(8,128)(2,1)}), bf16[4,520,256]{2,1,0:T(8,128)(2,1)S(1)}, u32[]{:S(2)}, u32[]{:S(2)}) %all-to-all-start.2) | async-done | bytes 1064992 | tf_op jit(solution)/shard_map/all_to_all | solution.py:20
  38.3 1.0 tile.11
  39.3 19.0 %all-to-all-start.6 = ((bf16[64,18,256]{2,1,0:T(8,128)(2,1)}), bf16[64,18,256]{2,1,0:T(8,128)(2,1)S(1)}, u32[]{:S(2)}, u32[]{:S(2)}) async-start(bf16[64,18,256]{2,1,0:T(8,128)(2,1)} %bitcast.35), calls=%async_computation.6 | async-start | bytes 1572864 | tf_op jit(solution)/shard_map/all_to_all | solution.py:20
  58.3 0.1 fusion.23
  58.4 0.1 fusion.22
  58.6 0.2 fusion.21
  58.7 0.2 fusion.20
  58.9 0.7 fusion.33
  59.6 0.6 multiply_convert_fusion
  60.3 24.2 %all-to-all-done.6 = bf16[64,18,256]{2,1,0:T(8,128)(2,1)S(1)} async-done(((bf16[64,18,256]{2,1,0:T(8,128)(2,1)}), bf16[64,18,256]{2,1,0:T(8,128)(2,1)S(1)}, u32[]{:S(2)}, u32[]{:S(2)}) %all-to-all-start.6) | async-done | bytes 589856 | tf_op jit(solution)/shard_map/all_to_all | solution.py:20
  84.4 0.7 broadcast_in_dim.17
  85.2 7.7 %all-to-all-start.5 = ((bf16[8,16,1024]{2,1,0:T(8,128)(2,1)}), bf16[8,16,1024]{2,1,0:T(8,128)(2,1)}, u32[]{:S(2)}, u32[]{:S(2)}) async-start(bf16[8,16,1024]{2,1,0:T(8,128)(2,1)} %broadcast_in_dim.17), calls=%async_computation.5 | async-start | bytes 524288 | tf_op jit(solution)/shard_map/all_to_all | solution.py:20
  92.8 0.1 fusion.58
  92.9 0.6 mul.196
  93.5 0.6 add_divide_fusion
  94.1 0.2 convolution_convert_fusion
  94.4 0.9 reshape.268
  95.2 0.1 copy.38
  95.4 0.1 reshape.273
  95.5 3.1 %all-to-all-done.5 = bf16[8,16,1024]{2,1,0:T(8,128)(2,1)} async-done(((bf16[8,16,1024]{2,1,0:T(8,128)(2,1)}), bf16[8,16,1024]{2,1,0:T(8,128)(2,1)}, u32[]{:S(2)}, u32[]{:S(2)}) %all-to-all-start.5) | async-done | bytes 262176 | tf_op jit(solution)/shard_map/all_to_all | solution.py:20
  98.6 6.4 %all-to-all-start.3 = ((bf16[128,4,256]{2,1,0:T(4,128)(2,1)}), bf16[128,4,256]{2,1,0:T(4,128)(2,1)S(1)}, u32[]{:S(2)}, u32[]{:S(2)}) async-start(bf16[128,4,256]{2,1,0:T(4,128)(2,1)} %reshape.268), calls=%async_computation.3 | async-start | bytes 524288 | tf_op jit(solution)/shard_map/all_to_all | solution.py:20
  105.1 0.2 fusion.73
  105.3 0.1 copy.39
  105.4 0.1 copy.40
  105.5 0.1 copy.41
  105.6 1.2 fusion.74
  106.8 1.5 convolution_convert_fusion.1
  108.3 0.2 reshape.274
  108.5 0.7 copy.42
  109.3 11.1 %all-to-all-done.3 = bf16[128,4,256]{2,1,0:T(4,128)(2,1)S(1)} async-done(((bf16[128,4,256]{2,1,0:T(4,128)(2,1)}), bf16[128,4,256]{2,1,0:T(4,128)(2,1)S(1)}, u32[]{:S(2)}, u32[]{:S(2)}) %all-to-all-start.3) | async-done | bytes 262176 | tf_op jit(solution)/shard_map/all_to_all | solution.py:20
  120.4 4.4 %all-to-all-start.7 = ((bf16[32,16,256]{2,1,0:T(8,128)(2,1)}), bf16[32,16,256]{2,1,0:T(8,128)(2,1)S(1)}, u32[]{:S(2)}, u32[]{:S(2)}) async-start(bf16[32,16,256]{2,1,0:T(8,128)(2,1)} %bitcast.38), calls=%async_computation.7 | async-start | bytes 524288 | tf_op jit(solution)/shard_map/all_to_all | solution.py:20
  124.8 1.5 fusion.18
  126.3 2.2 %convolution_convert_fusion.2 = bf16[128,1024]{1,0:T(8,128)(2,1)S(1)} fusion(bf16[128,1024]{1,0:T(8,128)(2,1)S(1)} %bitcast.170, bf16[1,352,1024]{2,1,0:T(8,128)(2,1)} %param.39, bf16[1,1024,352]{1,2,0:T(8,128)(2,1)} %param.38, f32[128,352]{0,1:T(8,128)S(1)} %fusion.18), kind=kOutput, calls=%fused_computation.2 | convolution fusion | flops 184950784 | bytes 2146304 | tf_op jit(solution)/shard_map/dot_general | solution.py:39
  128.6 0.9 reshape.270
  129.4 3.6 %all-to-all-done.7 = bf16[32,16,256]{2,1,0:T(8,128)(2,1)S(1)} async-done(((bf16[32,16,256]{2,1,0:T(8,128)(2,1)}), bf16[32,16,256]{2,1,0:T(8,128)(2,1)S(1)}, u32[]{:S(2)}, u32[]{:S(2)}) %all-to-all-start.7) | async-done | bytes 262176 | tf_op jit(solution)/shard_map/all_to_all | solution.py:20
  133.0 8.6 %all-to-all-start.4 = ((bf16[512,2,128]{2,1,0:T(2,128)(2,1)}), bf16[512,2,128]{2,1,0:T(2,128)(2,1)S(1)}, u32[]{:S(2)}, u32[]{:S(2)}) async-start(bf16[512,2,128]{2,1,0:T(2,128)(2,1)} %reshape.270), calls=%async_computation.4 | async-start | bytes 524288 | tf_op jit(solution)/shard_map/all_to_all | solution.py:20
  141.8 0.2 multiply_reduce_fusion
  142.0 16.3 %all-to-all-done.4 = bf16[512,2,128]{2,1,0:T(2,128)(2,1)S(1)} async-done(((bf16[512,2,128]{2,1,0:T(2,128)(2,1)}), bf16[512,2,128]{2,1,0:T(2,128)(2,1)S(1)}, u32[]{:S(2)}, u32[]{:S(2)}) %all-to-all-start.4) | async-done | bytes 262176 | tf_op jit(solution)/shard_map/all_to_all | solution.py:20
  158.3 0.2 reshape.271
  158.5 0.3 reduce_sum.98
  158.8 0.2 fusion.2
  159.0 1.4 add_convert_fusion
  (59 shorter events, 0.4 us)
Async XLA Ops:
  0.0 14.3 %copy-start = (f32[16,1,128,128]{3,2,1,0:T(8,128)S(1)}, f32[16,1,128,128]{3,2,1,0:T(8,128)}, u32[]{:S(2)}) copy-start(f32[16,1,128,128]{3,2,1,0:T(8,128)} %param.31) | copy-start | bytes 3145732
  0.0 14.0 %copy-start.1 = (bf16[1024,128]{1,0:T(8,128)(2,1)S(1)}, bf16[1024,128]{1,0:T(8,128)(2,1)}, u32[]{:S(2)}) copy-start(bf16[1024,128]{1,0:T(8,128)(2,1)} %param.25) | copy-start | bytes 786436
  1.4 9.1 %all-to-all-start = ((bf16[4,16,256]{2,1,0:T(8,128)(2,1)}), bf16[4,16,256]{2,1,0:T(8,128)(2,1)S(1)}, u32[]{:S(2)}, u32[]{:S(2)}) async-start(bf16[4,16,256]{2,1,0:T(8,128)(2,1)} %broadcast_in_dim.12), calls=%async_computation | async-start | bytes 65536 | tf_op jit(solution)/shard_map/all_to_all | solution.py:20
  11.5 3.8 %copy-start.16 = (bf16[1024,1]{0,1:T(2,128)(2,1)S(1)}, bf16[1024,1]{0,1:T(2,128)(2,1)}, u32[]{:S(2)}) copy-start(bf16[1024,1]{0,1:T(2,128)(2,1)} %param.29) | copy-start | bytes 6148
  11.5 3.8 %copy-start.18 = (f32[16,1]{0,1:T(1,128)S(1)}, f32[16,1]{0,1:T(1,128)}, u32[]{:S(2)}) copy-start(f32[16,1]{0,1:T(1,128)} %param.33) | copy-start | bytes 196
  11.6 3.9 %copy-start.17 = (bf16[1024,1]{0,1:T(2,128)(2,1)S(1)}, bf16[1024,1]{0,1:T(2,128)(2,1)}, u32[]{:S(2)}) copy-start(bf16[1024,1]{0,1:T(2,128)(2,1)} %param.28) | copy-start | bytes 6148
  11.6 4.0 %copy-start.15 = (bf16[1024,128]{1,0:T(8,128)(2,1)S(1)}, bf16[1024,128]{1,0:T(8,128)(2,1)}, u32[]{:S(2)}) copy-start(bf16[1024,128]{1,0:T(8,128)(2,1)} %param.26) | copy-start | bytes 786436
  12.7 6.8 %copy-start.2 = (bf16[512,256]{1,0:T(8,128)(2,1)S(1)}, bf16[512,256]{1,0:T(8,128)(2,1)}, u32[]{:S(2)}) copy-start(bf16[512,256]{1,0:T(8,128)(2,1)} %param.30) | copy-start | bytes 786436
  16.3 7.4 %all-to-all-start.1 = ((bf16[4,16,128]{2,1,0:T(8,128)(2,1)}), bf16[4,16,128]{2,1,0:T(8,128)(2,1)S(1)}, u32[]{:S(2)}, u32[]{:S(2)}) async-start(bf16[4,16,128]{2,1,0:T(8,128)(2,1)} %broadcast_in_dim.13), calls=%async_computation.1 | async-start | bytes 32768 | tf_op jit(solution)/shard_map/all_to_all | solution.py:20
  24.8 3.7 %copy-start.6 = (bf16[256,24]{0,1:T(8,128)(2,1)S(1)}, bf16[256,24]{0,1:T(8,128)(2,1)}, u32[]{:S(2)}) copy-start(bf16[256,24]{0,1:T(8,128)(2,1)} %param.40) | copy-start | bytes 36868
  24.8 3.7 %copy-start.7 = (bf16[256,24]{0,1:T(8,128)(2,1)S(1)}, bf16[256,24]{0,1:T(8,128)(2,1)}, u32[]{:S(2)}) copy-start(bf16[256,24]{0,1:T(8,128)(2,1)} %param.41) | copy-start | bytes 36868
  24.8 3.7 %copy-start.8 = (bf16[24,256]{1,0:T(8,128)(2,1)S(1)}, bf16[24,256]{1,0:T(8,128)(2,1)}, u32[]{:S(2)}) copy-start(bf16[24,256]{1,0:T(8,128)(2,1)} %param.42) | copy-start | bytes 36868
  24.8 13.5 %all-to-all-start.2 = ((bf16[4,520,256]{2,1,0:T(8,128)(2,1)}), bf16[4,520,256]{2,1,0:T(8,128)(2,1)S(1)}, u32[]{:S(2)}, u32[]{:S(2)}) async-start(bf16[4,520,256]{2,1,0:T(8,128)(2,1)} %broadcast_in_dim.16), calls=%async_computation.2 | async-start | bytes 2129920 | tf_op jit(solution)/shard_map/all_to_all | solution.py:20
  39.3 20.4 %copy-start.4 = (f32[1024]{0:T(1024)S(1)}, f32[1024]{0:T(1024)}, u32[]{:S(2)}) copy-start(f32[1024]{0:T(1024)} %param.34) | copy-start | bytes 12292
  39.3 45.2 %all-to-all-start.6 = ((bf16[64,18,256]{2,1,0:T(8,128)(2,1)}), bf16[64,18,256]{2,1,0:T(8,128)(2,1)S(1)}, u32[]{:S(2)}, u32[]{:S(2)}) async-start(bf16[64,18,256]{2,1,0:T(8,128)(2,1)} %bitcast.35), calls=%async_computation.6 | async-start | bytes 1572864 | tf_op jit(solution)/shard_map/all_to_all | solution.py:20
  58.4 34.4 %copy-start.12 = (s32[16,2]{0,1:T(2,128)S(1)}, s32[16,2]{0,1:T(2,128)}, u32[]{:S(2)}) copy-start(s32[16,2]{0,1:T(2,128)} %param.35) | copy-start | bytes 388
  58.4 35.1 %copy-start.9 = (f32[16,2]{0,1:T(2,128)S(1)}, f32[16,2]{0,1:T(2,128)}, u32[]{:S(2)}) copy-start(f32[16,2]{0,1:T(2,128)} %param.36) | copy-start | bytes 388
  59.6 33.9 %copy-start.10 = (f32[16]{0:T(128)}, f32[16]{0:T(128)S(1)}, u32[]{:S(2)}) copy-start(f32[16]{0:T(128)S(1)} %add_rsqrt_fusion) | copy-start | bytes 196
  85.2 13.5 %all-to-all-start.5 = ((bf16[8,16,1024]{2,1,0:T(8,128)(2,1)}), bf16[8,16,1024]{2,1,0:T(8,128)(2,1)}, u32[]{:S(2)}, u32[]{:S(2)}) async-start(bf16[8,16,1024]{2,1,0:T(8,128)(2,1)} %broadcast_in_dim.17), calls=%async_computation.5 | async-start | bytes 524288 | tf_op jit(solution)/shard_map/all_to_all | solution.py:20
  98.6 21.7 %all-to-all-start.3 = ((bf16[128,4,256]{2,1,0:T(4,128)(2,1)}), bf16[128,4,256]{2,1,0:T(4,128)(2,1)S(1)}, u32[]{:S(2)}, u32[]{:S(2)}) async-start(bf16[128,4,256]{2,1,0:T(4,128)(2,1)} %reshape.268), calls=%async_computation.3 | async-start | bytes 524288 | tf_op jit(solution)/shard_map/all_to_all | solution.py:20
  120.4 12.7 %all-to-all-start.7 = ((bf16[32,16,256]{2,1,0:T(8,128)(2,1)}), bf16[32,16,256]{2,1,0:T(8,128)(2,1)S(1)}, u32[]{:S(2)}, u32[]{:S(2)}) async-start(bf16[32,16,256]{2,1,0:T(8,128)(2,1)} %bitcast.38), calls=%async_computation.7 | async-start | bytes 524288 | tf_op jit(solution)/shard_map/all_to_all | solution.py:20
  128.5 13.2 %copy-start.3 = (bf16[16,4,256]{2,0,1:T(8,128)(2,1)S(1)}, bf16[16,4,256]{2,0,1:T(8,128)(2,1)}, u32[]{:S(2)}) copy-start(bf16[16,4,256]{2,0,1:T(8,128)(2,1)} %get-tuple-element.8) | copy-start | bytes 98308
  128.5 13.2 %copy-start.5 = (f32[4,256]{1,0:T(4,128)S(1)}, f32[4,256]{1,0:T(4,128)}, u32[]{:S(2)}) copy-start(f32[4,256]{1,0:T(4,128)} %mul.196) | copy-start | bytes 12292
  128.5 13.2 %copy-start.11 = (f32[16]{0:T(128)S(1)}, f32[16]{0:T(128)}, u32[]{:S(2)}) copy-start(f32[16]{0:T(128)} %copy-done.10) | copy-start | bytes 196
  128.5 30.3 %copy-start.13 = (s32[16,2]{0,1:T(2,128)S(1)}, s32[16,2]{0,1:T(2,128)}, u32[]{:S(2)}) copy-start(s32[16,2]{0,1:T(2,128)} %param.35) | copy-start | bytes 388
  128.6 30.3 %copy-start.14 = (f32[16,2]{0,1:T(2,128)S(1)}, f32[16,2]{0,1:T(2,128)}, u32[]{:S(2)}) copy-start(f32[16,2]{0,1:T(2,128)} %add_divide_fusion) | copy-start | bytes 388
  133.0 25.3 %all-to-all-start.4 = ((bf16[512,2,128]{2,1,0:T(2,128)(2,1)}), bf16[512,2,128]{2,1,0:T(2,128)(2,1)S(1)}, u32[]{:S(2)}, u32[]{:S(2)}) async-start(bf16[512,2,128]{2,1,0:T(2,128)(2,1)} %reshape.270), calls=%async_computation.4 | async-start | bytes 524288 | tf_op jit(solution)/shard_map/all_to_all | solution.py:20

commit v2 on v1

--- a/solution.py
+++ b/solution.py
@@ -5,6 +5,7 @@
 
 HEAD = 128
 TOP = 2
+SLOT = 8
 
 epsilon = 1e-06
 highest = lax.Precision.HIGHEST
@@ -39,7 +40,16 @@
     return jnp.dot(a, b, preferred_element_type=f32)
 
 
-def local(
+def shifted(array, axis, step):
+    size = lax.axis_size(axis)
+    return lax.ppermute(array, axis, [(i, (i + step) % size) for i in range(size)])
+
+
+def swapped(array, axis, flip):
+    return lax.ppermute(array, axis, [(i, i ^ flip) for i in range(lax.axis_size(axis))])
+
+
+def layer(
     tokens,
     gain_mix,
     w_query,
@@ -69,19 +79,27 @@
     near = lax.axis_size(NEAR)
     experts = lax.axis_size(EP)
     me = lax.axis_index("x")
-    columns = dense_gate.shape[1]
-    slim = columns // tp
-
-    full_tokens = side_by_side(exchange(to_all(tokens, tp), "x"))
-
-    extra = jnp.concatenate([dense_mix[None], jnp.zeros((7, quarter), bf16)], axis=0)
-    mix_out = exchange(to_all(jnp.concatenate([w_mix_out, extra], axis=0), tp), "x")
+    place = lax.axis_index(NEAR)
+    slim = dense_gate.shape[1] // tp
 
     packed = jnp.stack([dense_gate.T, dense_up.T, dense_down]).reshape(3, tp, slim, quarter)
-    packed = jnp.moveaxis(packed, 1, 0).reshape(tp, 3 * slim, quarter)
-    dense = exchange(jnp.tile(packed, (far, 1, 1)), FAR + ("x",))
-    dense = dense.reshape(far, tp, 3, slim, quarter)
-    dense = jnp.transpose(dense, (2, 0, 3, 1, 4)).reshape(3, far * slim, tp * quarter)
+    packed = jnp.pad(jnp.moveaxis(packed, 1, 0), ((0, 0), (0, 0), (0, SLOT - slim), (0, 0)))
+    packed = packed.reshape(tp, 3 * SLOT, quarter)
+    last = jnp.pad(dense_mix[None], ((0, 7), (0, 0)))
+    sent = jnp.concatenate([to_all(tokens, tp), packed, to_all(last, tp)], axis=1)
+    first = exchange(sent, "x")
+    full_tokens = side_by_side(first[:, :seqs])
+    mix_row = first[:, seqs + 3 * SLOT].reshape(1, -1)
+
+    mix_out = [w_mix_out]
+    for step in (2, 1, 3):
+        mix_out.append(shifted(w_mix_out, "x", step))
+    mix_out = jnp.stack([mix_out[0], mix_out[2], mix_out[1], mix_out[3]])
+
+    dense = first[None, :, seqs : seqs + 3 * SLOT]
+    for axis, flip in (("zh", 2), ("yh", 2), ("zh", 1), ("yh", 1)):
+        other = swapped(dense, axis, flip)
+        dense = jnp.concatenate([dense, other], axis=0)
 
     normed_mix = rms_norm(full_tokens, gain_mix)
 
@@ -103,49 +121,63 @@
     cell_out = numerator / jnp.maximum(jnp.abs(denominator), 1.0)[..., None]
     mixed = (jax.nn.sigmoid(out_gate) * cell_out.reshape(seqs, -1)).astype(bf16)
 
-    all_heads = side_by_side(exchange(to_all(mixed, tp), "x"))
-    width = all_heads.shape[1]
-    added = jnp.concatenate([dot(all_heads, mix_out[k, :width]) for k in range(tp)], axis=1)
-    resid = (full_tokens.astype(f32) + added).astype(bf16)
-    normed = rms_norm(resid, gain_ffn)
-    own_resid = lax.dynamic_slice_in_dim(resid, me * quarter, quarter, 1)
-    mix_row = mix_out[:, width, :].reshape(1, -1)
-    mix_logit = jnp.sum(normed.astype(f32) * mix_row.astype(f32), axis=1, keepdims=True)
+    sent = to_all(jnp.concatenate([mixed, tokens], axis=1), near * tp)
+    second = exchange(sent, NEAR + ("x",))
+    second = second.reshape(near, tp, seqs, HEAD + quarter)
+    all_heads = jnp.concatenate(
+        [second[:, k, :, :HEAD].reshape(near * seqs, HEAD) for k in range(tp)], axis=1
+    )
+    resid = []
+    for k in range(tp):
+        added = dot(all_heads, lax.dynamic_index_in_dim(mix_out, (me - k) % tp, 0, False))
+        old = second[:, k, :, HEAD:].reshape(near * seqs, quarter)
+        resid.append((old.astype(f32) + added).astype(bf16))
+    resid = jnp.concatenate(resid, axis=1)
+    group = rms_norm(resid, gain_ffn)
+    normed = lax.dynamic_slice_in_dim(group, place * seqs, seqs, 0)
+    own_resid = lax.dynamic_slice(resid, (place * seqs, me * quarter), (seqs, quarter))
 
     flat_ids = route_ids.reshape(-1)
     picks = (flat_ids[:, None] == jnp.arange(experts, dtype=jnp.int32)[None, :]).astype(bf16)
     chosen = picks.reshape(seqs, TOP, experts).sum(axis=1)
     outgoing = lax.dot_general(chosen, normed, (((0,), (0,)), ((), ())), preferred_element_type=f32)
-    received = exchange(outgoing.astype(bf16).reshape(experts, 4, -1), EP)
-
-    group = exchange(to_all(normed, near), NEAR).reshape(near * seqs, -1)
+    outgoing = outgoing.astype(bf16).reshape(experts, 4, -1)
+    received = exchange(outgoing, EP)
 
     rows = received.reshape(experts, -1)
     hidden = (jax.nn.silu(dot(rows, expert_gate[0])) * dot(rows, expert_up[0])).astype(bf16)
-    partial = dot(hidden, expert_down[0]).astype(bf16)
-    returned = exchange(partial.reshape(experts * tp, 2, -1), EP + ("x",))
+    partial = dot(hidden, expert_down[0]).astype(bf16).reshape(experts, 4, -1)
+    returned = exchange(partial, EP)
+
+    def matrix(place):
+        part = dense[:, :, place * SLOT : (place + 1) * SLOT]
+        return jnp.moveaxis(part, 1, 2).reshape(far * SLOT, tp * quarter)
 
     transposed = (((1,), (1,)), ((), ()))
-    gate_cols = lax.dot_general(group, dense[0], transposed, preferred_element_type=f32)
-    up_cols = lax.dot_general(group, dense[1], transposed, preferred_element_type=f32)
+    gate_cols = lax.dot_general(group, matrix(0), transposed, preferred_element_type=f32)
+    up_cols = lax.dot_general(group, matrix(1), transposed, preferred_element_type=f32)
     dense_hidden = (jax.nn.silu(gate_cols) * up_cols).astype(bf16)
-    dense_part = dot(dense_hidden, dense[2]).astype(bf16)
-    dense_part = jnp.transpose(dense_part.reshape(near, seqs, tp, quarter), (0, 2, 1, 3))
-    dense_sum = exchange(dense_part.reshape(near * tp, seqs, quarter), NEAR + ("x",))
-    dense_out = dense_sum.astype(f32).sum(axis=0)
-
-    result = returned.reshape(experts, tp, quarter).astype(f32).sum(axis=1).astype(bf16)
-    picked = dot(picks, result).reshape(seqs, TOP, quarter)
+    dense_part = dot(dense_hidden, matrix(2)).reshape(near, seqs, -1)
+
+    picked = dot(picks, returned.reshape(experts, -1)).reshape(seqs, TOP, -1)
     route_weight = jax.nn.sigmoid(route_logits - route_logits[:, ::-1])
     moe = jnp.sum(route_weight[..., None] * picked, axis=1)
-    total = own_resid.astype(f32) + moe + jax.nn.sigmoid(mix_logit) * dense_out
+    mix_gate = jax.nn.sigmoid(
+        jnp.sum(group.astype(f32) * mix_row.astype(f32), axis=1, keepdims=True)
+    ).reshape(near, seqs, 1)
+    mine = (jnp.arange(near) == place)[:, None, None]
+    part = mix_gate * dense_part + jnp.where(mine, moe[None], 0.0)
+    part = jnp.swapaxes(part.astype(bf16).reshape(near, seqs, tp, quarter), 1, 2)
+    part = part.reshape(near * tp, seqs, quarter)
+    parts = exchange(part, NEAR + ("x",))
+    total = own_resid.astype(f32) + parts.astype(f32).sum(axis=0)
     return total.astype(bf16)
 
 
 def solution(mesh):
     fine = Mesh(mesh.devices.reshape(4, 2, 4, 2, 2, 4), EP + ("x",))
     return jax.shard_map(
-        local,
+        layer,
         mesh=fine,
         in_specs=(
             P(EP, "x"),

time: 161 us -> 152 us (0.944)
  waiting for transfers between devices: 74.8 us -> 51.8 us
  starting transfers between devices: 57.9 us -> 71.3 us
  local copies, waits for them, and re-layouts: 10.6 us -> 14.5 us
  matrix products: 11.4 us -> 7.53 us
    all_to_all x8 -> x5, waiting for transfers between devices: 74.8 us -> 35.6 us  [exchange(): return lax.all_to_all(blocks, axis, 0, 0, tiled=True)]
    ppermute x0 -> x7, starting transfers between devices: none -> 34.2 us  [the longest x4 23.9 us: swapped(): lax.ppermute(array, axis, [(i, i ^ flip) for i in range(lax.axis_size(axi...]
    all_to_all x8 -> x5, starting transfers between devices: 57.9 us -> 37.1 us  [exchange(): return lax.all_to_all(blocks, axis, 0, 0, tiled=True)]
    ppermute x0 -> x7, waiting for transfers between devices: none -> 16.3 us  [the longest x4 16.3 us: swapped(): lax.ppermute(array, axis, [(i, i ^ flip) for i in range(lax.axis_size(axi...]
    unnamed x43 -> x49, local copies, waits for them, and re-layouts: 0.19 us -> 8.31 us
    dot_general x14, matrix products: 9.05 us -> 5.84 us  [dot(): return jnp.dot(a, b, preferred_element_type=f32)]
    broadcast_in_dim x4 -> x3, local copies, waits for them, and re-layouts: 3.81 us -> 0.8 us  [to_all(): return jnp.broadcast_to(shard[None], (size, *shard.shape))]
    another operation x0 -> x2, other arithmetic: none -> 1.96 us  [the longest x1 1.24 us: layer(): mix_out = jnp.stack([mix_out[0], mix_out[2], mix_out[1], mix_out[3]])]
  transfers between devices with their start and end apart: 8 -> 12, of which waited for: 8 -> 8; matrix products, arithmetic and copies ran while one was open for 9% -> 8% of each run, Pallas kernels for 0% -> 0%
where the time goes in v2:
time: 152 us; the launch traced here: 151 us
  starting transfers between devices  71.3 us (47%)
  waiting for transfers between devices  51.8 us (34%)
  local copies, waits for them, and re-layouts  14.5 us (10%)
  matrix products  7.53 us (5%)
  other arithmetic  4.89 us (3%)
    all_to_all x5, starting transfers between devices, exchange(): return lax.all_to_all(blocks, axis, 0, 0, tiled=True)  37.1 us
    all_to_all x5, waiting for transfers between devices, exchange(): return lax.all_to_all(blocks, axis, 0, 0, tiled=True)  35.6 us
    ppermute x4, starting transfers between devices, swapped(): lax.ppermute(array, axis, [(i, i ^ flip) for i in range(lax.axis_size(axi...  23.9 us
    ppermute x4, waiting for transfers between devices, swapped(): lax.ppermute(array, axis, [(i, i ^ flip) for i in range(lax.axis_size(axi...  16.3 us
    ppermute x3, starting transfers between devices, shifted(): lax.ppermute(array, axis, [(i, (i + step) % size) for i in range(size)])  10.3 us
    unnamed x49, local copies, waits for them, and re-layouts  8.31 us
    dot_general x14, matrix products, dot(): return jnp.dot(a, b, preferred_element_type=f32)  5.84 us
  transfers between devices with their start and end apart: 12, of which 8 were waited for; matrix products, arithmetic and copies ran while one was open for 8% of the time, Pallas kernels for 0%

profile of v2, /device:TPU:1, one launch (start us, length us, event | category | flops | bytes accessed | tf_op | source)
XLA Modules:
  0.0 150.6 jit_solution(13659204237879195848)
XLA Ops:
  0.0 5.3 %collective-permute-start.2 = (bf16[512,256]{1,0:T(8,128)(2,1)}, bf16[512,256]{1,0:T(8,128)(2,1)}, u32[]{:S(2)}, u32[]{:S(2)}) collective-permute-start(bf16[512,256]{1,0:T(8,128)(2,1)} %param.30), channel_id=1, source_target_pairs={{0,3},{1,0},{2,1},{3,2},{4,7},{5,4},{6,5},{7,6},{8,11},{9,8},{10,9... | collective-permute-start | bytes 786440 | tf_op jit(solution)/shard_map/ppermute | solution.py:45
  5.3 2.4 %collective-permute-start.1 = (bf16[512,256]{1,0:T(8,128)(2,1)}, bf16[512,256]{1,0:T(8,128)(2,1)}, u32[]{:S(2)}, u32[]{:S(2)}) collective-permute-start(bf16[512,256]{1,0:T(8,128)(2,1)} %param.30), channel_id=1, source_target_pairs={{0,2},{1,3},{2,0},{3,1},{4,6},{5,7},{6,4},{7,5},{8,10},{9,11},{10,... | collective-permute-start | bytes 786440 | tf_op jit(solution)/shard_map/ppermute | solution.py:45
  7.8 2.5 %collective-permute-start = (bf16[512,256]{1,0:T(8,128)(2,1)}, bf16[512,256]{1,0:T(8,128)(2,1)S(1)}, u32[]{:S(2)}, u32[]{:S(2)}) collective-permute-start(bf16[512,256]{1,0:T(8,128)(2,1)} %param.30), channel_id=1, source_target_pairs={{0,1},{1,2},{2,3},{3,0},{4,5},{5,6},{6,7},{7,4},{8,9},{9,10},{10,1... | collective-permute-start | bytes 786440 | tf_op jit(solution)/shard_map/ppermute | solution.py:45
  10.3 0.7 broadcast_in_dim.24
  11.0 0.7 stack.29
  11.7 0.7 copy-done.13
  12.5 0.7 copy-done.10
  13.2 0.6 pad_maximum_fusion.6
  13.8 3.3 %all-to-all-start = ((bf16[4,48,256]{2,1,0:T(8,128)(2,1)}), bf16[4,48,256]{2,1,0:T(8,128)(2,1)S(1)}, u32[]{:S(2)}, u32[]{:S(2)}) async-start(bf16[4,48,256]{2,1,0:T(8,128)(2,1)} %pad_maximum_fusion.6), calls=%async_computation | async-start | bytes 196608 | tf_op jit(solution)/shard_map/all_to_all | solution.py:21
  17.2 0.7 copy-done.11
  17.9 0.7 copy-done.16
  18.6 0.7 copy-done.17
  19.4 3.0 %all-to-all-done = bf16[4,48,256]{2,1,0:T(8,128)(2,1)S(1)} async-done(((bf16[4,48,256]{2,1,0:T(8,128)(2,1)}), bf16[4,48,256]{2,1,0:T(8,128)(2,1)S(1)}, u32[]{:S(2)}, u32[]{:S(2)}) %all-to-all-start) | async-done | bytes 98336 | tf_op jit(solution)/shard_map/all_to_all | solution.py:21
  22.7 0.2 fusion.14
  22.8 0.6 copy-done.5
  23.4 0.3 fusion.51
  23.7 0.3 fusion.16
  24.0 1.0 fusion.18
  25.0 0.7 copy-done.21
  25.6 0.1 bitcast_add_fusion
  25.8 0.5 copy-done.20
  26.5 0.2 fusion.15
  26.6 0.8 broadcast_in_dim.26
  27.4 10.7 %all-to-all-start.1 = ((bf16[32,16,384]{2,1,0:T(8,128)(2,1)}), bf16[32,16,384]{2,1,0:T(8,128)(2,1)S(1)}, u32[]{:S(2)}, u32[]{:S(2)}) async-start(bf16[32,16,384]{2,1,0:T(8,128)(2,1)} %broadcast_in_dim.26), calls=%async_computation.1 | async-start | bytes 786432 | tf_op jit(solution)/shard_map/all_to_all | solution.py:21
  38.1 6.9 %collective-permute-start.3 = (bf16[1,4,24,256]{3,2,1,0:T(8,128)(2,1)S(1)}, bf16[1,4,24,256]{3,2,1,0:T(8,128)(2,1)S(1)}, u32[]{:S(2)}, u32[]{:S(2)}) collective-permute-start(bf16[1,4,24,256]{3,2,1,0:T(8,128)(2,1)S(1)} %slice_bitcast_fusion), channel_id=1, source_target_pairs={{0,256},{128,384},{256,0},{384,128},{1,257},{129,385},{257,1},{385... | collective-permute-start | bytes 147464 | tf_op jit(solution)/shard_map/ppermute | solution.py:49
  45.0 4.0 %collective-permute-done.3 = bf16[1,4,24,256]{3,2,1,0:T(8,128)(2,1)S(1)} collective-permute-done((bf16[1,4,24,256]{3,2,1,0:T(8,128)(2,1)S(1)}, bf16[1,4,24,256]{3,2,1,0:T(8,128)(2,1)S(1)}, u32[]{:S(2)}, u32[]{:S(2)}) %collective-permute-start.3) | collective-permute-done | bytes 49184 | tf_op jit(solution)/shard_map/ppermute | solution.py:49
  49.0 6.7 %collective-permute-start.4 = (bf16[2,4,24,256]{3,2,1,0:T(8,128)(2,1)S(1)}, bf16[2,4,24,256]{3,2,1,0:T(8,128)(2,1)S(1)}, u32[]{:S(2)}, u32[]{:S(2)}) collective-permute-start(bf16[2,4,24,256]{3,2,1,0:T(8,128)(2,1)S(1)} %pad_maximum_fusion.7), channel_id=1, source_target_pairs={{0,32},{16,48},{32,0},{48,16},{1,33},{17,49},{33,1},{49,17},{2,34}... | collective-permute-start | bytes 294920 | tf_op jit(solution)/shard_map/ppermute | solution.py:49
  55.7 2.8 %collective-permute-done.4 = bf16[2,4,24,256]{3,2,1,0:T(8,128)(2,1)S(1)} collective-permute-done((bf16[2,4,24,256]{3,2,1,0:T(8,128)(2,1)S(1)}, bf16[2,4,24,256]{3,2,1,0:T(8,128)(2,1)S(1)}, u32[]{:S(2)}, u32[]{:S(2)}) %collective-permute-start.4) | collective-permute-done | bytes 98336 | tf_op jit(solution)/shard_map/ppermute | solution.py:49
  58.5 5.5 %collective-permute-start.5 = (bf16[4,4,24,256]{3,2,1,0:T(8,128)(2,1)S(1)}, bf16[4,4,24,256]{3,2,1,0:T(8,128)(2,1)S(1)}, u32[]{:S(2)}, u32[]{:S(2)}) collective-permute-start(bf16[4,4,24,256]{3,2,1,0:T(8,128)(2,1)S(1)} %pad_maximum_fusion.4), channel_id=1, source_target_pairs={{0,128},{128,0},{256,384},{384,256},{1,129},{129,1},{257,385},{385... | collective-permute-start | bytes 589832 | tf_op jit(solution)/shard_map/ppermute | solution.py:49
  64.1 0.7 copy-done.9
  64.8 1.2 pad_maximum_fusion
  66.0 7.5 %collective-permute-done.5 = bf16[4,4,24,256]{3,2,1,0:T(8,128)(2,1)S(1)} collective-permute-done((bf16[4,4,24,256]{3,2,1,0:T(8,128)(2,1)S(1)}, bf16[4,4,24,256]{3,2,1,0:T(8,128)(2,1)S(1)}, u32[]{:S(2)}, u32[]{:S(2)}) %collective-permute-start.5) | collective-permute-done | bytes 196640 | tf_op jit(solution)/shard_map/ppermute | solution.py:49
  73.5 0.8 pad_maximum_fusion.1
  74.3 4.9 %collective-permute-start.6 = (bf16[8,4,24,256]{3,2,1,0:T(8,128)(2,1)}, bf16[8,4,24,256]{3,2,1,0:T(8,128)(2,1)}, u32[]{:S(2)}, u32[]{:S(2)}) collective-permute-start(bf16[8,4,24,256]{3,2,1,0:T(8,128)(2,1)} %pad_maximum_fusion.1), channel_id=1, source_target_pairs={{0,16},{16,0},{32,48},{48,32},{1,17},{17,1},{33,49},{49,33},{2,18}... | collective-permute-start | bytes 1179656 | tf_op jit(solution)/shard_map/ppermute | solution.py:49
  79.3 0.2 fusion.7
  79.5 0.2 fusion.6
  79.7 0.2 fusion.5
  79.9 0.2 fusion.4
  80.1 0.1 fusion.25
  80.3 0.7 copy-done.15
  81.0 0.2 multiply_reduce_fusion
  81.2 0.2 convolution_convert_fusion
  81.5 0.9 reshape.216
  82.3 11.9 %all-to-all-start.2 = ((bf16[128,4,256]{2,1,0:T(4,128)(2,1)}), bf16[128,4,256]{2,1,0:T(4,128)(2,1)S(1)}, u32[]{:S(2)}, u32[]{:S(2)}) async-start(bf16[128,4,256]{2,1,0:T(4,128)(2,1)} %reshape.216), calls=%async_computation.2 | async-start | bytes 524288 | tf_op jit(solution)/shard_map/all_to_all | solution.py:21
  94.3 0.9 copy-done.2
  95.2 2.0 %collective-permute-done.6 = bf16[8,4,24,256]{3,2,1,0:T(8,128)(2,1)} collective-permute-done((bf16[8,4,24,256]{3,2,1,0:T(8,128)(2,1)}, bf16[8,4,24,256]{3,2,1,0:T(8,128)(2,1)}, u32[]{:S(2)}, u32[]{:S(2)}) %collective-permute-start.6) | collective-permute-done | bytes 393248 | tf_op jit(solution)/shard_map/ppermute | solution.py:49
  97.3 1.0 constant_dynamic-update-slice_fusion
  98.3 0.8 fusion.68
  99.1 10.4 %all-to-all-done.2 = bf16[128,4,256]{2,1,0:T(4,128)(2,1)S(1)} async-done(((bf16[128,4,256]{2,1,0:T(4,128)(2,1)}), bf16[128,4,256]{2,1,0:T(4,128)(2,1)S(1)}, u32[]{:S(2)}, u32[]{:S(2)}) %all-to-all-start.2) | async-done | bytes 262176 | tf_op jit(solution)/shard_map/all_to_all | solution.py:21
  109.6 1.5 %fusion.23 = f32[128,352]{0,1:T(8,128)S(1)} fusion(bf16[128,1024]{1,0:T(8,128)(2,1)S(1)} %bitcast.143, bf16[1,1024,352]{1,2,0:T(8,128)(2,1)} %param.37), kind=kOutput, calls=%fused_computation.37 | convolution fusion | flops 92274688 | bytes 1163264 | tf_op jit(solution)/shard_map/dot_general | solution.py:40
  111.1 2.0 %convolution_convert_fusion.1 = bf16[128,1024]{1,0:T(8,128)(2,1)S(1)} fusion(bf16[128,1024]{1,0:T(8,128)(2,1)S(1)} %bitcast.144, bf16[1,352,1024]{2,1,0:T(8,128)(2,1)S(1)} %copy-done.3, bf16[1,1024,352]{1,2,0:T(8,128)(2,1)} %param.38, f32[128,352]{0,1:T(8,128)S(1)} %fusion.23), kind=kOutput, calls=%fused_computation.4 | convolution fusion | flops 184950784 | bytes 2146304 | tf_op jit(solution)/shard_map/dot_general | solution.py:40
  113.1 0.9 reshape.218
  114.0 6.3 %all-to-all-start.3 = ((bf16[128,4,256]{2,1,0:T(4,128)(2,1)}), bf16[128,4,256]{2,1,0:T(4,128)(2,1)S(1)}, u32[]{:S(2)}, u32[]{:S(2)}) async-start(bf16[128,4,256]{2,1,0:T(4,128)(2,1)} %reshape.218), calls=%async_computation.3 | async-start | bytes 524288 | tf_op jit(solution)/shard_map/all_to_all | solution.py:21
  120.4 0.2 fusion.72
  120.6 0.7 copy-done.7
  121.3 0.2 multiply_convert_fusion
  121.6 13.9 %all-to-all-done.3 = bf16[128,4,256]{2,1,0:T(4,128)(2,1)S(1)} async-done(((bf16[128,4,256]{2,1,0:T(4,128)(2,1)}), bf16[128,4,256]{2,1,0:T(4,128)(2,1)S(1)}, u32[]{:S(2)}, u32[]{:S(2)}) %all-to-all-start.3) | async-done | bytes 262176 | tf_op jit(solution)/shard_map/all_to_all | solution.py:21
  135.5 0.2 reshape.234
  135.7 0.2 fusion.3
  135.9 0.2 fusion.1
  136.2 0.7 pad_maximum_fusion.3
  136.9 4.8 %all-to-all-start.4 = ((bf16[32,16,256]{2,1,0:T(8,128)(2,1)}), bf16[32,16,256]{2,1,0:T(8,128)(2,1)S(1)}, u32[]{:S(2)}, u32[]{:S(2)}) async-start(bf16[32,16,256]{2,1,0:T(8,128)(2,1)} %bitcast.53), calls=%async_computation.4 | async-start | bytes 524288 | tf_op jit(solution)/shard_map/all_to_all | solution.py:21
  141.7 8.2 %all-to-all-done.4 = bf16[32,16,256]{2,1,0:T(8,128)(2,1)S(1)} async-done(((bf16[32,16,256]{2,1,0:T(8,128)(2,1)}), bf16[32,16,256]{2,1,0:T(8,128)(2,1)S(1)}, u32[]{:S(2)}, u32[]{:S(2)}) %all-to-all-start.4) | async-done | bytes 262176 | tf_op jit(solution)/shard_map/all_to_all | solution.py:21
  150.0 0.6 add_convert_fusion
  (72 shorter events, 1.0 us)
Async XLA Ops:
  0.0 24.0 %copy-start = (f32[16,1,128,128]{3,2,1,0:T(8,128)S(1)}, f32[16,1,128,128]{3,2,1,0:T(8,128)}, u32[]{:S(2)}) copy-start(f32[16,1,128,128]{3,2,1,0:T(8,128)} %param.31) | copy-start | bytes 3145732
  0.0 64.0 %collective-permute-start.2 = (bf16[512,256]{1,0:T(8,128)(2,1)}, bf16[512,256]{1,0:T(8,128)(2,1)}, u32[]{:S(2)}, u32[]{:S(2)}) collective-permute-start(bf16[512,256]{1,0:T(8,128)(2,1)} %param.30), channel_id=1, source_target_pairs={{0,3},{1,0},{2,1},{3,2},{4,7},{5,4},{6,5},{7,6},{8,11},{9,8},{10,9... | collective-permute-start | bytes 786440 | tf_op jit(solution)/shard_map/ppermute | solution.py:45
  5.3 58.7 %collective-permute-start.1 = (bf16[512,256]{1,0:T(8,128)(2,1)}, bf16[512,256]{1,0:T(8,128)(2,1)}, u32[]{:S(2)}, u32[]{:S(2)}) collective-permute-start(bf16[512,256]{1,0:T(8,128)(2,1)} %param.30), channel_id=1, source_target_pairs={{0,2},{1,3},{2,0},{3,1},{4,6},{5,7},{6,4},{7,5},{8,10},{9,11},{10,... | collective-permute-start | bytes 786440 | tf_op jit(solution)/shard_map/ppermute | solution.py:45
  7.8 56.3 %collective-permute-start = (bf16[512,256]{1,0:T(8,128)(2,1)}, bf16[512,256]{1,0:T(8,128)(2,1)S(1)}, u32[]{:S(2)}, u32[]{:S(2)}) collective-permute-start(bf16[512,256]{1,0:T(8,128)(2,1)} %param.30), channel_id=1, source_target_pairs={{0,1},{1,2},{2,3},{3,0},{4,5},{5,6},{6,7},{7,4},{8,9},{9,10},{10,1... | collective-permute-start | bytes 786440 | tf_op jit(solution)/shard_map/ppermute | solution.py:45
  11.0 0.7 copy-start.12
  11.7 0.7 copy-start.13
  12.5 0.7 copy-start.10
  13.8 8.5 %all-to-all-start = ((bf16[4,48,256]{2,1,0:T(8,128)(2,1)}), bf16[4,48,256]{2,1,0:T(8,128)(2,1)S(1)}, u32[]{:S(2)}, u32[]{:S(2)}) async-start(bf16[4,48,256]{2,1,0:T(8,128)(2,1)} %pad_maximum_fusion.6), calls=%async_computation | async-start | bytes 196608 | tf_op jit(solution)/shard_map/all_to_all | solution.py:21
  17.2 0.7 copy-start.11
  17.9 0.7 copy-start.16
  18.6 0.7 copy-start.17
  18.6 4.0 %copy-start.4 = (bf16[1024,128]{1,0:T(8,128)(2,1)S(1)}, bf16[1024,128]{1,0:T(8,128)(2,1)}, u32[]{:S(2)}) copy-start(bf16[1024,128]{1,0:T(8,128)(2,1)} %param.27) | copy-start | bytes 786436
  22.5 1.0 copy-start.5
  22.7 0.8 copy-start.14
  22.7 1.0 copy-start.6
  24.0 1.0 copy-start.19
  24.0 2.5 %copy-start.18 = (bf16[1024,128]{1,0:T(8,128)(2,1)S(1)}, bf16[1024,128]{1,0:T(8,128)(2,1)}, u32[]{:S(2)}) copy-start(bf16[1024,128]{1,0:T(8,128)(2,1)} %param.26) | copy-start | bytes 786436
  25.0 0.7 copy-start.21
  25.6 0.7 copy-start.20
  27.4 51.8 %all-to-all-start.1 = ((bf16[32,16,384]{2,1,0:T(8,128)(2,1)}), bf16[32,16,384]{2,1,0:T(8,128)(2,1)S(1)}, u32[]{:S(2)}, u32[]{:S(2)}) async-start(bf16[32,16,384]{2,1,0:T(8,128)(2,1)} %broadcast_in_dim.26), calls=%async_computation.1 | async-start | bytes 786432 | tf_op jit(solution)/shard_map/all_to_all | solution.py:21
  38.1 10.9 %collective-permute-start.3 = (bf16[1,4,24,256]{3,2,1,0:T(8,128)(2,1)S(1)}, bf16[1,4,24,256]{3,2,1,0:T(8,128)(2,1)S(1)}, u32[]{:S(2)}, u32[]{:S(2)}) collective-permute-start(bf16[1,4,24,256]{3,2,1,0:T(8,128)(2,1)S(1)} %slice_bitcast_fusion), channel_id=1, source_target_pairs={{0,256},{128,384},{256,0},{384,128},{1,257},{129,385},{257,1},{385... | collective-permute-start | bytes 147464 | tf_op jit(solution)/shard_map/ppermute | solution.py:49
  49.0 15.8 %copy-start.8 = (bf16[512,256]{1,0:T(8,128)(2,1)S(1)}, bf16[512,256]{1,0:T(8,128)(2,1)}, u32[]{:S(2)}) copy-start(bf16[512,256]{1,0:T(8,128)(2,1)} %param.30) | copy-start | bytes 786436
  49.0 9.5 %collective-permute-start.4 = (bf16[2,4,24,256]{3,2,1,0:T(8,128)(2,1)S(1)}, bf16[2,4,24,256]{3,2,1,0:T(8,128)(2,1)S(1)}, u32[]{:S(2)}, u32[]{:S(2)}) collective-permute-start(bf16[2,4,24,256]{3,2,1,0:T(8,128)(2,1)S(1)} %pad_maximum_fusion.7), channel_id=1, source_target_pairs={{0,32},{16,48},{32,0},{48,16},{1,33},{17,49},{33,1},{49,17},{2,34}... | collective-permute-start | bytes 294920 | tf_op jit(solution)/shard_map/ppermute | solution.py:49
  58.5 15.0 %collective-permute-start.5 = (bf16[4,4,24,256]{3,2,1,0:T(8,128)(2,1)S(1)}, bf16[4,4,24,256]{3,2,1,0:T(8,128)(2,1)S(1)}, u32[]{:S(2)}, u32[]{:S(2)}) collective-permute-start(bf16[4,4,24,256]{3,2,1,0:T(8,128)(2,1)S(1)} %pad_maximum_fusion.4), channel_id=1, source_target_pairs={{0,128},{128,0},{256,384},{384,256},{1,129},{129,1},{257,385},{385... | collective-permute-start | bytes 589832 | tf_op jit(solution)/shard_map/ppermute | solution.py:49
  64.1 0.7 copy-start.9
  73.5 0.8 copy-start.1
  74.3 23.0 %collective-permute-start.6 = (bf16[8,4,24,256]{3,2,1,0:T(8,128)(2,1)}, bf16[8,4,24,256]{3,2,1,0:T(8,128)(2,1)}, u32[]{:S(2)}, u32[]{:S(2)}) collective-permute-start(bf16[8,4,24,256]{3,2,1,0:T(8,128)(2,1)} %pad_maximum_fusion.1), channel_id=1, source_target_pairs={{0,16},{16,0},{32,48},{48,32},{1,17},{17,1},{33,49},{49,33},{2,18}... | collective-permute-start | bytes 1179656 | tf_op jit(solution)/shard_map/ppermute | solution.py:49
  80.3 0.7 copy-start.15
  82.3 27.2 %all-to-all-start.2 = ((bf16[128,4,256]{2,1,0:T(4,128)(2,1)}), bf16[128,4,256]{2,1,0:T(4,128)(2,1)S(1)}, u32[]{:S(2)}, u32[]{:S(2)}) async-start(bf16[128,4,256]{2,1,0:T(4,128)(2,1)} %reshape.216), calls=%async_computation.2 | async-start | bytes 524288 | tf_op jit(solution)/shard_map/all_to_all | solution.py:21
  94.3 0.9 copy-start.2
  109.5 1.6 %copy-start.3 = (bf16[1,352,1024]{2,1,0:T(8,128)(2,1)S(1)}, bf16[1,352,1024]{2,1,0:T(8,128)(2,1)}, u32[]{:S(2)}) copy-start(bf16[1,352,1024]{2,1,0:T(8,128)(2,1)} %param.39) | copy-start | bytes 2162692
  114.0 21.5 %all-to-all-start.3 = ((bf16[128,4,256]{2,1,0:T(4,128)(2,1)}), bf16[128,4,256]{2,1,0:T(4,128)(2,1)S(1)}, u32[]{:S(2)}, u32[]{:S(2)}) async-start(bf16[128,4,256]{2,1,0:T(4,128)(2,1)} %reshape.218), calls=%async_computation.3 | async-start | bytes 524288 | tf_op jit(solution)/shard_map/all_to_all | solution.py:21
  120.4 1.0 copy-start.7
  136.9 13.1 %all-to-all-start.4 = ((bf16[32,16,256]{2,1,0:T(8,128)(2,1)}), bf16[32,16,256]{2,1,0:T(8,128)(2,1)S(1)}, u32[]{:S(2)}, u32[]{:S(2)}) async-start(bf16[32,16,256]{2,1,0:T(8,128)(2,1)} %bitcast.53), calls=%async_computation.4 | async-start | bytes 524288 | tf_op jit(solution)/shard_map/all_to_all | solution.py:21

commit v3 on v2

--- a/solution.py
+++ b/solution.py
@@ -5,7 +5,6 @@
 
 HEAD = 128
 TOP = 2
-SLOT = 8
 
 epsilon = 1e-06
 highest = lax.Precision.HIGHEST
@@ -45,10 +44,6 @@
     return lax.ppermute(array, axis, [(i, (i + step) % size) for i in range(size)])
 
 
-def swapped(array, axis, flip):
-    return lax.ppermute(array, axis, [(i, i ^ flip) for i in range(lax.axis_size(axis))])
-
-
 def layer(
     tokens,
     gain_mix,
@@ -83,23 +78,22 @@
     slim = dense_gate.shape[1] // tp
 
     packed = jnp.stack([dense_gate.T, dense_up.T, dense_down]).reshape(3, tp, slim, quarter)
-    packed = jnp.pad(jnp.moveaxis(packed, 1, 0), ((0, 0), (0, 0), (0, SLOT - slim), (0, 0)))
-    packed = packed.reshape(tp, 3 * SLOT, quarter)
-    last = jnp.pad(dense_mix[None], ((0, 7), (0, 0)))
+    packed = jnp.moveaxis(packed, 1, 0).reshape(tp, 3 * slim, quarter)
+    last = jnp.pad(dense_mix[None], ((0, 5), (0, 0)))
     sent = jnp.concatenate([to_all(tokens, tp), packed, to_all(last, tp)], axis=1)
     first = exchange(sent, "x")
     full_tokens = side_by_side(first[:, :seqs])
-    mix_row = first[:, seqs + 3 * SLOT].reshape(1, -1)
+    mix_row = first[:, seqs + 3 * slim].reshape(1, -1)
 
     mix_out = [w_mix_out]
     for step in (2, 1, 3):
         mix_out.append(shifted(w_mix_out, "x", step))
     mix_out = jnp.stack([mix_out[0], mix_out[2], mix_out[1], mix_out[3]])
 
-    dense = first[None, :, seqs : seqs + 3 * SLOT]
-    for axis, flip in (("zh", 2), ("yh", 2), ("zh", 1), ("yh", 1)):
-        other = swapped(dense, axis, flip)
-        dense = jnp.concatenate([dense, other], axis=0)
+    dense = to_all(first[:, seqs : seqs + 3 * slim].reshape(tp * 3 * slim, quarter), far)
+    dense = exchange(dense, FAR)
+    dense = jnp.transpose(dense.reshape(far, tp, 3, slim, quarter), (2, 0, 3, 1, 4))
+    dense = dense.reshape(3, far * slim, tp * quarter)
 
     normed_mix = rms_norm(full_tokens, gain_mix)
 
@@ -149,15 +143,11 @@
     partial = dot(hidden, expert_down[0]).astype(bf16).reshape(experts, 4, -1)
     returned = exchange(partial, EP)
 
-    def matrix(place):
-        part = dense[:, :, place * SLOT : (place + 1) * SLOT]
-        return jnp.moveaxis(part, 1, 2).reshape(far * SLOT, tp * quarter)
-
     transposed = (((1,), (1,)), ((), ()))
-    gate_cols = lax.dot_general(group, matrix(0), transposed, preferred_element_type=f32)
-    up_cols = lax.dot_general(group, matrix(1), transposed, preferred_element_type=f32)
+    gate_cols = lax.dot_general(group, dense[0], transposed, preferred_element_type=f32)
+    up_cols = lax.dot_general(group, dense[1], transposed, preferred_element_type=f32)
     dense_hidden = (jax.nn.silu(gate_cols) * up_cols).astype(bf16)
-    dense_part = dot(dense_hidden, matrix(2)).reshape(near, seqs, -1)
+    dense_part = dot(dense_hidden, dense[2]).reshape(near, seqs, -1)
 
     picked = dot(picks, returned.reshape(experts, -1)).reshape(seqs, TOP, -1)
     route_weight = jax.nn.sigmoid(route_logits - route_logits[:, ::-1])

time: 152 us -> 148 us (0.974)
  waiting for transfers between devices: 51.8 us -> 65.2 us
  starting transfers between devices: 71.3 us -> 58 us
  local copies, waits for them, and re-layouts: 14.5 us -> 12.3 us
  other arithmetic: 4.89 us -> 3.32 us
    ppermute x4 -> x0, starting transfers between devices: 23.9 us -> none  [swapped(): lax.ppermute(array, axis, [(i, i ^ flip) for i in range(lax.axis_size(axi...]
    all_to_all x5 -> x6, waiting for transfers between devices: 35.6 us -> 56.8 us  [exchange(): return lax.all_to_all(blocks, axis, 0, 0, tiled=True)]
    ppermute x4 -> x0, waiting for transfers between devices: 16.3 us -> none  [swapped(): lax.ppermute(array, axis, [(i, i ^ flip) for i in range(lax.axis_size(axi...]
    all_to_all x5 -> x6, starting transfers between devices: 37.1 us -> 48 us  [exchange(): return lax.all_to_all(blocks, axis, 0, 0, tiled=True)]
    ppermute x3, waiting for transfers between devices: 0.01 us -> 8.38 us  [shifted(): lax.ppermute(array, axis, [(i, (i + step) % size) for i in range(size)])]
    unnamed x49 -> x39, local copies, waits for them, and re-layouts: 8.31 us -> 5.41 us
  transfers between devices with their start and end apart: 12 -> 9, of which waited for: 8 -> 7; matrix products, arithmetic and copies ran while one was open for 8% -> 3% of each run, Pallas kernels for 0% -> 0%
where the time goes in v3:
time: 148 us; the launch traced here: 147 us
  waiting for transfers between devices  65.2 us (44%)
  starting transfers between devices  58 us (39%)
  local copies, waits for them, and re-layouts  12.3 us (8%)
  matrix products  7.66 us (5%)
  other arithmetic  3.32 us (2%)
    all_to_all x6, waiting for transfers between devices, exchange(): return lax.all_to_all(blocks, axis, 0, 0, tiled=True)  56.8 us
    all_to_all x6, starting transfers between devices, exchange(): return lax.all_to_all(blocks, axis, 0, 0, tiled=True)  48 us
    ppermute x3, starting transfers between devices, shifted(): lax.ppermute(array, axis, [(i, (i + step) % size) for i in range(size)])  10.1 us
    ppermute x3, waiting for transfers between devices, shifted(): lax.ppermute(array, axis, [(i, (i + step) % size) for i in range(size)])  8.38 us
    dot_general x14, matrix products, dot(): return jnp.dot(a, b, preferred_element_type=f32)  5.99 us
    unnamed x39, local copies, waits for them, and re-layouts  5.41 us
  transfers between devices with their start and end apart: 9, of which 7 were waited for; matrix products, arithmetic and copies ran while one was open for 3% of the time, Pallas kernels for 0%

profile of v3, /device:TPU:1, one launch (start us, length us, event | category | flops | bytes accessed | tf_op | source)
XLA Modules:
  0.0 147.0 jit_solution(16643270063763560786)
XLA Ops:
  0.0 0.7 broadcast_in_dim.26
  0.8 0.7 stack.27
  1.5 0.7 copy-done.9
  2.3 0.7 copy-done.6
  3.1 0.6 copy.52
  3.7 5.0 %all-to-all-start = ((bf16[4,40,256]{2,1,0:T(8,128)(2,1)}), bf16[4,40,256]{2,1,0:T(8,128)(2,1)S(1)}, u32[]{:S(2)}, u32[]{:S(2)}) async-start(bf16[4,40,256]{2,1,0:T(8,128)(2,1)} %copy.52), calls=%async_computation | async-start | bytes 163840 | tf_op jit(solution)/shard_map/all_to_all | solution.py:20
  8.7 4.6 %all-to-all-done = bf16[4,40,256]{2,1,0:T(8,128)(2,1)S(1)} async-done(((bf16[4,40,256]{2,1,0:T(8,128)(2,1)}), bf16[4,40,256]{2,1,0:T(8,128)(2,1)S(1)}, u32[]{:S(2)}, u32[]{:S(2)}) %all-to-all-start) | async-done | bytes 81952 | tf_op jit(solution)/shard_map/all_to_all | solution.py:20
  13.2 0.1 fusion.43
  13.4 0.1 fusion.46
  13.5 0.1 multiply_convert_fusion
  13.6 0.2 fusion.15
  13.8 0.7 copy-done.2
  14.4 0.3 fusion.52
  14.7 0.3 fusion.17
  15.0 1.0 fusion.19
  16.0 0.7 copy-done.17
  16.6 0.1 bitcast_add_fusion
  16.8 0.5 copy-done.16
  17.3 0.1 maximum_bitcast_fusion.1
  17.5 0.2 fusion.16
  17.6 0.8 broadcast_in_dim.28
  18.4 10.1 %all-to-all-start.1 = ((bf16[32,16,384]{2,1,0:T(8,128)(2,1)}), bf16[32,16,384]{2,1,0:T(8,128)(2,1)S(1)}, u32[]{:S(2)}, u32[]{:S(2)}) async-start(bf16[32,16,384]{2,1,0:T(8,128)(2,1)} %broadcast_in_dim.28), calls=%async_computation.1 | async-start | bytes 786432 | tf_op jit(solution)/shard_map/all_to_all | solution.py:20
  28.6 3.3 %collective-permute-start = (bf16[512,256]{1,0:T(8,128)(2,1)S(1)}, bf16[512,256]{1,0:T(8,128)(2,1)S(1)}, u32[]{:S(2)}, u32[]{:S(2)}) collective-permute-start(bf16[512,256]{1,0:T(8,128)(2,1)S(1)} %copy-done.4), channel_id=1, source_target_pairs={{0,1},{1,2},{2,3},{3,0},{4,5},{5,6},{6,7},{7,4},{8,9},{9,10},{10,1... | collective-permute-start | bytes 786440 | tf_op jit(solution)/shard_map/ppermute | solution.py:44
  31.8 3.2 %collective-permute-start.2 = (bf16[512,256]{1,0:T(8,128)(2,1)S(1)}, bf16[512,256]{1,0:T(8,128)(2,1)S(1)}, u32[]{:S(2)}, u32[]{:S(2)}) collective-permute-start(bf16[512,256]{1,0:T(8,128)(2,1)S(1)} %copy-done.4), channel_id=1, source_target_pairs={{0,3},{1,0},{2,1},{3,2},{4,7},{5,4},{6,5},{7,6},{8,11},{9,8},{10,9... | collective-permute-start | bytes 786440 | tf_op jit(solution)/shard_map/ppermute | solution.py:44
  35.1 3.6 %collective-permute-start.1 = (bf16[512,256]{1,0:T(8,128)(2,1)S(1)}, bf16[512,256]{1,0:T(8,128)(2,1)S(1)}, u32[]{:S(2)}, u32[]{:S(2)}) collective-permute-start(bf16[512,256]{1,0:T(8,128)(2,1)S(1)} %copy-done.4), channel_id=1, source_target_pairs={{0,2},{1,3},{2,0},{3,1},{4,6},{5,7},{6,4},{7,5},{8,10},{9,11},{10,... | collective-permute-start | bytes 786440 | tf_op jit(solution)/shard_map/ppermute | solution.py:44
  38.8 0.7 copy-done.13
  39.5 3.7 %collective-permute-done = bf16[512,256]{1,0:T(8,128)(2,1)S(1)} collective-permute-done((bf16[512,256]{1,0:T(8,128)(2,1)S(1)}, bf16[512,256]{1,0:T(8,128)(2,1)S(1)}, u32[]{:S(2)}, u32[]{:S(2)}) %collective-permute-start) | collective-permute-done | bytes 262176 | tf_op jit(solution)/shard_map/ppermute | solution.py:44
  43.2 4.7 %collective-permute-done.1 = bf16[512,256]{1,0:T(8,128)(2,1)S(1)} collective-permute-done((bf16[512,256]{1,0:T(8,128)(2,1)S(1)}, bf16[512,256]{1,0:T(8,128)(2,1)S(1)}, u32[]{:S(2)}, u32[]{:S(2)}) %collective-permute-start.1) | collective-permute-done | bytes 262176 | tf_op jit(solution)/shard_map/ppermute | solution.py:44
  47.9 0.7 copy-done.5
  48.6 1.1 pad_maximum_fusion
  49.7 0.9 broadcast_in_dim.30
  50.6 11.1 %all-to-all-start.2 = ((bf16[16,72,256]{2,1,0:T(8,128)(2,1)}), bf16[16,72,256]{2,1,0:T(8,128)(2,1)S(1)}, u32[]{:S(2)}, u32[]{:S(2)}) async-start(bf16[16,72,256]{2,1,0:T(8,128)(2,1)} %broadcast_in_dim.30), calls=%async_computation.2 | async-start | bytes 1179648 | tf_op jit(solution)/shard_map/all_to_all | solution.py:20
  61.8 0.2 fusion.5
  62.0 0.2 fusion.6
  62.2 0.2 fusion.7
  62.4 0.2 fusion.4
  62.6 0.1 fusion.26
  62.8 0.7 copy-done.11
  63.4 0.2 multiply_reduce_fusion
  63.7 0.2 convolution_convert_fusion
  63.9 0.9 reshape.216
  64.8 14.9 %all-to-all-done.2 = bf16[16,72,256]{2,1,0:T(8,128)(2,1)S(1)} async-done(((bf16[16,72,256]{2,1,0:T(8,128)(2,1)}), bf16[16,72,256]{2,1,0:T(8,128)(2,1)S(1)}, u32[]{:S(2)}, u32[]{:S(2)}) %all-to-all-start.2) | async-done | bytes 589856 | tf_op jit(solution)/shard_map/all_to_all | solution.py:20
  79.7 12.3 %all-to-all-start.3 = ((bf16[128,4,256]{2,1,0:T(4,128)(2,1)}), bf16[128,4,256]{2,1,0:T(4,128)(2,1)S(1)}, u32[]{:S(2)}, u32[]{:S(2)}) async-start(bf16[128,4,256]{2,1,0:T(4,128)(2,1)} %reshape.216), calls=%async_computation.3 | async-start | bytes 524288 | tf_op jit(solution)/shard_map/all_to_all | solution.py:20
  92.1 0.1 copy.56
  92.3 15.0 %all-to-all-done.3 = bf16[128,4,256]{2,1,0:T(4,128)(2,1)S(1)} async-done(((bf16[128,4,256]{2,1,0:T(4,128)(2,1)}), bf16[128,4,256]{2,1,0:T(4,128)(2,1)S(1)}, u32[]{:S(2)}, u32[]{:S(2)}) %all-to-all-start.3) | async-done | bytes 262176 | tf_op jit(solution)/shard_map/all_to_all | solution.py:20
  107.3 1.5 fusion.24
  108.7 2.2 %convolution_convert_fusion.1 = bf16[128,1024]{1,0:T(8,128)(2,1)S(1)} fusion(bf16[128,1024]{1,0:T(8,128)(2,1)S(1)} %bitcast.136, bf16[1,352,1024]{2,1,0:T(8,128)(2,1)} %param.39, bf16[1,1024,352]{1,2,0:T(8,128)(2,1)} %param.38, f32[128,352]{0,1:T(8,128)S(1)} %fusion.24), kind=kOutput, calls=%fused_computation.4 | convolution fusion | flops 184950784 | bytes 2146304 | tf_op jit(solution)/shard_map/dot_general | solution.py:39
  110.9 0.9 reshape.218
  111.8 5.5 %all-to-all-start.4 = ((bf16[128,4,256]{2,1,0:T(4,128)(2,1)}), bf16[128,4,256]{2,1,0:T(4,128)(2,1)S(1)}, u32[]{:S(2)}, u32[]{:S(2)}) async-start(bf16[128,4,256]{2,1,0:T(4,128)(2,1)} %reshape.218), calls=%async_computation.4 | async-start | bytes 524288 | tf_op jit(solution)/shard_map/all_to_all | solution.py:20
  117.4 0.2 copy.60
  117.6 0.1 reshape.233
  117.7 0.2 copy.58
  117.9 0.2 copy.57
  118.1 0.2 fusion.73
  118.3 0.2 fusion.8
  118.6 0.1 copy.59
  118.7 14.0 %all-to-all-done.4 = bf16[128,4,256]{2,1,0:T(4,128)(2,1)S(1)} async-done(((bf16[128,4,256]{2,1,0:T(4,128)(2,1)}), bf16[128,4,256]{2,1,0:T(4,128)(2,1)S(1)}, u32[]{:S(2)}, u32[]{:S(2)}) %all-to-all-start.4) | async-done | bytes 262176 | tf_op jit(solution)/shard_map/all_to_all | solution.py:20
  132.7 0.2 reshape.234
  132.9 0.2 fusion.3
  133.1 0.2 fusion.1
  133.4 0.7 pad_maximum_fusion.2
  134.1 3.9 %all-to-all-start.5 = ((bf16[32,16,256]{2,1,0:T(8,128)(2,1)}), bf16[32,16,256]{2,1,0:T(8,128)(2,1)S(1)}, u32[]{:S(2)}, u32[]{:S(2)}) async-start(bf16[32,16,256]{2,1,0:T(8,128)(2,1)} %bitcast.48), calls=%async_computation.5 | async-start | bytes 524288 | tf_op jit(solution)/shard_map/all_to_all | solution.py:20
  138.0 8.3 %all-to-all-done.5 = bf16[32,16,256]{2,1,0:T(8,128)(2,1)S(1)} async-done(((bf16[32,16,256]{2,1,0:T(8,128)(2,1)}), bf16[32,16,256]{2,1,0:T(8,128)(2,1)S(1)}, u32[]{:S(2)}, u32[]{:S(2)}) %all-to-all-start.5) | async-done | bytes 262176 | tf_op jit(solution)/shard_map/all_to_all | solution.py:20
  146.4 0.6 add_convert_fusion
  (62 shorter events, 0.7 us)
Async XLA Ops:
  0.0 15.0 %copy-start = (f32[16,1,128,128]{3,2,1,0:T(8,128)S(1)}, f32[16,1,128,128]{3,2,1,0:T(8,128)}, u32[]{:S(2)}) copy-start(f32[16,1,128,128]{3,2,1,0:T(8,128)} %param.31) | copy-start | bytes 3145732
  0.8 0.7 copy-start.8
  1.5 0.7 copy-start.9
  2.3 0.7 copy-start.6
  3.7 5.0 %copy-start.7 = (f32[1024]{0:T(1024)S(1)}, f32[1024]{0:T(1024)}, u32[]{:S(2)}) copy-start(f32[1024]{0:T(1024)} %param.23) | copy-start | bytes 12292
  3.7 9.5 %all-to-all-start = ((bf16[4,40,256]{2,1,0:T(8,128)(2,1)}), bf16[4,40,256]{2,1,0:T(8,128)(2,1)S(1)}, u32[]{:S(2)}, u32[]{:S(2)}) async-start(bf16[4,40,256]{2,1,0:T(8,128)(2,1)} %copy.52), calls=%async_computation | async-start | bytes 163840 | tf_op jit(solution)/shard_map/all_to_all | solution.py:20
  8.7 4.9 %copy-start.1 = (bf16[1024,128]{1,0:T(8,128)(2,1)S(1)}, bf16[1024,128]{1,0:T(8,128)(2,1)}, u32[]{:S(2)}) copy-start(bf16[1024,128]{1,0:T(8,128)(2,1)} %param.27) | copy-start | bytes 786436
  13.5 1.0 copy-start.2
  13.6 0.8 copy-start.10
  13.6 1.1 copy-start.3
  15.0 1.0 copy-start.15
  15.0 2.5 %copy-start.14 = (bf16[1024,128]{1,0:T(8,128)(2,1)S(1)}, bf16[1024,128]{1,0:T(8,128)(2,1)}, u32[]{:S(2)}) copy-start(bf16[1024,128]{1,0:T(8,128)(2,1)} %param.26) | copy-start | bytes 786436
  16.0 0.7 copy-start.17
  16.6 0.7 copy-start.16
  18.4 10.1 %copy-start.4 = (bf16[512,256]{1,0:T(8,128)(2,1)S(1)}, bf16[512,256]{1,0:T(8,128)(2,1)}, u32[]{:S(2)}) copy-start(bf16[512,256]{1,0:T(8,128)(2,1)} %param.30) | copy-start | bytes 786436
  18.4 20.2 %copy-start.12 = (s32[16,2]{0,1:T(2,128)S(1)}, s32[16,2]{0,1:T(2,128)}, u32[]{:S(2)}) copy-start(s32[16,2]{0,1:T(2,128)} %param.35) | copy-start | bytes 388
  18.4 31.3 %all-to-all-start.1 = ((bf16[32,16,384]{2,1,0:T(8,128)(2,1)}), bf16[32,16,384]{2,1,0:T(8,128)(2,1)S(1)}, u32[]{:S(2)}, u32[]{:S(2)}) async-start(bf16[32,16,384]{2,1,0:T(8,128)(2,1)} %broadcast_in_dim.28), calls=%async_computation.1 | async-start | bytes 786432 | tf_op jit(solution)/shard_map/all_to_all | solution.py:20
  28.6 14.7 %collective-permute-start = (bf16[512,256]{1,0:T(8,128)(2,1)S(1)}, bf16[512,256]{1,0:T(8,128)(2,1)S(1)}, u32[]{:S(2)}, u32[]{:S(2)}) collective-permute-start(bf16[512,256]{1,0:T(8,128)(2,1)S(1)} %copy-done.4), channel_id=1, source_target_pairs={{0,1},{1,2},{2,3},{3,0},{4,5},{5,6},{6,7},{7,4},{8,9},{9,10},{10,1... | collective-permute-start | bytes 786440 | tf_op jit(solution)/shard_map/ppermute | solution.py:44
  31.8 11.4 %collective-permute-start.2 = (bf16[512,256]{1,0:T(8,128)(2,1)S(1)}, bf16[512,256]{1,0:T(8,128)(2,1)S(1)}, u32[]{:S(2)}, u32[]{:S(2)}) collective-permute-start(bf16[512,256]{1,0:T(8,128)(2,1)S(1)} %copy-done.4), channel_id=1, source_target_pairs={{0,3},{1,0},{2,1},{3,2},{4,7},{5,4},{6,5},{7,6},{8,11},{9,8},{10,9... | collective-permute-start | bytes 786440 | tf_op jit(solution)/shard_map/ppermute | solution.py:44
  35.1 12.8 %collective-permute-start.1 = (bf16[512,256]{1,0:T(8,128)(2,1)S(1)}, bf16[512,256]{1,0:T(8,128)(2,1)S(1)}, u32[]{:S(2)}, u32[]{:S(2)}) collective-permute-start(bf16[512,256]{1,0:T(8,128)(2,1)S(1)} %copy-done.4), channel_id=1, source_target_pairs={{0,2},{1,3},{2,0},{3,1},{4,6},{5,7},{6,4},{7,5},{8,10},{9,11},{10,... | collective-permute-start | bytes 786440 | tf_op jit(solution)/shard_map/ppermute | solution.py:44
  38.7 0.7 copy-start.13
  47.9 0.7 copy-start.5
  50.6 29.1 %all-to-all-start.2 = ((bf16[16,72,256]{2,1,0:T(8,128)(2,1)}), bf16[16,72,256]{2,1,0:T(8,128)(2,1)S(1)}, u32[]{:S(2)}, u32[]{:S(2)}) async-start(bf16[16,72,256]{2,1,0:T(8,128)(2,1)} %broadcast_in_dim.30), calls=%async_computation.2 | async-start | bytes 1179648 | tf_op jit(solution)/shard_map/all_to_all | solution.py:20
  62.7 0.7 copy-start.11
  79.7 27.5 %all-to-all-start.3 = ((bf16[128,4,256]{2,1,0:T(4,128)(2,1)}), bf16[128,4,256]{2,1,0:T(4,128)(2,1)S(1)}, u32[]{:S(2)}, u32[]{:S(2)}) async-start(bf16[128,4,256]{2,1,0:T(4,128)(2,1)} %reshape.216), calls=%async_computation.3 | async-start | bytes 524288 | tf_op jit(solution)/shard_map/all_to_all | solution.py:20
  111.8 20.9 %all-to-all-start.4 = ((bf16[128,4,256]{2,1,0:T(4,128)(2,1)}), bf16[128,4,256]{2,1,0:T(4,128)(2,1)S(1)}, u32[]{:S(2)}, u32[]{:S(2)}) async-start(bf16[128,4,256]{2,1,0:T(4,128)(2,1)} %reshape.218), calls=%async_computation.4 | async-start | bytes 524288 | tf_op jit(solution)/shard_map/all_to_all | solution.py:20
  134.1 12.3 %all-to-all-start.5 = ((bf16[32,16,256]{2,1,0:T(8,128)(2,1)}), bf16[32,16,256]{2,1,0:T(8,128)(2,1)S(1)}, u32[]{:S(2)}, u32[]{:S(2)}) async-start(bf16[32,16,256]{2,1,0:T(8,128)(2,1)} %bitcast.48), calls=%async_computation.5 | async-start | bytes 524288 | tf_op jit(solution)/shard_map/all_to_all | solution.py:20

commit v4 on v3

--- a/solution.py
+++ b/solution.py
@@ -85,10 +85,9 @@
     full_tokens = side_by_side(first[:, :seqs])
     mix_row = first[:, seqs + 3 * slim].reshape(1, -1)
 
-    mix_out = [w_mix_out]
+    mix_out = {0: w_mix_out}
     for step in (2, 1, 3):
-        mix_out.append(shifted(w_mix_out, "x", step))
-    mix_out = jnp.stack([mix_out[0], mix_out[2], mix_out[1], mix_out[3]])
+        mix_out[step] = shifted(w_mix_out, "x", step)
 
     dense = to_all(first[:, seqs : seqs + 3 * slim].reshape(tp * 3 * slim, quarter), far)
     dense = exchange(dense, FAR)
@@ -115,21 +114,14 @@
     cell_out = numerator / jnp.maximum(jnp.abs(denominator), 1.0)[..., None]
     mixed = (jax.nn.sigmoid(out_gate) * cell_out.reshape(seqs, -1)).astype(bf16)
 
-    sent = to_all(jnp.concatenate([mixed, tokens], axis=1), near * tp)
-    second = exchange(sent, NEAR + ("x",))
-    second = second.reshape(near, tp, seqs, HEAD + quarter)
-    all_heads = jnp.concatenate(
-        [second[:, k, :, :HEAD].reshape(near * seqs, HEAD) for k in range(tp)], axis=1
-    )
-    resid = []
-    for k in range(tp):
-        added = dot(all_heads, lax.dynamic_index_in_dim(mix_out, (me - k) % tp, 0, False))
-        old = second[:, k, :, HEAD:].reshape(near * seqs, quarter)
-        resid.append((old.astype(f32) + added).astype(bf16))
-    resid = jnp.concatenate(resid, axis=1)
-    group = rms_norm(resid, gain_ffn)
-    normed = lax.dynamic_slice_in_dim(group, place * seqs, seqs, 0)
-    own_resid = lax.dynamic_slice(resid, (place * seqs, me * quarter), (seqs, quarter))
+    sent = to_all(mixed, tp)
+    second = exchange(sent, "x")
+    all_heads = side_by_side(second)
+    added = jnp.stack([dot(all_heads, mix_out[k]) for k in range(tp)])
+    added = [lax.dynamic_index_in_dim(added, (me - k) & (tp - 1), 0, False) for k in range(tp)]
+    resid = (full_tokens.astype(f32) + jnp.concatenate(added, axis=1)).astype(bf16)
+    normed = rms_norm(resid, gain_ffn)
+    own_resid = lax.dynamic_slice_in_dim(resid, me * quarter, quarter, 1)
 
     flat_ids = route_ids.reshape(-1)
     picks = (flat_ids[:, None] == jnp.arange(experts, dtype=jnp.int32)[None, :]).astype(bf16)
@@ -137,6 +129,14 @@
     outgoing = lax.dot_general(chosen, normed, (((0,), (0,)), ((), ())), preferred_element_type=f32)
     outgoing = outgoing.astype(bf16).reshape(experts, 4, -1)
     received = exchange(outgoing, EP)
+
+    group = normed
+    for axis in ("c", "yl", "zl"):
+        other = lax.ppermute(group, axis, [(0, 1), (1, 0)])
+        low = lax.axis_index(axis) == 0
+        group = jnp.concatenate(
+            [jnp.where(low, group, other), jnp.where(low, other, group)], axis=0
+        )
 
     rows = received.reshape(experts, -1)
     hidden = (jax.nn.silu(dot(rows, expert_gate[0])) * dot(rows, expert_up[0])).astype(bf16)

time: 148 us -> 143 us (0.966)
  waiting for transfers between devices: 65.2 us -> 59.4 us
  starting transfers between devices: 58 us -> 62.2 us
    ppermute x0 -> x3, starting transfers between devices: none -> 15.5 us  [layer(): other = lax.ppermute(group, axis, [(0, 1), (1, 0)])]
    all_to_all x6, starting transfers between devices: 48 us -> 36.5 us  [exchange(): return lax.all_to_all(blocks, axis, 0, 0, tiled=True)]
    ppermute x3, waiting for transfers between devices: 8.38 us -> 0.01 us  [shifted(): lax.ppermute(array, axis, [(i, (i + step) % size) for i in range(size)])]
    all_to_all x6, waiting for transfers between devices: 56.8 us -> 58.6 us  [exchange(): return lax.all_to_all(blocks, axis, 0, 0, tiled=True)]
  transfers between devices with their start and end apart: 9 -> 12, of which waited for: 7 -> 7; matrix products, arithmetic and copies ran while one was open for 3% -> 9% of each run, Pallas kernels for 0% -> 0%
where the time goes in v4:
time: 143 us; the launch traced here: 142 us
  starting transfers between devices  62.2 us (43%)
  waiting for transfers between devices  59.4 us (42%)
  local copies, waits for them, and re-layouts  11.3 us (8%)
  matrix products  6.36 us (4%)
  other arithmetic  2.32 us (2%)
    all_to_all x6, waiting for transfers between devices, exchange(): return lax.all_to_all(blocks, axis, 0, 0, tiled=True)  58.6 us
    all_to_all x6, starting transfers between devices, exchange(): return lax.all_to_all(blocks, axis, 0, 0, tiled=True)  36.5 us
    ppermute x3, starting transfers between devices, layer(): other = lax.ppermute(group, axis, [(0, 1), (1, 0)])  15.5 us
    ppermute x3, starting transfers between devices, shifted(): lax.ppermute(array, axis, [(i, (i + step) % size) for i in range(size)])  10.3 us
    unnamed x39, local copies, waits for them, and re-layouts  4.75 us
    dot_general x14, matrix products, dot(): return jnp.dot(a, b, preferred_element_type=f32)  4.68 us
  transfers between devices with their start and end apart: 12, of which 7 were waited for; matrix products, arithmetic and copies ran while one was open for 9% of the time, Pallas kernels for 0%

profile of v4, /device:TPU:1, one launch (start us, length us, event | category | flops | bytes accessed | tf_op | source)
XLA Modules:
  0.0 142.2 jit_solution(10647944443974358315)
XLA Ops:
  0.0 5.3 %collective-permute-start.2 = (bf16[512,256]{1,0:T(8,128)(2,1)}, bf16[512,256]{1,0:T(8,128)(2,1)S(1)}, u32[]{:S(2)}, u32[]{:S(2)}) collective-permute-start(bf16[512,256]{1,0:T(8,128)(2,1)} %param.30), channel_id=1, source_target_pairs={{0,3},{1,0},{2,1},{3,2},{4,7},{5,4},{6,5},{7,6},{8,11},{9,8},{10,9... | collective-permute-start | bytes 786440 | tf_op jit(solution)/shard_map/ppermute | solution.py:44
  5.3 2.4 %collective-permute-start.1 = (bf16[512,256]{1,0:T(8,128)(2,1)}, bf16[512,256]{1,0:T(8,128)(2,1)S(1)}, u32[]{:S(2)}, u32[]{:S(2)}) collective-permute-start(bf16[512,256]{1,0:T(8,128)(2,1)} %param.30), channel_id=1, source_target_pairs={{0,2},{1,3},{2,0},{3,1},{4,6},{5,7},{6,4},{7,5},{8,10},{9,11},{10,... | collective-permute-start | bytes 786440 | tf_op jit(solution)/shard_map/ppermute | solution.py:44
  7.8 2.5 %collective-permute-start = (bf16[512,256]{1,0:T(8,128)(2,1)}, bf16[512,256]{1,0:T(8,128)(2,1)S(1)}, u32[]{:S(2)}, u32[]{:S(2)}) collective-permute-start(bf16[512,256]{1,0:T(8,128)(2,1)} %param.30), channel_id=1, source_target_pairs={{0,1},{1,2},{2,3},{3,0},{4,5},{5,6},{6,7},{7,4},{8,9},{9,10},{10,1... | collective-permute-start | bytes 786440 | tf_op jit(solution)/shard_map/ppermute | solution.py:44
  10.3 0.7 broadcast_in_dim.26
  11.0 0.7 stack.29
  11.7 0.7 copy-done.8
  12.5 0.7 copy-done.9
  13.3 0.7 copy.66
  13.9 3.5 %all-to-all-start = ((bf16[4,40,256]{2,1,0:T(8,128)(2,1)}), bf16[4,40,256]{2,1,0:T(8,128)(2,1)S(1)}, u32[]{:S(2)}, u32[]{:S(2)}) async-start(bf16[4,40,256]{2,1,0:T(8,128)(2,1)} %copy.66), calls=%async_computation | async-start | bytes 163840 | tf_op jit(solution)/shard_map/all_to_all | solution.py:20
  17.5 4.9 %all-to-all-done = bf16[4,40,256]{2,1,0:T(8,128)(2,1)S(1)} async-done(((bf16[4,40,256]{2,1,0:T(8,128)(2,1)}), bf16[4,40,256]{2,1,0:T(8,128)(2,1)S(1)}, u32[]{:S(2)}, u32[]{:S(2)}) %all-to-all-start) | async-done | bytes 81952 | tf_op jit(solution)/shard_map/all_to_all | solution.py:20
  22.4 0.1 fusion.33
  22.8 0.2 fusion.10
  22.9 0.6 copy-done.3
  23.5 0.3 fusion.50
  23.8 0.3 fusion.12
  24.1 1.0 fusion.14
  25.1 0.7 copy-done.17
  25.7 0.1 bitcast_add_fusion
  25.8 0.5 copy-done.16
  26.4 0.1 maximum_bitcast_fusion.1
  26.5 0.2 fusion.11
  26.7 0.6 broadcast_in_dim.28
  27.3 3.4 %all-to-all-start.1 = ((bf16[4,16,128]{2,1,0:T(8,128)(2,1)}), bf16[4,16,128]{2,1,0:T(8,128)(2,1)S(1)}, u32[]{:S(2)}, u32[]{:S(2)}) async-start(bf16[4,16,128]{2,1,0:T(8,128)(2,1)} %broadcast_in_dim.28), calls=%async_computation.1 | async-start | bytes 32768 | tf_op jit(solution)/shard_map/all_to_all | solution.py:20
  30.8 4.1 %all-to-all-done.1 = bf16[4,16,128]{2,1,0:T(8,128)(2,1)S(1)} async-done(((bf16[4,16,128]{2,1,0:T(8,128)(2,1)}), bf16[4,16,128]{2,1,0:T(8,128)(2,1)S(1)}, u32[]{:S(2)}, u32[]{:S(2)}) %all-to-all-start.1) | async-done | bytes 16416 | tf_op jit(solution)/shard_map/all_to_all | solution.py:20
  34.9 0.1 convolution_bitcast_fusion.3
  35.0 0.2 convolution_bitcast_fusion
  35.2 0.2 convolution_bitcast_fusion.1
  35.3 0.2 convolution_bitcast_fusion.2
  35.5 0.1 multiply_reduce_fusion.1
  35.7 0.7 copy-done.12
  36.4 10.3 %collective-permute-start.3 = (bf16[16,1024]{1,0:T(8,128)(2,1)S(1)}, bf16[16,1024]{1,0:T(8,128)(2,1)S(1)}, u32[]{:S(2)}, u32[]{:S(2)}) collective-permute-start(bf16[16,1024]{1,0:T(8,128)(2,1)S(1)} %get-tuple-element.5), channel_id=1, source_target_pairs={{0,4},{4,0},{1,5},{5,1},{2,6},{6,2},{3,7},{7,3},{8,12},{12,8},{9,1... | collective-permute-start | bytes 98312 | tf_op jit(solution)/shard_map/ppermute | solution.py:135
  46.8 0.8 collective-permute-done.3
  47.6 1.9 %collective-permute-start.4 = (bf16[32,1024]{1,0:T(8,128)(2,1)S(1)}, bf16[32,1024]{1,0:T(8,128)(2,1)S(1)}, u32[]{:S(2)}, u32[]{:S(2)}) collective-permute-start(bf16[32,1024]{1,0:T(8,128)(2,1)S(1)} %pad_maximum_fusion.7), channel_id=1, source_target_pairs={{0,8},{8,0},{1,9},{9,1},{2,10},{10,2},{3,11},{11,3},{4,12},{12,4},... | collective-permute-start | bytes 196616 | tf_op jit(solution)/shard_map/ppermute | solution.py:135
  49.5 0.2 convolution_convert_fusion
  49.8 0.9 reshape.216
  50.6 13.2 %all-to-all-start.3 = ((bf16[128,4,256]{2,1,0:T(4,128)(2,1)}), bf16[128,4,256]{2,1,0:T(4,128)(2,1)S(1)}, u32[]{:S(2)}, u32[]{:S(2)}) async-start(bf16[128,4,256]{2,1,0:T(4,128)(2,1)} %reshape.216), calls=%async_computation.3 | async-start | bytes 524288 | tf_op jit(solution)/shard_map/all_to_all | solution.py:20
  63.9 3.3 %collective-permute-start.5 = (bf16[64,1024]{1,0:T(8,128)(2,1)S(1)}, bf16[64,1024]{1,0:T(8,128)(2,1)S(1)}, u32[]{:S(2)}, u32[]{:S(2)}) collective-permute-start(bf16[64,1024]{1,0:T(8,128)(2,1)S(1)} %pad_maximum_fusion.2), channel_id=1, source_target_pairs={{0,64},{64,0},{1,65},{65,1},{2,66},{66,2},{3,67},{67,3},{4,68},{68... | collective-permute-start | bytes 393224 | tf_op jit(solution)/shard_map/ppermute | solution.py:135
  67.2 11.9 %all-to-all-done.3 = bf16[128,4,256]{2,1,0:T(4,128)(2,1)S(1)} async-done(((bf16[128,4,256]{2,1,0:T(4,128)(2,1)}), bf16[128,4,256]{2,1,0:T(4,128)(2,1)S(1)}, u32[]{:S(2)}, u32[]{:S(2)}) %all-to-all-start.3) | async-done | bytes 262176 | tf_op jit(solution)/shard_map/all_to_all | solution.py:20
  79.1 0.9 broadcast_in_dim.30
  80.0 3.6 %all-to-all-start.2 = ((bf16[16,72,256]{2,1,0:T(8,128)(2,1)}), bf16[16,72,256]{2,1,0:T(8,128)(2,1)S(1)}, u32[]{:S(2)}, u32[]{:S(2)}) async-start(bf16[16,72,256]{2,1,0:T(8,128)(2,1)} %broadcast_in_dim.30), calls=%async_computation.2 | async-start | bytes 1179648 | tf_op jit(solution)/shard_map/all_to_all | solution.py:20
  83.6 0.1 multiply_reduce_fusion
  83.8 0.1 div.50
  83.9 0.8 copy-done.1
  84.7 0.3 fusion.19
  85.0 2.2 %convolution_convert_fusion.1 = bf16[128,1024]{1,0:T(8,128)(2,1)S(1)} fusion(bf16[128,1024]{1,0:T(8,128)(2,1)S(1)} %bitcast.175, bf16[1,352,1024]{2,1,0:T(8,128)(2,1)} %param.39, bf16[1,1024,352]{1,2,0:T(8,128)(2,1)} %param.38, f32[128,352]{0,1:T(8,128)S(1)} %fusion.19), kind=kOutput, calls=%fused_computation.4 | convolution fusion | flops 184950784 | bytes 2146304 | tf_op jit(solution)/shard_map/dot_general | solution.py:39
  87.2 0.9 reshape.218
  88.1 15.6 %all-to-all-done.2 = bf16[16,72,256]{2,1,0:T(8,128)(2,1)S(1)} async-done(((bf16[16,72,256]{2,1,0:T(8,128)(2,1)}), bf16[16,72,256]{2,1,0:T(8,128)(2,1)S(1)}, u32[]{:S(2)}, u32[]{:S(2)}) %all-to-all-start.2) | async-done | bytes 589856 | tf_op jit(solution)/shard_map/all_to_all | solution.py:20
  103.7 9.0 %all-to-all-start.4 = ((bf16[128,4,256]{2,1,0:T(4,128)(2,1)}), bf16[128,4,256]{2,1,0:T(4,128)(2,1)S(1)}, u32[]{:S(2)}, u32[]{:S(2)}) async-start(bf16[128,4,256]{2,1,0:T(4,128)(2,1)} %reshape.218), calls=%async_computation.4 | async-start | bytes 524288 | tf_op jit(solution)/shard_map/all_to_all | solution.py:20
  112.7 0.1 copy.71
  112.8 0.2 copy.72
  113.0 0.2 copy.73
  113.2 0.2 fusion.31
  113.4 0.2 multiply_convert_fusion.2
  113.7 0.1 copy.74
  113.8 0.2 copy.75
  114.0 0.1 reshape.229
  114.1 13.8 %all-to-all-done.4 = bf16[128,4,256]{2,1,0:T(4,128)(2,1)S(1)} async-done(((bf16[128,4,256]{2,1,0:T(4,128)(2,1)}), bf16[128,4,256]{2,1,0:T(4,128)(2,1)S(1)}, u32[]{:S(2)}, u32[]{:S(2)}) %all-to-all-start.4) | async-done | bytes 262176 | tf_op jit(solution)/shard_map/all_to_all | solution.py:20
  127.9 0.2 reshape.230
  128.1 0.2 fusion.3
  128.3 0.2 fusion.1
  128.5 0.7 pad_maximum_fusion.1
  129.3 3.9 %all-to-all-start.5 = ((bf16[32,16,256]{2,1,0:T(8,128)(2,1)}), bf16[32,16,256]{2,1,0:T(8,128)(2,1)S(1)}, u32[]{:S(2)}, u32[]{:S(2)}) async-start(bf16[32,16,256]{2,1,0:T(8,128)(2,1)} %bitcast.43), calls=%async_computation.5 | async-start | bytes 524288 | tf_op jit(solution)/shard_map/all_to_all | solution.py:20
  133.2 8.3 %all-to-all-done.5 = bf16[32,16,256]{2,1,0:T(8,128)(2,1)S(1)} async-done(((bf16[32,16,256]{2,1,0:T(8,128)(2,1)}), bf16[32,16,256]{2,1,0:T(8,128)(2,1)S(1)}, u32[]{:S(2)}, u32[]{:S(2)}) %all-to-all-start.5) | async-done | bytes 262176 | tf_op jit(solution)/shard_map/all_to_all | solution.py:20
  141.6 0.6 add_convert_fusion
  (72 shorter events, 1.0 us)
Async XLA Ops:
  0.0 24.0 %copy-start = (f32[16,1,128,128]{3,2,1,0:T(8,128)S(1)}, f32[16,1,128,128]{3,2,1,0:T(8,128)}, u32[]{:S(2)}) copy-start(f32[16,1,128,128]{3,2,1,0:T(8,128)} %param.31) | copy-start | bytes 3145732
  0.0 35.0 %collective-permute-start.2 = (bf16[512,256]{1,0:T(8,128)(2,1)}, bf16[512,256]{1,0:T(8,128)(2,1)S(1)}, u32[]{:S(2)}, u32[]{:S(2)}) collective-permute-start(bf16[512,256]{1,0:T(8,128)(2,1)} %param.30), channel_id=1, source_target_pairs={{0,3},{1,0},{2,1},{3,2},{4,7},{5,4},{6,5},{7,6},{8,11},{9,8},{10,9... | collective-permute-start | bytes 786440 | tf_op jit(solution)/shard_map/ppermute | solution.py:44
  5.3 29.8 %collective-permute-start.1 = (bf16[512,256]{1,0:T(8,128)(2,1)}, bf16[512,256]{1,0:T(8,128)(2,1)S(1)}, u32[]{:S(2)}, u32[]{:S(2)}) collective-permute-start(bf16[512,256]{1,0:T(8,128)(2,1)} %param.30), channel_id=1, source_target_pairs={{0,2},{1,3},{2,0},{3,1},{4,6},{5,7},{6,4},{7,5},{8,10},{9,11},{10,... | collective-permute-start | bytes 786440 | tf_op jit(solution)/shard_map/ppermute | solution.py:44
  7.8 27.6 %collective-permute-start = (bf16[512,256]{1,0:T(8,128)(2,1)}, bf16[512,256]{1,0:T(8,128)(2,1)S(1)}, u32[]{:S(2)}, u32[]{:S(2)}) collective-permute-start(bf16[512,256]{1,0:T(8,128)(2,1)} %param.30), channel_id=1, source_target_pairs={{0,1},{1,2},{2,3},{3,0},{4,5},{5,6},{6,7},{7,4},{8,9},{9,10},{10,1... | collective-permute-start | bytes 786440 | tf_op jit(solution)/shard_map/ppermute | solution.py:44
  11.0 0.7 copy-start.7
  11.7 0.7 copy-start.8
  12.5 0.7 copy-start.9
  13.9 3.5 %copy-start.13 = (f32[16,2]{0,1:T(2,128)S(1)}, f32[16,2]{0,1:T(2,128)}, u32[]{:S(2)}) copy-start(f32[16,2]{0,1:T(2,128)} %param.36) | copy-start | bytes 388
  13.9 3.5 %copy-start.6 = (f32[1024]{0:T(1024)S(1)}, f32[1024]{0:T(1024)}, u32[]{:S(2)}) copy-start(f32[1024]{0:T(1024)} %param.23) | copy-start | bytes 12292
  13.9 8.5 %all-to-all-start = ((bf16[4,40,256]{2,1,0:T(8,128)(2,1)}), bf16[4,40,256]{2,1,0:T(8,128)(2,1)S(1)}, u32[]{:S(2)}, u32[]{:S(2)}) async-start(bf16[4,40,256]{2,1,0:T(8,128)(2,1)} %copy.66), calls=%async_computation | async-start | bytes 163840 | tf_op jit(solution)/shard_map/all_to_all | solution.py:20
  17.4 5.3 %copy-start.2 = (bf16[1024,128]{1,0:T(8,128)(2,1)S(1)}, bf16[1024,128]{1,0:T(8,128)(2,1)}, u32[]{:S(2)}) copy-start(bf16[1024,128]{1,0:T(8,128)(2,1)} %param.27) | copy-start | bytes 786436
  22.6 1.0 copy-start.3
  22.7 0.8 copy-start.10
  22.7 1.0 copy-start.4
  24.1 1.0 copy-start.15
  24.1 2.5 %copy-start.14 = (bf16[1024,128]{1,0:T(8,128)(2,1)S(1)}, bf16[1024,128]{1,0:T(8,128)(2,1)}, u32[]{:S(2)}) copy-start(bf16[1024,128]{1,0:T(8,128)(2,1)} %param.26) | copy-start | bytes 786436
  25.0 0.7 copy-start.17
  25.7 0.7 copy-start.16
  26.5 8.3 %copy-start.5 = (bf16[512,256]{1,0:T(8,128)(2,1)S(1)}, bf16[512,256]{1,0:T(8,128)(2,1)}, u32[]{:S(2)}) copy-start(bf16[512,256]{1,0:T(8,128)(2,1)} %param.30) | copy-start | bytes 786436
  27.3 3.4 %copy-start.11 = (s32[16,2]{0,1:T(2,128)S(1)}, s32[16,2]{0,1:T(2,128)}, u32[]{:S(2)}) copy-start(s32[16,2]{0,1:T(2,128)} %param.35) | copy-start | bytes 388
  27.3 7.6 %all-to-all-start.1 = ((bf16[4,16,128]{2,1,0:T(8,128)(2,1)}), bf16[4,16,128]{2,1,0:T(8,128)(2,1)S(1)}, u32[]{:S(2)}, u32[]{:S(2)}) async-start(bf16[4,16,128]{2,1,0:T(8,128)(2,1)} %broadcast_in_dim.28), calls=%async_computation.1 | async-start | bytes 32768 | tf_op jit(solution)/shard_map/all_to_all | solution.py:20
  35.7 0.7 copy-start.12
  36.4 11.1 %collective-permute-start.3 = (bf16[16,1024]{1,0:T(8,128)(2,1)S(1)}, bf16[16,1024]{1,0:T(8,128)(2,1)S(1)}, u32[]{:S(2)}, u32[]{:S(2)}) collective-permute-start(bf16[16,1024]{1,0:T(8,128)(2,1)S(1)} %get-tuple-element.5), channel_id=1, source_target_pairs={{0,4},{4,0},{1,5},{5,1},{2,6},{6,2},{3,7},{7,3},{8,12},{12,8},{9,1... | collective-permute-start | bytes 98312 | tf_op jit(solution)/shard_map/ppermute | solution.py:135
  47.6 16.3 %collective-permute-start.4 = (bf16[32,1024]{1,0:T(8,128)(2,1)S(1)}, bf16[32,1024]{1,0:T(8,128)(2,1)S(1)}, u32[]{:S(2)}, u32[]{:S(2)}) collective-permute-start(bf16[32,1024]{1,0:T(8,128)(2,1)S(1)} %pad_maximum_fusion.7), channel_id=1, source_target_pairs={{0,8},{8,0},{1,9},{9,1},{2,10},{10,2},{3,11},{11,3},{4,12},{12,4},... | collective-permute-start | bytes 196616 | tf_op jit(solution)/shard_map/ppermute | solution.py:135
  50.6 28.5 %all-to-all-start.3 = ((bf16[128,4,256]{2,1,0:T(4,128)(2,1)}), bf16[128,4,256]{2,1,0:T(4,128)(2,1)S(1)}, u32[]{:S(2)}, u32[]{:S(2)}) async-start(bf16[128,4,256]{2,1,0:T(4,128)(2,1)} %reshape.216), calls=%async_computation.3 | async-start | bytes 524288 | tf_op jit(solution)/shard_map/all_to_all | solution.py:20
  63.9 19.6 %collective-permute-start.5 = (bf16[64,1024]{1,0:T(8,128)(2,1)S(1)}, bf16[64,1024]{1,0:T(8,128)(2,1)S(1)}, u32[]{:S(2)}, u32[]{:S(2)}) collective-permute-start(bf16[64,1024]{1,0:T(8,128)(2,1)S(1)} %pad_maximum_fusion.2), channel_id=1, source_target_pairs={{0,64},{64,0},{1,65},{65,1},{2,66},{66,2},{3,67},{67,3},{4,68},{68... | collective-permute-start | bytes 393224 | tf_op jit(solution)/shard_map/ppermute | solution.py:135
  80.0 23.7 %all-to-all-start.2 = ((bf16[16,72,256]{2,1,0:T(8,128)(2,1)}), bf16[16,72,256]{2,1,0:T(8,128)(2,1)S(1)}, u32[]{:S(2)}, u32[]{:S(2)}) async-start(bf16[16,72,256]{2,1,0:T(8,128)(2,1)} %broadcast_in_dim.30), calls=%async_computation.2 | async-start | bytes 1179648 | tf_op jit(solution)/shard_map/all_to_all | solution.py:20
  83.6 1.1 copy-start.1
  103.7 24.2 %all-to-all-start.4 = ((bf16[128,4,256]{2,1,0:T(4,128)(2,1)}), bf16[128,4,256]{2,1,0:T(4,128)(2,1)S(1)}, u32[]{:S(2)}, u32[]{:S(2)}) async-start(bf16[128,4,256]{2,1,0:T(4,128)(2,1)} %reshape.218), calls=%async_computation.4 | async-start | bytes 524288 | tf_op jit(solution)/shard_map/all_to_all | solution.py:20
  129.3 12.3 %all-to-all-start.5 = ((bf16[32,16,256]{2,1,0:T(8,128)(2,1)}), bf16[32,16,256]{2,1,0:T(8,128)(2,1)S(1)}, u32[]{:S(2)}, u32[]{:S(2)}) async-start(bf16[32,16,256]{2,1,0:T(8,128)(2,1)} %bitcast.43), calls=%async_computation.5 | async-start | bytes 524288 | tf_op jit(solution)/shard_map/all_to_all | solution.py:20

commit v5 on v3

v5 whole, which is shorter than its diff:
```python
import jax
import jax.numpy as jnp
from jax import lax
from jax.experimental import pallas as pl
from jax.experimental.pallas import tpu as pltpu
from jax.sharding import Mesh, PartitionSpec as P

HEAD = 128
TOP = 2

epsilon = 1e-06
f32 = jnp.float32
bf16 = jnp.bfloat16

FAR = ("zh", "yh")
NEAR = ("zl", "yl", "c")
EP = ("zh", "zl", "yh", "yl", "c")


def exchange(blocks, axis):
    return lax.all_to_all(blocks, axis, 0, 0, tiled=True)


def to_all(shard, size):
    return jnp.broadcast_to(shard[None], (size, *shard.shape))


def dot(a, b):
    return jnp.dot(a, b, preferred_element_type=f32)


def shifted(array, axis, step):
    size = lax.axis_size(axis)
    return lax.ppermute(array, axis, [(i, (i + step) % size) for i in range(size)])


def pack_kernel(tokens, gate, up, down, mix, out):
    seqs, quarter = tokens.shape
    count, columns = out.shape[0], gate.shape[0]
    slim = columns // count
    room = out.shape[1] - seqs
    source = jnp.concatenate([gate[...], up[...], down[...]], axis=0)
    row = lax.broadcasted_iota(jnp.int32, (room, 3 * columns), 0)
    column = lax.broadcasted_iota(jnp.int32, (room, 3 * columns), 1)
    wanted = jnp.where(
        row < slim,
        row,
        jnp.where(row < 2 * slim, row + columns - slim, row + 2 * (columns - slim)),
    )
    last = lax.broadcasted_iota(jnp.int32, (room, quarter), 0) == 3 * slim
    extra = jnp.where(last, jnp.broadcast_to(mix[...].astype(f32), (room, quarter)), 0.0)
    for k in range(count):
        pick = ((column == wanted + k * slim) & (row < 3 * slim)).astype(f32).astype(bf16)
        out[k, :seqs] = tokens[...]
        out[k, seqs:] = (dot(pick, source) + extra).astype(bf16)


def pack(tokens, gate, up, down, mix, count):
    seqs, quarter = tokens.shape
    slim = gate.shape[0] // count
    rows = -(-(seqs + 3 * slim + 1) // 8) * 8
    return pl.pallas_call(
        pack_kernel,
        out_shape=jax.ShapeDtypeStruct((count, rows, quarter), bf16),
        name="pack",
    )(tokens, gate, up, down, mix)


def cell_kernel(first, gain, wq, wk, wv, wo, wi, wf, state, norm, peak, out):
    seqs = norm.shape[0]
    values = jnp.concatenate([first[k, :seqs] for k in range(first.shape[0])], axis=1).astype(f32)
    scale = lax.rsqrt(jnp.mean(values * values, axis=1, keepdims=True) + epsilon)
    rows = (values * scale * gain[...]).astype(bf16)
    query = dot(rows, wq[...])
    key = dot(rows, wk[...]) * HEAD ** (-0.5)
    value = dot(rows, wv[...])
    gate = jax.nn.sigmoid(dot(rows, wo[...]))
    wide = rows.astype(f32)
    enter = jnp.sum(wide * wi[...].astype(f32), axis=1, keepdims=True)
    forget = jnp.sum(wide * wf[...].astype(f32), axis=1, keepdims=True)
    carried = jnp.minimum(forget, 0.0) - jnp.log1p(jnp.exp(-jnp.abs(forget))) + peak[...]
    stabilizer = jnp.maximum(carried, enter)
    old = jnp.exp(carried - stabilizer)
    new = jnp.exp(enter - stabilizer) * jnp.sum(query * key, axis=1, keepdims=True)
    turned = query.T
    read = [
        jnp.sum(turned[:, b : b + 1] * state[b], axis=0, keepdims=True) for b in range(seqs)
    ]
    numerator = old * jnp.concatenate(read, axis=0) + new * value
    denominator = old * jnp.sum(query * norm[...], axis=1, keepdims=True) + new
    mixed = gate * (numerator / jnp.maximum(jnp.abs(denominator), 1.0))
    for k in range(out.shape[0]):
        out[k] = mixed.astype(bf16)


def cell(first, gain, wq, wk, wv, wo, wi, wf, state, norm, peak):
    return pl.pallas_call(
        cell_kernel,
        out_shape=jax.ShapeDtypeStruct((1, *norm.shape), bf16),
        cost_estimate=pl.CostEstimate(flops=40000000, bytes_accessed=2200000, transcendentals=9000),
        compiler_params=pltpu.CompilerParams(vmem_limit_bytes=12 << 20),
        name="cell",
    )(first, gain, wq, wk, wv, wo, wi, wf, state, norm, peak)


def residual_kernel(me, place, second, w0, w1, w2, w3, gain, ids, group, outgoing, own, resid):
    near, tp, seqs, _ = second.shape
    quarter = w0.shape[1]
    heads = jnp.concatenate(
        [
            jnp.concatenate([second[s, k, :, :HEAD] for s in range(near)], axis=0)
            for k in range(tp)
        ],
        axis=1,
    )
    total = jnp.zeros((near * seqs, 1), f32)
    for step, weight in enumerate((w0, w1, w2, w3)):
        k = (me[0] + tp - step) & (tp - 1)
        added = dot(heads, weight[...])
        old = jnp.concatenate([second[s, k, :, HEAD:] for s in range(near)], axis=0)
        values = (old.astype(f32) + added).astype(bf16)
        wide = values.astype(f32)
        total = total + jnp.sum(wide * wide, axis=1, keepdims=True)
        resid[:, pl.ds(pl.multiple_of(k * quarter, quarter), quarter)] = wide
        if step == 0:
            group[:, :quarter] = values
    start = pl.multiple_of(place[0] * seqs, seqs)
    own[...] = group[pl.ds(start, seqs), :quarter]
    scale = lax.rsqrt(total * (1.0 / (tp * quarter)) + epsilon)
    group[...] = (resid[...] * scale * gain[...]).astype(bf16)
    experts = outgoing.shape[0]
    expert = lax.broadcasted_iota(jnp.int32, (experts, seqs), 0)
    chosen = ((expert == ids[0:1, :]) | (expert == ids[1:2, :])).astype(f32).astype(bf16)
    outgoing[...] = dot(chosen, group[pl.ds(start, seqs), :]).astype(bf16)


def residual(me, place, second, weights, gain, ids, experts):
    near, tp, seqs, _ = second.shape
    quarter = weights[0].shape[1]
    whole = pl.BlockSpec(memory_space=pltpu.VMEM)
    scalar = pl.BlockSpec(memory_space=pltpu.SMEM)
    return pl.pallas_call(
        residual_kernel,
        out_shape=(
            jax.ShapeDtypeStruct((near * seqs, tp * quarter), bf16),
            jax.ShapeDtypeStruct((experts, tp * quarter), bf16),
            jax.ShapeDtypeStruct((seqs, quarter), bf16),
        ),
        in_specs=[scalar, scalar] + [whole] * 7,
        out_specs=(whole, whole, whole),
        scratch_shapes=[pltpu.VMEM((near * seqs, tp * quarter), f32)],
        cost_estimate=pl.CostEstimate(flops=140000000, bytes_accessed=2000000, transcendentals=128),
        compiler_params=pltpu.CompilerParams(vmem_limit_bytes=12 << 20),
        name="residual",
    )(me[None], place[None], second, *weights, gain, ids)


def layer(
    tokens,
    gain_mix,
    w_query,
    w_key,
    w_value,
    w_outgate,
    w_input_gate,
    w_forget_gate,
    w_mix_out,
    cell_state,
    norm_state,
    max_state,
    gain_ffn,
    route_ids,
    route_logits,
    expert_gate,
    expert_up,
    expert_down,
    dense_gate,
    dense_up,
    dense_down,
    dense_mix,
):
    seqs, quarter = tokens.shape
    tp = lax.axis_size("x")
    far = lax.axis_size(FAR)
    near = lax.axis_size(NEAR)
    experts = lax.axis_size(EP)
    me = lax.axis_index("x")
    place = lax.axis_index(NEAR)
    slim = dense_gate.shape[1] // tp

    sent = pack(tokens, dense_gate.T, dense_up.T, dense_down, dense_mix[None], tp)
    first = exchange(sent, "x")
    mix_row = first[:, seqs + 3 * slim].reshape(1, -1)

    mix_out = {0: w_mix_out}
    for step in (2, 1, 3):
        mix_out[step] = shifted(w_mix_out, "x", step)

    dense = to_all(first[:, seqs : seqs + 3 * slim].reshape(tp * 3 * slim, quarter), far)
    dense = exchange(dense, FAR)
    dense = jnp.transpose(dense.reshape(far, tp, 3, slim, quarter), (2, 0, 3, 1, 4))
    dense = dense.reshape(3, far * slim, tp * quarter)

    mixed = cell(
        first,
        gain_mix[None],
        w_query,
        w_key,
        w_value,
        w_outgate,
        w_input_gate.T,
        w_forget_gate.T,
        cell_state[:, 0],
        norm_state[:, 0],
        max_state,
    )[0]
    sent = to_all(jnp.concatenate([mixed, tokens], axis=1), near * tp)
    second = exchange(sent, NEAR + ("x",))
    second = second.reshape(near, tp, seqs, HEAD + quarter)
    group, outgoing, own_resid = residual(
        me, place, second, [mix_out[k] for k in range(tp)], gain_ffn[None], route_ids.T, experts
    )

    flat_ids = route_ids.reshape(-1)
    picks = (flat_ids[:, None] == jnp.arange(experts, dtype=jnp.int32)[None, :]).astype(bf16)
    outgoing = outgoing.reshape(experts, 4, -1)
    received = exchange(outgoing, EP)

    rows = received.reshape(experts, -1)
    hidden = (jax.nn.silu(dot(rows, expert_gate[0])) * dot(rows, expert_up[0])).astype(bf16)
    partial = dot(hidden, expert_down[0]).astype(bf16).reshape(experts, 4, -1)
    returned = exchange(partial, EP)

    transposed = (((1,), (1,)), ((), ()))
    gate_cols = lax.dot_general(group, dense[0], transposed, preferred_element_type=f32)
    up_cols = lax.dot_general(group, dense[1], transposed, preferred_element_type=f32)
    dense_hidden = (jax.nn.silu(gate_cols) * up_cols).astype(bf16)
    dense_part = dot(dense_hidden, dense[2]).reshape(near, seqs, -1)

    picked = dot(picks, returned.reshape(experts, -1)).reshape(seqs, TOP, -1)
    route_weight = jax.nn.sigmoid(route_logits - route_logits[:, ::-1])
    moe = jnp.sum(route_weight[..., None] * picked, axis=1)
    mix_gate = jax.nn.sigmoid(
        jnp.sum(group.astype(f32) * mix_row.astype(f32), axis=1, keepdims=True)
    ).reshape(near, seqs, 1)
    mine = (jnp.arange(near) == place)[:, None, None]
    part = mix_gate * dense_part + jnp.where(mine, moe[None], 0.0)
    part = jnp.swapaxes(part.astype(bf16).reshape(near, seqs, tp, quarter), 1, 2)
    part = part.reshape(near * tp, seqs, quarter)
    parts = exchange(part, NEAR + ("x",))
    total = own_resid.astype(f32) + parts.astype(f32).sum(axis=0)
    return total.astype(bf16)


def solution(mesh):
    fine = Mesh(mesh.devices.reshape(4, 2, 4, 2, 2, 4), EP + ("x",))
    return jax.shard_map(
        layer,
        mesh=fine,
        in_specs=(
            P(EP, "x"),
            P(),
            P(None, "x"),
            P(None, "x"),
            P(None, "x"),
            P(None, "x"),
            P(None, "x"),
            P(None, "x"),
            P(None, "x"),
            P(EP, "x", None, None),
            P(EP, "x", None),
            P(EP, "x"),
            P(),
            P(EP, None),
            P(EP, None),
            P(EP, None, "x"),
            P(EP, None, "x"),
            P(EP, "x", None),
            P("x", EP),
            P("x", EP),
            P(EP, "x"),
            P("x"),
        ),
        out_specs=P(EP, "x"),
        check_vma=False,
    )
```

time: 148 us -> 137 us (0.926)
  waiting for transfers between devices: 65.2 us -> 50.9 us
  blocking collectives: 0 us -> 11.9 us
  matrix products: 7.66 us -> 3.23 us
  starting transfers between devices: 58 us -> 53.6 us
  Pallas kernels: 0 us -> 3.07 us
  other arithmetic: 3.32 us -> 0.85 us
    all_to_all x6 -> x5, waiting for transfers between devices: 56.8 us -> 43.4 us  [exchange(): return lax.all_to_all(blocks, axis, 0, 0, tiled=True)]
    all_to_all x0 -> x1, blocking collectives: none -> 11.9 us  [exchange(): return lax.all_to_all(blocks, axis, 0, 0, tiled=True)]
    all_to_all x6 -> x5, starting transfers between devices: 48 us -> 44.6 us  [exchange(): return lax.all_to_all(blocks, axis, 0, 0, tiled=True)]
    dot_general x14 -> x4, matrix products: 5.99 us -> 2.77 us  [dot(): return jnp.dot(a, b, preferred_element_type=f32)]
    pallas_call x0 -> x3, Pallas kernels: none -> 3.07 us  [the longest x1 1.53 us: pack(): pl.pallas_call(pack_kernel, out_shape=jax.ShapeDtypeStruct((count, rows,...]
    unnamed x39 -> x38, local copies, waits for them, and re-layouts: 5.41 us -> 6.31 us
  transfers between devices with their start and end apart: 9 -> 8, of which waited for: 7 -> 7; matrix products, arithmetic and copies ran while one was open for 3% -> 2% of each run, Pallas kernels for 0% -> 0%
where the time goes in v5:
time: 137 us; the launch traced here: 136 us
  starting transfers between devices  53.6 us (39%)
  waiting for transfers between devices  50.9 us (37%)
  local copies, waits for them, and re-layouts  12.2 us (9%)
  blocking collectives  11.9 us (9%)
  matrix products  3.23 us (2%)
  Pallas kernels  3.07 us (2%)
    all_to_all x5, starting transfers between devices, exchange(): return lax.all_to_all(blocks, axis, 0, 0, tiled=True)  44.6 us
    all_to_all x5, waiting for transfers between devices, exchange(): return lax.all_to_all(blocks, axis, 0, 0, tiled=True)  43.4 us
    all_to_all x1, blocking collectives, exchange(): return lax.all_to_all(blocks, axis, 0, 0, tiled=True)  11.9 us
    ppermute x3, starting transfers between devices, shifted(): lax.ppermute(array, axis, [(i, (i + step) % size) for i in range(size)])  8.97 us
    ppermute x3, waiting for transfers between devices, shifted(): lax.ppermute(array, axis, [(i, (i + step) % size) for i in range(size)])  7.51 us
    unnamed x38, local copies, waits for them, and re-layouts  6.31 us
    dot_general x4, matrix products, dot(): return jnp.dot(a, b, preferred_element_type=f32)  2.77 us
  transfers between devices with their start and end apart: 8, of which 7 were waited for; matrix products, arithmetic and copies ran while one was open for 2% of the time, Pallas kernels for 0%

profile of v5, /device:TPU:1, one launch (start us, length us, event | category | flops | bytes accessed | tf_op | source)
XLA Modules:
  0.0 136.1 jit_solution(7656414075662313837)
XLA Ops:
  0.0 0.0 copy-start
  0.0 0.0 copy-start.2
  0.0 1.3 broadcast_in_dim.55.mix
  1.3 1.5 %pack.1 = bf16[4,40,256]{2,1,0:T(8,128)(2,1)} custom-call(bf16[16,256]{1,0:T(8,128)(2,1)} %tokens.1, bf16[24,256]{1,0:T(8,128)(2,1)} %bitcast.69, bf16[24,256]{1,0:T(8,128)(2,1)} %bitcast.70, bf16[24,256]{1,0:T(8,128)(2,1)} %down.1, bf16[1,256]{1,0:T(2,128)(2,1)} %broadcast_in_dim.55.mix), custom_call_target="tpu_custom_call" | custom-call | tf_op jit(solution)/shard_map/pack/pallas_call | solution.py:62
  2.8 0.0 copy-start.16
  2.8 0.0 copy-start.10
  2.8 5.0 %all-to-all-start = ((bf16[4,40,256]{2,1,0:T(8,128)(2,1)}), bf16[4,40,256]{2,1,0:T(8,128)(2,1)S(1)}, u32[]{:S(2)}, u32[]{:S(2)}) async-start(bf16[4,40,256]{2,1,0:T(8,128)(2,1)} %pack.1), calls=%async_computation | async-start | bytes 163840 | tf_op jit(solution)/shard_map/all_to_all | solution.py:21
  7.8 0.0 copy-done.16
  7.8 0.1 copy.33.peak
  7.9 4.5 %all-to-all-done.first = bf16[4,40,256]{2,1,0:T(8,128)(2,1)S(1)} async-done(((bf16[4,40,256]{2,1,0:T(8,128)(2,1)}), bf16[4,40,256]{2,1,0:T(8,128)(2,1)S(1)}, u32[]{:S(2)}, u32[]{:S(2)}) %all-to-all-start) | async-done | bytes 81952 | tf_op jit(solution)/shard_map/all_to_all | solution.py:21
  12.4 0.0 copy-done.2
  12.4 0.0 copy-done.10
  12.4 0.0 copy-done.7
  12.4 0.7 copy-done.9
  13.1 0.0 copy-done.8
  13.1 1.2 copy-done.1
  14.3 0.9 copy-done.3
  15.3 0.9 copy-done.4
  16.2 0.9 copy-done.5
  17.2 0.9 cell.1
  18.1 0.0 copy-done.14
  18.1 0.8 broadcast_in_dim.57
  18.9 10.0 %all-to-all-start.1 = ((bf16[32,16,384]{2,1,0:T(8,128)(2,1)}), bf16[32,16,384]{2,1,0:T(8,128)(2,1)S(1)}, u32[]{:S(2)}, u32[]{:S(2)}) async-start(bf16[32,16,384]{2,1,0:T(8,128)(2,1)} %broadcast_in_dim.57), calls=%async_computation.1 | async-start | bytes 786432 | tf_op jit(solution)/shard_map/all_to_all | solution.py:21
  28.9 9.5 %all-to-all-done.1 = bf16[32,16,384]{2,1,0:T(8,128)(2,1)S(1)} async-done(((bf16[32,16,384]{2,1,0:T(8,128)(2,1)}), bf16[32,16,384]{2,1,0:T(8,128)(2,1)S(1)}, u32[]{:S(2)}, u32[]{:S(2)}) %all-to-all-start.1) | async-done | bytes 393248 | tf_op jit(solution)/shard_map/all_to_all | solution.py:21
  38.4 0.9 broadcast_in_dim.60
  39.3 11.2 %all-to-all-start.2 = ((bf16[16,72,256]{2,1,0:T(8,128)(2,1)}), bf16[16,72,256]{2,1,0:T(8,128)(2,1)S(1)}, u32[]{:S(2)}, u32[]{:S(2)}) async-start(bf16[16,72,256]{2,1,0:T(8,128)(2,1)} %broadcast_in_dim.60), calls=%async_computation.2 | async-start | bytes 1179648 | tf_op jit(solution)/shard_map/all_to_all | solution.py:21
  50.5 0.0 copy-done.6
  50.5 2.5 %collective-permute-start.1 = (bf16[512,256]{1,0:T(8,128)(2,1)S(1)}, bf16[512,256]{1,0:T(8,128)(2,1)S(1)}, u32[]{:S(2)}, u32[]{:S(2)}) collective-permute-start(bf16[512,256]{1,0:T(8,128)(2,1)S(1)} %copy-done.6), channel_id=1, source_target_pairs={{0,2},{1,3},{2,0},{3,1},{4,6},{5,7},{6,4},{7,5},{8,10},{9,11},{10,... | collective-permute-start | bytes 786440 | tf_op jit(solution)/shard_map/ppermute | solution.py:34
  53.0 2.8 %collective-permute-start = (bf16[512,256]{1,0:T(8,128)(2,1)S(1)}, bf16[512,256]{1,0:T(8,128)(2,1)S(1)}, u32[]{:S(2)}, u32[]{:S(2)}) collective-permute-start(bf16[512,256]{1,0:T(8,128)(2,1)S(1)} %copy-done.6), channel_id=1, source_target_pairs={{0,1},{1,2},{2,3},{3,0},{4,5},{5,6},{6,7},{7,4},{8,9},{9,10},{10,1... | collective-permute-start | bytes 786440 | tf_op jit(solution)/shard_map/ppermute | solution.py:34
  55.7 3.7 %collective-permute-start.2 = (bf16[512,256]{1,0:T(8,128)(2,1)S(1)}, bf16[512,256]{1,0:T(8,128)(2,1)S(1)}, u32[]{:S(2)}, u32[]{:S(2)}) collective-permute-start(bf16[512,256]{1,0:T(8,128)(2,1)S(1)} %copy-done.6), channel_id=1, source_target_pairs={{0,3},{1,0},{2,1},{3,2},{4,7},{5,4},{6,5},{7,6},{8,11},{9,8},{10,9... | collective-permute-start | bytes 786440 | tf_op jit(solution)/shard_map/ppermute | solution.py:34
  59.5 0.0 copy-start.15
  59.5 0.7 copy-done.15
  60.2 0.7 collective-permute-done.1.w2
  60.9 6.8 %collective-permute-done.w1 = bf16[512,256]{1,0:T(8,128)(2,1)S(1)} collective-permute-done((bf16[512,256]{1,0:T(8,128)(2,1)S(1)}, bf16[512,256]{1,0:T(8,128)(2,1)S(1)}, u32[]{:S(2)}, u32[]{:S(2)}) %collective-permute-start) | collective-permute-done | bytes 262176 | tf_op jit(solution)/shard_map/ppermute | solution.py:34
  67.7 0.0 collective-permute-done.2.w3
  67.7 0.7 copy-done.11
  68.4 0.0 copy-done.12
  68.4 0.6 residual.1
  69.1 0.9 reshape.93
  70.0 0.5 all-to-all-done.2
  70.5 13.0 %all-to-all-start.3 = ((bf16[128,4,256]{2,1,0:T(4,128)(2,1)}), bf16[128,4,256]{2,1,0:T(4,128)(2,1)S(1)}, u32[]{:S(2)}, u32[]{:S(2)}) async-start(bf16[128,4,256]{2,1,0:T(4,128)(2,1)} %reshape.93), calls=%async_computation.3 | async-start | bytes 524288 | tf_op jit(solution)/shard_map/all_to_all | solution.py:21
  83.5 0.1 multiply_reduce_fusion
  83.6 0.1 div.24
  83.7 0.1 copy.34
  83.8 14.9 %all-to-all-done.3 = bf16[128,4,256]{2,1,0:T(4,128)(2,1)S(1)} async-done(((bf16[128,4,256]{2,1,0:T(4,128)(2,1)}), bf16[128,4,256]{2,1,0:T(4,128)(2,1)S(1)}, u32[]{:S(2)}, u32[]{:S(2)}) %all-to-all-start.3) | async-done | bytes 262176 | tf_op jit(solution)/shard_map/all_to_all | solution.py:21
  98.7 0.0 copy-done.13
  98.7 0.4 fusion.7
  99.1 0.0 copy-done
  99.1 2.0 %convolution_convert_fusion = bf16[128,1024]{1,0:T(8,128)(2,1)S(1)} fusion(bf16[128,1024]{1,0:T(8,128)(2,1)S(1)} %bitcast.60, bf16[1,352,1024]{2,1,0:T(8,128)(2,1)S(1)} %copy-done, bf16[1,1024,352]{1,2,0:T(8,128)(2,1)} %param.38, f32[128,352]{0,1:T(8,128)S(1)} %fusion.7), kind=kOutput, calls=%fused_computation.3 | convolution fusion | flops 184950784 | bytes 2146304 | tf_op jit(solution)/shard_map/dot_general | solution.py:29
  101.1 0.9 reshape.95
  102.0 5.5 %all-to-all-start.4 = ((bf16[128,4,256]{2,1,0:T(4,128)(2,1)}), bf16[128,4,256]{2,1,0:T(4,128)(2,1)S(1)}, u32[]{:S(2)}, u32[]{:S(2)}) async-start(bf16[128,4,256]{2,1,0:T(4,128)(2,1)} %reshape.95), calls=%async_computation.4 | async-start | bytes 524288 | tf_op jit(solution)/shard_map/all_to_all | solution.py:21
  107.6 0.2 copy.38
  107.7 0.1 reshape.99
  107.9 0.2 copy.36
  108.1 0.2 copy.35
  108.2 0.2 fusion.21
  108.5 0.2 multiply_convert_fusion
  108.7 0.1 copy.37
  108.8 14.0 %all-to-all-done.4 = bf16[128,4,256]{2,1,0:T(4,128)(2,1)S(1)} async-done(((bf16[128,4,256]{2,1,0:T(4,128)(2,1)}), bf16[128,4,256]{2,1,0:T(4,128)(2,1)S(1)}, u32[]{:S(2)}, u32[]{:S(2)}) %all-to-all-start.4) | async-done | bytes 262176 | tf_op jit(solution)/shard_map/all_to_all | solution.py:21
  122.9 0.2 reshape.100
  123.0 0.2 fusion.3
  123.2 0.2 fusion.1
  123.5 11.9 %all_to_all.30 = bf16[32,16,256]{2,1,0:T(8,128)(2,1)S(1)} all-to-all(bf16[32,16,256]{2,1,0:T(8,128)(2,1)S(1)} %bitcast.62), channel_id=1, replica_groups=mesh['zh'=4,'zl'=2,'yh'=4,'yl'=2,'c'=2,'x'=4] {'zl','yl','c','x'}, dimensions={0} | all-to-all | bytes 524288 | tf_op jit(solution)/shard_map/all_to_all | solution.py:21
  135.5 0.6 add_convert_fusion
  (27 shorter events, 0.3 us)
Async XLA Ops:
  0.0 99.1 %copy-start = (bf16[1,352,1024]{2,1,0:T(8,128)(2,1)S(1)}, bf16[1,352,1024]{2,1,0:T(8,128)(2,1)}, u32[]{:S(2)}) copy-start(bf16[1,352,1024]{2,1,0:T(8,128)(2,1)} %param.39) | copy-start | bytes 2162692
  0.0 12.4 %copy-start.2 = (bf16[1024,128]{1,0:T(8,128)(2,1)S(1)}, bf16[1024,128]{1,0:T(8,128)(2,1)}, u32[]{:S(2)}) copy-start(bf16[1024,128]{1,0:T(8,128)(2,1)} %wq.1) | copy-start | bytes 786436
  2.8 5.0 %copy-start.16 = (f32[16,1]{0,1:T(1,128)S(1)}, f32[16,1]{0,1:T(1,128)}, u32[]{:S(2)}) copy-start(f32[16,1]{0,1:T(1,128)} %param.33) | copy-start | bytes 196
  2.8 9.5 %copy-start.10 = (bf16[1024,1]{0,1:T(2,128)(2,1)S(1)}, bf16[1024,1]{0,1:T(2,128)(2,1)}, u32[]{:S(2)}) copy-start(bf16[1024,1]{0,1:T(2,128)(2,1)} %param.29) | copy-start | bytes 6148
  2.8 9.5 %all-to-all-start = ((bf16[4,40,256]{2,1,0:T(8,128)(2,1)}), bf16[4,40,256]{2,1,0:T(8,128)(2,1)S(1)}, u32[]{:S(2)}, u32[]{:S(2)}) async-start(bf16[4,40,256]{2,1,0:T(8,128)(2,1)} %pack.1), calls=%async_computation | async-start | bytes 163840 | tf_op jit(solution)/shard_map/all_to_all | solution.py:21
  7.8 4.6 %copy-start.7 = (f32[16,1,128]{2,1,0:T(1,128)S(1)}, f32[16,1,128]{2,1,0:T(1,128)}, u32[]{:S(2)}) copy-start(f32[16,1,128]{2,1,0:T(1,128)} %param.32) | copy-start | bytes 24580
  12.4 0.7 copy-start.9
  12.4 0.7 copy-start.8
  13.1 1.2 copy-start.1
  14.3 0.9 copy-start.3
  15.3 0.9 copy-start.4
  16.2 0.9 copy-start.5
  17.2 0.9 copy-start.14
  18.9 19.5 %all-to-all-start.1 = ((bf16[32,16,384]{2,1,0:T(8,128)(2,1)}), bf16[32,16,384]{2,1,0:T(8,128)(2,1)S(1)}, u32[]{:S(2)}, u32[]{:S(2)}) async-start(bf16[32,16,384]{2,1,0:T(8,128)(2,1)} %broadcast_in_dim.57), calls=%async_computation.1 | async-start | bytes 786432 | tf_op jit(solution)/shard_map/all_to_all | solution.py:21
  39.3 11.2 %copy-start.6 = (bf16[512,256]{1,0:T(8,128)(2,1)S(1)}, bf16[512,256]{1,0:T(8,128)(2,1)}, u32[]{:S(2)}) copy-start(bf16[512,256]{1,0:T(8,128)(2,1)} %w0.1) | copy-start | bytes 786436
  39.3 31.2 %all-to-all-start.2 = ((bf16[16,72,256]{2,1,0:T(8,128)(2,1)}), bf16[16,72,256]{2,1,0:T(8,128)(2,1)S(1)}, u32[]{:S(2)}, u32[]{:S(2)}) async-start(bf16[16,72,256]{2,1,0:T(8,128)(2,1)} %broadcast_in_dim.60), calls=%async_computation.2 | async-start | bytes 1179648 | tf_op jit(solution)/shard_map/all_to_all | solution.py:21
  50.5 10.4 %collective-permute-start.1 = (bf16[512,256]{1,0:T(8,128)(2,1)S(1)}, bf16[512,256]{1,0:T(8,128)(2,1)S(1)}, u32[]{:S(2)}, u32[]{:S(2)}) collective-permute-start(bf16[512,256]{1,0:T(8,128)(2,1)S(1)} %copy-done.6), channel_id=1, source_target_pairs={{0,2},{1,3},{2,0},{3,1},{4,6},{5,7},{6,4},{7,5},{8,10},{9,11},{10,... | collective-permute-start | bytes 786440 | tf_op jit(solution)/shard_map/ppermute | solution.py:34
  53.0 14.8 %collective-permute-start = (bf16[512,256]{1,0:T(8,128)(2,1)S(1)}, bf16[512,256]{1,0:T(8,128)(2,1)S(1)}, u32[]{:S(2)}, u32[]{:S(2)}) collective-permute-start(bf16[512,256]{1,0:T(8,128)(2,1)S(1)} %copy-done.6), channel_id=1, source_target_pairs={{0,1},{1,2},{2,3},{3,0},{4,5},{5,6},{6,7},{7,4},{8,9},{9,10},{10,1... | collective-permute-start | bytes 786440 | tf_op jit(solution)/shard_map/ppermute | solution.py:34
  55.7 12.0 %collective-permute-start.2 = (bf16[512,256]{1,0:T(8,128)(2,1)S(1)}, bf16[512,256]{1,0:T(8,128)(2,1)S(1)}, u32[]{:S(2)}, u32[]{:S(2)}) collective-permute-start(bf16[512,256]{1,0:T(8,128)(2,1)S(1)} %copy-done.6), channel_id=1, source_target_pairs={{0,3},{1,0},{2,1},{3,2},{4,7},{5,4},{6,5},{7,6},{8,11},{9,8},{10,9... | collective-permute-start | bytes 786440 | tf_op jit(solution)/shard_map/ppermute | solution.py:34
  59.5 0.7 copy-start.15
  67.7 0.7 copy-start.11
  67.7 0.7 copy-start.12
  70.5 28.2 %all-to-all-start.3 = ((bf16[128,4,256]{2,1,0:T(4,128)(2,1)}), bf16[128,4,256]{2,1,0:T(4,128)(2,1)S(1)}, u32[]{:S(2)}, u32[]{:S(2)}) async-start(bf16[128,4,256]{2,1,0:T(4,128)(2,1)} %reshape.93), calls=%async_computation.3 | async-start | bytes 524288 | tf_op jit(solution)/shard_map/all_to_all | solution.py:21
  83.7 15.0 %copy-start.13 = (bf16[1,1024,352]{1,2,0:T(8,128)(2,1)S(1)}, bf16[1,1024,352]{1,2,0:T(8,128)(2,1)}, u32[]{:S(2)}) copy-start(bf16[1,1024,352]{1,2,0:T(8,128)(2,1)} %param.37) | copy-start | bytes 2162692
  102.0 20.9 %all-to-all-start.4 = ((bf16[128,4,256]{2,1,0:T(4,128)(2,1)}), bf16[128,4,256]{2,1,0:T(4,128)(2,1)S(1)}, u32[]{:S(2)}, u32[]{:S(2)}) async-start(bf16[128,4,256]{2,1,0:T(4,128)(2,1)} %reshape.95), calls=%async_computation.4 | async-start | bytes 524288 | tf_op jit(solution)/shard_map/all_to_all | solution.py:21

commit v6 on v5

--- a/solution.py
+++ b/solution.py
@@ -6,14 +6,14 @@
 from jax.sharding import Mesh, PartitionSpec as P
 
 HEAD = 128
-TOP = 2
 
 epsilon = 1e-06
 f32 = jnp.float32
 bf16 = jnp.bfloat16
 
-FAR = ("zh", "yh")
-NEAR = ("zl", "yl", "c")
+FAR = ("zh", "yh", "c")
+NEAR = ("zl", "yl")
+SLOT = 8
 EP = ("zh", "zl", "yh", "yl", "c")
 
 
@@ -27,6 +27,10 @@
 
 def dot(a, b):
     return jnp.dot(a, b, preferred_element_type=f32)
+
+
+def dot_turned(a, b):
+    return lax.dot_general(a, b, (((1,), (1,)), ((), ())), preferred_element_type=f32)
 
 
 def shifted(array, axis, step):
@@ -42,26 +46,21 @@
     source = jnp.concatenate([gate[...], up[...], down[...]], axis=0)
     row = lax.broadcasted_iota(jnp.int32, (room, 3 * columns), 0)
     column = lax.broadcasted_iota(jnp.int32, (room, 3 * columns), 1)
-    wanted = jnp.where(
-        row < slim,
-        row,
-        jnp.where(row < 2 * slim, row + columns - slim, row + 2 * (columns - slim)),
-    )
-    last = lax.broadcasted_iota(jnp.int32, (room, quarter), 0) == 3 * slim
+    slot = row & (SLOT - 1)
+    wanted = slot + lax.div(row, SLOT) * columns
+    last = lax.broadcasted_iota(jnp.int32, (room, quarter), 0) == 3 * SLOT
     extra = jnp.where(last, jnp.broadcast_to(mix[...].astype(f32), (room, quarter)), 0.0)
     for k in range(count):
-        pick = ((column == wanted + k * slim) & (row < 3 * slim)).astype(f32).astype(bf16)
+        pick = (column == wanted + k * slim) & (slot < slim) & (row < 3 * SLOT)
         out[k, :seqs] = tokens[...]
-        out[k, seqs:] = (dot(pick, source) + extra).astype(bf16)
+        out[k, seqs:] = (dot(pick.astype(f32).astype(bf16), source) + extra).astype(bf16)
 
 
 def pack(tokens, gate, up, down, mix, count):
     seqs, quarter = tokens.shape
-    slim = gate.shape[0] // count
-    rows = -(-(seqs + 3 * slim + 1) // 8) * 8
     return pl.pallas_call(
         pack_kernel,
-        out_shape=jax.ShapeDtypeStruct((count, rows, quarter), bf16),
+        out_shape=jax.ShapeDtypeStruct((count, seqs + 4 * SLOT, quarter), bf16),
         name="pack",
     )(tokens, gate, up, down, mix)
 
@@ -98,7 +97,6 @@
         cell_kernel,
         out_shape=jax.ShapeDtypeStruct((1, *norm.shape), bf16),
         cost_estimate=pl.CostEstimate(flops=40000000, bytes_accessed=2200000, transcendentals=9000),
-        compiler_params=pltpu.CompilerParams(vmem_limit_bytes=12 << 20),
         name="cell",
     )(first, gain, wq, wk, wv, wo, wi, wf, state, norm, peak)
 
@@ -153,6 +151,68 @@
         compiler_params=pltpu.CompilerParams(vmem_limit_bytes=12 << 20),
         name="residual",
     )(me[None], place[None], second, *weights, gain, ids)
+
+
+def dense_kernel(group, weights, mix, out):
+    far, tp, _, quarter = weights.shape
+
+    def matrix(k, place):
+        return weights[:, k, place * SLOT : (place + 1) * SLOT].reshape(far * SLOT, quarter)
+
+    rows = group[...]
+    gate, up = 0.0, 0.0
+    for k in range(tp):
+        part = rows[:, k * quarter : (k + 1) * quarter]
+        gate = gate + dot_turned(part, matrix(k, 0))
+        up = up + dot_turned(part, matrix(k, 1))
+    hidden = (gate * jax.nn.sigmoid(gate) * up).astype(bf16)
+    logit = jnp.sum(rows.astype(f32) * mix[...].astype(f32), axis=1, keepdims=True)
+    mix_gate = jax.nn.sigmoid(logit)
+    for k in range(tp):
+        out[:, k * quarter : (k + 1) * quarter] = mix_gate * dot(hidden, matrix(k, 2))
+
+
+def dense_branch(group, weights, mix):
+    return pl.pallas_call(
+        dense_kernel,
+        out_shape=jax.ShapeDtypeStruct(group.shape, f32),
+        compiler_params=pltpu.CompilerParams(vmem_limit_bytes=12 << 20),
+        cost_estimate=pl.CostEstimate(flops=100000000, bytes_accessed=1800000, transcendentals=32000),
+        name="dense",
+    )(group, weights, mix)
+
+
+def combine_kernel(place, part, returned, ids, weights, out):
+    seqs, quarter = out.shape[1:]
+    experts = returned.shape[0]
+    tp = returned.shape[1] // quarter
+    expert = lax.broadcasted_iota(jnp.int32, (seqs, experts), 1)
+    here = ids[...]
+    weight = weights[...]
+    rows = returned[...]
+    first = dot((expert == here[:, 0:1]).astype(f32).astype(bf16), rows)
+    second = dot((expert == here[:, 1:2]).astype(f32).astype(bf16), rows)
+    moe = weight[:, 0:1] * first + weight[:, 1:2] * second
+    for s in range(out.shape[0] // tp):
+        mine = jnp.where(place[0] == s, 1.0, 0.0)
+        for k in range(tp):
+            columns = slice(k * quarter, (k + 1) * quarter)
+            value = part[s * seqs : (s + 1) * seqs, columns] + mine * moe[:, columns]
+            out[s * tp + k] = value.astype(bf16)
+
+
+def combine(place, part, returned, ids, weights, quarter):
+    seqs = ids.shape[0]
+    whole = pl.BlockSpec(memory_space=pltpu.VMEM)
+    count = part.shape[0] // seqs * (part.shape[1] // quarter)
+    return pl.pallas_call(
+        combine_kernel,
+        out_shape=jax.ShapeDtypeStruct((count, seqs, quarter), bf16),
+        in_specs=[pl.BlockSpec(memory_space=pltpu.SMEM)] + [whole] * 4,
+        out_specs=whole,
+        compiler_params=pltpu.CompilerParams(vmem_limit_bytes=8 << 20),
+        name="combine",
+    )(place[None], part, returned, ids, weights)
 
 
 def layer(
@@ -186,20 +246,19 @@
     experts = lax.axis_size(EP)
     me = lax.axis_index("x")
     place = lax.axis_index(NEAR)
-    slim = dense_gate.shape[1] // tp
 
     sent = pack(tokens, dense_gate.T, dense_up.T, dense_down, dense_mix[None], tp)
     first = exchange(sent, "x")
-    mix_row = first[:, seqs + 3 * slim].reshape(1, -1)
+    mix_row = first[:, seqs + 3 * SLOT].reshape(1, -1)
+
+    route_weight = jax.nn.sigmoid(route_logits - route_logits[:, ::-1])
 
     mix_out = {0: w_mix_out}
     for step in (2, 1, 3):
         mix_out[step] = shifted(w_mix_out, "x", step)
 
-    dense = to_all(first[:, seqs : seqs + 3 * slim].reshape(tp * 3 * slim, quarter), far)
-    dense = exchange(dense, FAR)
-    dense = jnp.transpose(dense.reshape(far, tp, 3, slim, quarter), (2, 0, 3, 1, 4))
-    dense = dense.reshape(3, far * slim, tp * quarter)
+    dense = lax.all_gather(first[:, seqs : seqs + 3 * SLOT].reshape(-1, quarter), FAR)
+    dense = dense.reshape(far, tp, 3 * SLOT, quarter)
 
     mixed = cell(
         first,
@@ -221,8 +280,6 @@
         me, place, second, [mix_out[k] for k in range(tp)], gain_ffn[None], route_ids.T, experts
     )
 
-    flat_ids = route_ids.reshape(-1)
-    picks = (flat_ids[:, None] == jnp.arange(experts, dtype=jnp.int32)[None, :]).astype(bf16)
     outgoing = outgoing.reshape(experts, 4, -1)
     received = exchange(outgoing, EP)
 
@@ -231,22 +288,8 @@
     partial = dot(hidden, expert_down[0]).astype(bf16).reshape(experts, 4, -1)
     returned = exchange(partial, EP)
 
-    transposed = (((1,), (1,)), ((), ()))
-    gate_cols = lax.dot_general(group, dense[0], transposed, preferred_element_type=f32)
-    up_cols = lax.dot_general(group, dense[1], transposed, preferred_element_type=f32)
-    dense_hidden = (jax.nn.silu(gate_cols) * up_cols).astype(bf16)
-    dense_part = dot(dense_hidden, dense[2]).reshape(near, seqs, -1)
-
-    picked = dot(picks, returned.reshape(experts, -1)).reshape(seqs, TOP, -1)
-    route_weight = jax.nn.sigmoid(route_logits - route_logits[:, ::-1])
-    moe = jnp.sum(route_weight[..., None] * picked, axis=1)
-    mix_gate = jax.nn.sigmoid(
-        jnp.sum(group.astype(f32) * mix_row.astype(f32), axis=1, keepdims=True)
-    ).reshape(near, seqs, 1)
-    mine = (jnp.arange(near) == place)[:, None, None]
-    part = mix_gate * dense_part + jnp.where(mine, moe[None], 0.0)
-    part = jnp.swapaxes(part.astype(bf16).reshape(near, seqs, tp, quarter), 1, 2)
-    part = part.reshape(near * tp, seqs, quarter)
+    part = dense_branch(group, dense, mix_row)
+    part = combine(place, part, returned.reshape(experts, -1), route_ids, route_weight, quarter)
     parts = exchange(part, NEAR + ("x",))
     total = own_resid.astype(f32) + parts.astype(f32).sum(axis=0)
     return total.astype(bf16)

time: 137 us -> 130 us (0.949)
  blocking collectives: 11.9 us -> 59.2 us
  starting transfers between devices: 53.6 us -> 21.2 us
  waiting for transfers between devices: 50.9 us -> 19.6 us
  between operations: 0.31 us -> 13.6 us
  local copies, waits for them, and re-layouts: 12.2 us -> 7.48 us
  Pallas kernels: 3.07 us -> 6.12 us
  matrix products: 3.23 us -> 1.22 us
    all_to_all x1 -> x3, blocking collectives: 11.9 us -> 59.2 us  [exchange(): return lax.all_to_all(blocks, axis, 0, 0, tiled=True)]
    all_to_all x5 -> x2, starting transfers between devices: 44.6 us -> 10.5 us  [exchange(): return lax.all_to_all(blocks, axis, 0, 0, tiled=True)]
    all_to_all x5 -> x2, waiting for transfers between devices: 43.4 us -> 14.2 us  [exchange(): return lax.all_to_all(blocks, axis, 0, 0, tiled=True)]
    unnamed x38 -> x25, local copies, waits for them, and re-layouts: 6.31 us -> 3 us
    pallas_call x1, Pallas kernels: 0.9 us -> 3.09 us  [cell(): pl.pallas_call(cell_kernel, out_shape=jax.ShapeDtypeStruct((1, *norm.shap...]
    ppermute x3, waiting for transfers between devices: 7.51 us -> 5.39 us  [shifted(): lax.ppermute(array, axis, [(i, (i + step) % size) for i in range(size)])]
    ppermute x3, starting transfers between devices: 8.97 us -> 10.7 us  [shifted(): lax.ppermute(array, axis, [(i, (i + step) % size) for i in range(size)])]
    dot_general x4 -> x2, matrix products: 2.77 us -> 1.22 us  [dot(): return jnp.dot(a, b, preferred_element_type=f32)]
  transfers between devices with their start and end apart: 8 -> 6, of which waited for: 7 -> 3; matrix products, arithmetic and copies ran while one was open for 2% -> 5% of each run, Pallas kernels for 0% -> 3%
where the time goes in v6:
time: 130 us
  blocking collectives  59.2 us (46%)
  starting transfers between devices  21.2 us (16%)
  waiting for transfers between devices  19.6 us (15%)
  between operations  13.6 us (10%)
  local copies, waits for them, and re-layouts  7.48 us (6%)
  Pallas kernels  6.12 us (5%)
  other arithmetic  1.31 us (1%)
    all_to_all x3, blocking collectives, exchange(): return lax.all_to_all(blocks, axis, 0, 0, tiled=True)  59.2 us
    all_to_all x2, waiting for transfers between devices, exchange(): return lax.all_to_all(blocks, axis, 0, 0, tiled=True)  14.2 us
    ppermute x3, starting transfers between devices, shifted(): lax.ppermute(array, axis, [(i, (i + step) % size) for i in range(size)])  10.7 us
    all_to_all x2, starting transfers between devices, exchange(): return lax.all_to_all(blocks, axis, 0, 0, tiled=True)  10.5 us
    ppermute x3, waiting for transfers between devices, shifted(): lax.ppermute(array, axis, [(i, (i + step) % size) for i in range(size)])  5.39 us
    pallas_call x1, Pallas kernels, cell(): pl.pallas_call(cell_kernel, out_shape=jax.ShapeDtypeStruct((1, *norm.shap...  3.09 us
    unnamed x25, local copies, waits for them, and re-layouts  3 us
  transfers between devices with their start and end apart: 6, of which 3 were waited for; matrix products, arithmetic and copies ran while one was open for 5% of the time, Pallas kernels for 3%

profile of v6, /device:TPU:1, one launch (start us, length us, event | category | flops | bytes accessed | tf_op | source)
XLA Modules:
  0.0 129.8 jit_solution(12721368857561745583)
XLA Ops:
  6.5 0.0 copy-start
  6.5 0.0 copy-start.8
  6.5 0.0 all-gather.2.cloned.1.call-start
  6.5 1.3 %broadcast_in_dim.24.mix = bf16[1,256]{1,0:T(2,128)(2,1)} reshape(bf16[256]{0:T(256)(128)(2,1)} %param.43) | data formatting | bytes 1024 | tf_op jit(solution)/shard_map/broadcast_in_dim | solution.py:250
  7.8 1.6 %pack.1 = bf16[4,48,256]{2,1,0:T(8,128)(2,1)} custom-call(bf16[16,256]{1,0:T(8,128)(2,1)} %tokens.1, bf16[24,256]{1,0:T(8,128)(2,1)} %bitcast.45, bf16[24,256]{1,0:T(8,128)(2,1)} %bitcast.46, bf16[24,256]{1,0:T(8,128)(2,1)} %down.1, bf16[1,256]{1,0:T(2,128)(2,1)} %broadcast_in_dim.24.mix), custom_call_target="tpu_custom_call" | custom-call | tf_op jit(solution)/shard_map/pack/pallas_call | solution.py:61
  9.4 0.0 copy-start.2
  9.4 9.6 %all_to_all.25.first = bf16[4,48,256]{2,1,0:T(8,128)(2,1)S(1)} all-to-all(bf16[4,48,256]{2,1,0:T(8,128)(2,1)} %pack.1), channel_id=1, replica_groups=mesh['zh'=4,'zl'=2,'yh'=4,'yl'=2,'c'=2,'x'=4] {'x'}, dimensions={0} | all-to-all | bytes 196608 | tf_op jit(solution)/shard_map/all_to_all | solution.py:21
  19.0 0.0 copy-start.7
  19.0 0.0 copy-start.3
  19.0 0.0 copy-start.4
  19.0 0.6 slice.8
  19.6 0.0 all-gather.2.cloned.1.call-update
  19.7 1.3 %copy.31.peak = f32[16,1]{1,0:T(8,128)} copy(f32[16,1]{0,1:T(1,128)} %param.33) | data formatting | bytes 128 | tf_op args[11]
  21.0 0.0 copy-done.7
  21.0 3.1 %cell.1 = bf16[1,16,128]{2,1,0:T(8,128)(2,1)} custom-call(bf16[4,48,256]{2,1,0:T(8,128)(2,1)} %copy-done.7, f32[1,1024]{1,0:T(1,128)} %bitcast.48, bf16[1024,128]{1,0:T(8,128)(2,1)} %wq.1, bf16[1024,128]{1,0:T(8,128)(2,1)} %wk.1, bf16[1024,128]{1,0:T(8,128)(2,1)} %wv.1, bf16[1024,128]{1,0:T(8,128)(2,1)} %wo.1, bf16[1,1024]{1,0:T(2,128)(2,1)} %bitcast.49, ...), custom_call_target="tpu_custom_call" | custom-call | flops 40000000 | bytes 2200000 | tf_op jit(solution)/shard_map/cell/pallas_call | solution.py:96
  24.1 0.0 copy-done.8
  24.1 0.7 pad_maximum_fusion
  24.8 0.7 broadcast_in_dim.26
  25.5 0.0 copy-start.5
  25.5 5.2 %all-to-all-start.1 = ((bf16[16,16,384]{2,1,0:T(8,128)(2,1)}), bf16[16,16,384]{2,1,0:T(8,128)(2,1)S(1)}, u32[]{:S(2)}, u32[]{:S(2)}) async-start(bf16[16,16,384]{2,1,0:T(8,128)(2,1)} %broadcast_in_dim.26), calls=%async_computation.1 | async-start | bytes 393216 | tf_op jit(solution)/shard_map/all_to_all | solution.py:21
  30.7 0.0 copy-done.2
  30.7 3.3 %collective-permute-start = (bf16[512,256]{1,0:T(8,128)(2,1)S(1)}, bf16[512,256]{1,0:T(8,128)(2,1)S(1)}, u32[]{:S(2)}, u32[]{:S(2)}) collective-permute-start(bf16[512,256]{1,0:T(8,128)(2,1)S(1)} %copy-done.2), channel_id=1, source_target_pairs={{0,1},{1,2},{2,3},{3,0},{4,5},{5,6},{6,7},{7,4},{8,9},{9,10},{10,1... | collective-permute-start | bytes 786440 | tf_op jit(solution)/shard_map/ppermute | solution.py:38
  34.0 4.3 %collective-permute-start.1 = (bf16[512,256]{1,0:T(8,128)(2,1)S(1)}, bf16[512,256]{1,0:T(8,128)(2,1)S(1)}, u32[]{:S(2)}, u32[]{:S(2)}) collective-permute-start(bf16[512,256]{1,0:T(8,128)(2,1)S(1)} %copy-done.2), channel_id=1, source_target_pairs={{0,2},{1,3},{2,0},{3,1},{4,6},{5,7},{6,4},{7,5},{8,10},{9,11},{10,... | collective-permute-start | bytes 786440 | tf_op jit(solution)/shard_map/ppermute | solution.py:38
  38.3 3.1 %collective-permute-start.2 = (bf16[512,256]{1,0:T(8,128)(2,1)S(1)}, bf16[512,256]{1,0:T(8,128)(2,1)S(1)}, u32[]{:S(2)}, u32[]{:S(2)}) collective-permute-start(bf16[512,256]{1,0:T(8,128)(2,1)S(1)} %copy-done.2), channel_id=1, source_target_pairs={{0,3},{1,0},{2,1},{3,2},{4,7},{5,4},{6,5},{7,6},{8,11},{9,8},{10,9... | collective-permute-start | bytes 786440 | tf_op jit(solution)/shard_map/ppermute | solution.py:38
  41.4 0.0 collective-permute-done.w1
  41.4 3.9 %collective-permute-done.1.w2 = bf16[512,256]{1,0:T(8,128)(2,1)S(1)} collective-permute-done((bf16[512,256]{1,0:T(8,128)(2,1)S(1)}, bf16[512,256]{1,0:T(8,128)(2,1)S(1)}, u32[]{:S(2)}, u32[]{:S(2)}) %collective-permute-start.1) | collective-permute-done | bytes 262176 | tf_op jit(solution)/shard_map/ppermute | solution.py:38
  45.4 1.4 %collective-permute-done.2.w3 = bf16[512,256]{1,0:T(8,128)(2,1)S(1)} collective-permute-done((bf16[512,256]{1,0:T(8,128)(2,1)S(1)}, bf16[512,256]{1,0:T(8,128)(2,1)S(1)}, u32[]{:S(2)}, u32[]{:S(2)}) %collective-permute-start.2) | collective-permute-done | bytes 262176 | tf_op jit(solution)/shard_map/ppermute | solution.py:38
  46.8 0.0 all-to-all-done.1
  46.8 0.0 copy-done.3
  46.8 0.0 copy-done.4
  46.8 0.6 residual.1
  47.4 0.0 copy-start.6
  47.4 0.2 reshape.21
  47.6 38.7 %all_to_all.26 = bf16[128,4,256]{2,1,0:T(4,128)(2,1)S(1)} all-to-all(bf16[128,4,256]{2,1,0:T(4,128)(2,1)S(1)} %reshape.21), channel_id=1, replica_groups=mesh['zh'=4,'zl'=2,'yh'=4,'yl'=2,'c'=2,'x'=4] {'zh','zl','yh','yl','c'}, dimensions={0} | all-to-all | bytes 524288 | tf_op jit(solution)/shard_map/all_to_all | solution.py:21
  86.4 0.0 copy-done.5
  86.4 0.4 fusion.4
  86.8 0.0 copy-done
  86.8 0.0 copy-done.6
  86.8 0.0 copy-start.9
  86.8 0.9 convolution_convert_fusion
  87.7 0.9 reshape.23
  88.5 5.3 %all-to-all-start.3 = ((bf16[128,4,256]{2,1,0:T(4,128)(2,1)}), bf16[128,4,256]{2,1,0:T(4,128)(2,1)S(1)}, u32[]{:S(2)}, u32[]{:S(2)}) async-start(bf16[128,4,256]{2,1,0:T(4,128)(2,1)} %reshape.23), calls=%async_computation.3 | async-start | bytes 524288 | tf_op jit(solution)/shard_map/all_to_all | solution.py:21
  93.8 0.1 copy.36.ids
  93.9 0.0 copy-done.9
  93.9 0.1 copy.33
  94.0 0.1 rev.3
  94.1 0.7 slice.9
  94.8 14.2 %all-to-all-done.3 = bf16[128,4,256]{2,1,0:T(4,128)(2,1)S(1)} async-done(((bf16[128,4,256]{2,1,0:T(4,128)(2,1)}), bf16[128,4,256]{2,1,0:T(4,128)(2,1)S(1)}, u32[]{:S(2)}, u32[]{:S(2)}) %all-to-all-start.3) | async-done | bytes 262176 | tf_op jit(solution)/shard_map/all_to_all | solution.py:21
  109.1 0.0 all-gather.2.cloned.1.call-done
  109.1 0.0 copy-start.1
  109.1 1.4 %copy-done.1 = bf16[32,96,256]{2,1,0:T(8,128)(2,1)S(1)} copy-done((bf16[32,96,256]{2,1,0:T(8,128)(2,1)S(1)}, bf16[32,96,256]{2,1,0:T(8,128)(2,1)}, u32[]{:S(2)}) %copy-start.1) | copy-done | bytes 1572888
  110.5 0.6 dense.1.part
  111.1 0.3 combine.1
  111.4 10.9 %all_to_all.27 = bf16[16,16,256]{2,1,0:T(8,128)(2,1)S(1)} all-to-all(bf16[16,16,256]{2,1,0:T(8,128)(2,1)S(1)} %combine.1), channel_id=1, replica_groups=mesh['zh'=4,'zl'=2,'yh'=4,'yl'=2,'c'=2,'x'=4] {'zl','yl','x'}, dimensions={0} | all-to-all | bytes 262144 | tf_op jit(solution)/shard_map/all_to_all | solution.py:21
  122.3 0.6 add_convert_fusion
  (4 shorter events, 0.1 us)
Async XLA Ops:
  6.5 80.2 %copy-start = (bf16[1,352,1024]{2,1,0:T(8,128)(2,1)S(1)}, bf16[1,352,1024]{2,1,0:T(8,128)(2,1)}, u32[]{:S(2)}) copy-start(bf16[1,352,1024]{2,1,0:T(8,128)(2,1)} %param.39) | copy-start | bytes 2162692
  6.5 17.6 %copy-start.8 = (bf16[16,256]{1,0:T(8,128)(2,1)S(1)}, bf16[16,256]{1,0:T(8,128)(2,1)}, u32[]{:S(2)}) copy-start(bf16[16,256]{1,0:T(8,128)(2,1)} %tokens.1) | copy-start | bytes 24580
  6.5 102.6 %all-gather.2.cloned.1.call-start = ((), (), s32[]{:S(2)}) async-start(), calls=%async_computation.5 | async-start | bytes 1622016 | tf_op jit(solution)/shard_map/all_gather | solution.py:260
  9.4 21.3 %copy-start.2 = (bf16[512,256]{1,0:T(8,128)(2,1)S(1)}, bf16[512,256]{1,0:T(8,128)(2,1)}, u32[]{:S(2)}) copy-start(bf16[512,256]{1,0:T(8,128)(2,1)} %w0.1) | copy-start | bytes 786436
  19.0 2.0 %copy-start.7 = (bf16[4,48,256]{2,1,0:T(8,128)(2,1)}, bf16[4,48,256]{2,1,0:T(8,128)(2,1)S(1)}, u32[]{:S(2)}) copy-start(bf16[4,48,256]{2,1,0:T(8,128)(2,1)S(1)} %all_to_all.25.first) | copy-start | bytes 294916
  19.0 27.8 %copy-start.3 = (f32[1024]{0:T(1024)S(1)}, f32[1024]{0:T(1024)}, u32[]{:S(2)}) copy-start(f32[1024]{0:T(1024)} %param.34) | copy-start | bytes 12292
  19.0 27.8 %copy-start.4 = (s32[16,2]{0,1:T(2,128)S(1)}, s32[16,2]{0,1:T(2,128)}, u32[]{:S(2)}) copy-start(s32[16,2]{0,1:T(2,128)} %param.35) | copy-start | bytes 388
  25.5 60.9 %copy-start.5 = (bf16[1,1024,352]{1,2,0:T(8,128)(2,1)S(1)}, bf16[1,1024,352]{1,2,0:T(8,128)(2,1)}, u32[]{:S(2)}) copy-start(bf16[1,1024,352]{1,2,0:T(8,128)(2,1)} %param.37) | copy-start | bytes 2162692
  25.5 21.3 %all-to-all-start.1 = ((bf16[16,16,384]{2,1,0:T(8,128)(2,1)}), bf16[16,16,384]{2,1,0:T(8,128)(2,1)S(1)}, u32[]{:S(2)}, u32[]{:S(2)}) async-start(bf16[16,16,384]{2,1,0:T(8,128)(2,1)} %broadcast_in_dim.26), calls=%async_computation.1 | async-start | bytes 393216 | tf_op jit(solution)/shard_map/all_to_all | solution.py:21
  30.7 10.7 %collective-permute-start = (bf16[512,256]{1,0:T(8,128)(2,1)S(1)}, bf16[512,256]{1,0:T(8,128)(2,1)S(1)}, u32[]{:S(2)}, u32[]{:S(2)}) collective-permute-start(bf16[512,256]{1,0:T(8,128)(2,1)S(1)} %copy-done.2), channel_id=1, source_target_pairs={{0,1},{1,2},{2,3},{3,0},{4,5},{5,6},{6,7},{7,4},{8,9},{9,10},{10,1... | collective-permute-start | bytes 786440 | tf_op jit(solution)/shard_map/ppermute | solution.py:38
  34.0 11.4 %collective-permute-start.1 = (bf16[512,256]{1,0:T(8,128)(2,1)S(1)}, bf16[512,256]{1,0:T(8,128)(2,1)S(1)}, u32[]{:S(2)}, u32[]{:S(2)}) collective-permute-start(bf16[512,256]{1,0:T(8,128)(2,1)S(1)} %copy-done.2), channel_id=1, source_target_pairs={{0,2},{1,3},{2,0},{3,1},{4,6},{5,7},{6,4},{7,5},{8,10},{9,11},{10,... | collective-permute-start | bytes 786440 | tf_op jit(solution)/shard_map/ppermute | solution.py:38
  38.3 8.5 %collective-permute-start.2 = (bf16[512,256]{1,0:T(8,128)(2,1)S(1)}, bf16[512,256]{1,0:T(8,128)(2,1)S(1)}, u32[]{:S(2)}, u32[]{:S(2)}) collective-permute-start(bf16[512,256]{1,0:T(8,128)(2,1)S(1)} %copy-done.2), channel_id=1, source_target_pairs={{0,3},{1,0},{2,1},{3,2},{4,7},{5,4},{6,5},{7,6},{8,11},{9,8},{10,9... | collective-permute-start | bytes 786440 | tf_op jit(solution)/shard_map/ppermute | solution.py:38
  47.4 39.3 %copy-start.6 = (bf16[1,1024,352]{1,2,0:T(8,128)(2,1)S(1)}, bf16[1,1024,352]{1,2,0:T(8,128)(2,1)}, u32[]{:S(2)}) copy-start(bf16[1,1024,352]{1,2,0:T(8,128)(2,1)} %param.38) | copy-start | bytes 2162692
  86.8 7.2 %copy-start.9 = (f32[16,2]{0,1:T(2,128)S(1)}, f32[16,2]{0,1:T(2,128)}, u32[]{:S(2)}) copy-start(f32[16,2]{0,1:T(2,128)} %param.36) | copy-start | bytes 388
  88.5 20.5 %all-to-all-start.3 = ((bf16[128,4,256]{2,1,0:T(4,128)(2,1)}), bf16[128,4,256]{2,1,0:T(4,128)(2,1)S(1)}, u32[]{:S(2)}, u32[]{:S(2)}) async-start(bf16[128,4,256]{2,1,0:T(4,128)(2,1)} %reshape.23), calls=%async_computation.3 | async-start | bytes 524288 | tf_op jit(solution)/shard_map/all_to_all | solution.py:21
  109.1 1.4 %copy-start.1 = (bf16[32,96,256]{2,1,0:T(8,128)(2,1)S(1)}, bf16[32,96,256]{2,1,0:T(8,128)(2,1)}, u32[]{:S(2)}) copy-start(bf16[32,96,256]{2,1,0:T(8,128)(2,1)} %all-gather.2.cloned.1.call-done) | copy-start | bytes 4718596
Sparse Core Ops, SparseCore 0:
  19.8 68.8 all-gather.1

commit v7 on v6

--- a/solution.py
+++ b/solution.py
@@ -21,10 +21,6 @@
     return lax.all_to_all(blocks, axis, 0, 0, tiled=True)
 
 
-def to_all(shard, size):
-    return jnp.broadcast_to(shard[None], (size, *shard.shape))
-
-
 def dot(a, b):
     return jnp.dot(a, b, preferred_element_type=f32)
 
@@ -36,6 +32,13 @@
 def shifted(array, axis, step):
     size = lax.axis_size(axis)
     return lax.ppermute(array, axis, [(i, (i + step) % size) for i in range(size)])
+
+
+def upright(row):
+    count = row.shape[1]
+    square = (count, count)
+    same = lax.broadcasted_iota(jnp.int32, square, 0) == lax.broadcasted_iota(jnp.int32, square, 1)
+    return jnp.sum(jnp.where(same, jnp.broadcast_to(row, square), 0.0), axis=1, keepdims=True)
 
 
 def pack_kernel(tokens, gate, up, down, mix, out):
@@ -49,7 +52,7 @@
     slot = row & (SLOT - 1)
     wanted = slot + lax.div(row, SLOT) * columns
     last = lax.broadcasted_iota(jnp.int32, (room, quarter), 0) == 3 * SLOT
-    extra = jnp.where(last, jnp.broadcast_to(mix[...].astype(f32), (room, quarter)), 0.0)
+    extra = jnp.where(last, jnp.broadcast_to(mix[...].astype(f32)[None], (room, quarter)), 0.0)
     for k in range(count):
         pick = (column == wanted + k * slim) & (slot < slim) & (row < 3 * SLOT)
         out[k, :seqs] = tokens[...]
@@ -65,7 +68,7 @@
     )(tokens, gate, up, down, mix)
 
 
-def cell_kernel(first, gain, wq, wk, wv, wo, wi, wf, state, norm, peak, out):
+def cell_kernel(first, gain, wq, wk, wv, wo, wi, wf, state, norm, peak, tokens, out):
     seqs = norm.shape[0]
     values = jnp.concatenate([first[k, :seqs] for k in range(first.shape[0])], axis=1).astype(f32)
     scale = lax.rsqrt(jnp.mean(values * values, axis=1, keepdims=True) + epsilon)
@@ -77,7 +80,7 @@
     wide = rows.astype(f32)
     enter = jnp.sum(wide * wi[...].astype(f32), axis=1, keepdims=True)
     forget = jnp.sum(wide * wf[...].astype(f32), axis=1, keepdims=True)
-    carried = jnp.minimum(forget, 0.0) - jnp.log1p(jnp.exp(-jnp.abs(forget))) + peak[...]
+    carried = jnp.minimum(forget, 0.0) - jnp.log1p(jnp.exp(-jnp.abs(forget))) + upright(peak[...])
     stabilizer = jnp.maximum(carried, enter)
     old = jnp.exp(carried - stabilizer)
     new = jnp.exp(enter - stabilizer) * jnp.sum(query * key, axis=1, keepdims=True)
@@ -88,17 +91,19 @@
     numerator = old * jnp.concatenate(read, axis=0) + new * value
     denominator = old * jnp.sum(query * norm[...], axis=1, keepdims=True) + new
     mixed = gate * (numerator / jnp.maximum(jnp.abs(denominator), 1.0))
+    mixed = mixed.astype(bf16)
     for k in range(out.shape[0]):
-        out[k] = mixed.astype(bf16)
-
-
-def cell(first, gain, wq, wk, wv, wo, wi, wf, state, norm, peak):
+        out[k, :, :HEAD] = mixed
+        out[k, :, HEAD:] = tokens[...]
+
+
+def cell(first, gain, wq, wk, wv, wo, wi, wf, state, norm, peak, tokens, count):
     return pl.pallas_call(
         cell_kernel,
-        out_shape=jax.ShapeDtypeStruct((1, *norm.shape), bf16),
+        out_shape=jax.ShapeDtypeStruct((count, norm.shape[0], HEAD + tokens.shape[1]), bf16),
         cost_estimate=pl.CostEstimate(flops=40000000, bytes_accessed=2200000, transcendentals=9000),
         name="cell",
-    )(first, gain, wq, wk, wv, wo, wi, wf, state, norm, peak)
+    )(first, gain, wq, wk, wv, wo, wi, wf, state, norm, peak, tokens)
 
 
 def residual_kernel(me, place, second, w0, w1, w2, w3, gain, ids, group, outgoing, own, resid):
@@ -129,7 +134,9 @@
     experts = outgoing.shape[0]
     expert = lax.broadcasted_iota(jnp.int32, (experts, seqs), 0)
     chosen = ((expert == ids[0:1, :]) | (expert == ids[1:2, :])).astype(f32).astype(bf16)
-    outgoing[...] = dot(chosen, group[pl.ds(start, seqs), :]).astype(bf16)
+    rows = dot(chosen, group[pl.ds(start, seqs), :])
+    for k in range(tp):
+        outgoing[:, k, :] = rows[:, k * quarter : (k + 1) * quarter].astype(bf16)
 
 
 def residual(me, place, second, weights, gain, ids, experts):
@@ -141,7 +148,7 @@
         residual_kernel,
         out_shape=(
             jax.ShapeDtypeStruct((near * seqs, tp * quarter), bf16),
-            jax.ShapeDtypeStruct((experts, tp * quarter), bf16),
+            jax.ShapeDtypeStruct((experts, tp, quarter), bf16),
             jax.ShapeDtypeStruct((seqs, quarter), bf16),
         ),
         in_specs=[scalar, scalar] + [whole] * 7,
@@ -182,17 +189,36 @@
     )(group, weights, mix)
 
 
+def expert_kernel(rows, gate, up, down, out):
+    parts, width = rows.shape[1:]
+    here = jnp.concatenate([rows[:, k, :] for k in range(parts)], axis=1)
+    opened = dot_turned(here, gate[...])
+    hidden = opened * jax.nn.sigmoid(opened) * dot_turned(here, up[...])
+    result = dot(hidden.astype(bf16), down[...]).astype(bf16)
+    for k in range(parts):
+        out[:, k, :] = result[:, k * width : (k + 1) * width]
+
+
+def expert(rows, gate, up, down):
+    return pl.pallas_call(
+        expert_kernel,
+        out_shape=jax.ShapeDtypeStruct(rows.shape, bf16),
+        compiler_params=pltpu.CompilerParams(vmem_limit_bytes=12 << 20),
+        cost_estimate=pl.CostEstimate(flops=277000000, bytes_accessed=2700000, transcendentals=45000),
+        name="expert",
+    )(rows, gate, up, down)
+
+
 def combine_kernel(place, part, returned, ids, weights, out):
     seqs, quarter = out.shape[1:]
-    experts = returned.shape[0]
-    tp = returned.shape[1] // quarter
+    experts, tp, _ = returned.shape
     expert = lax.broadcasted_iota(jnp.int32, (seqs, experts), 1)
     here = ids[...]
-    weight = weights[...]
-    rows = returned[...]
+    ahead, behind = upright(weights[0:1]), upright(weights[1:2])
+    rows = jnp.concatenate([returned[:, k, :] for k in range(tp)], axis=1)
     first = dot((expert == here[:, 0:1]).astype(f32).astype(bf16), rows)
     second = dot((expert == here[:, 1:2]).astype(f32).astype(bf16), rows)
-    moe = weight[:, 0:1] * first + weight[:, 1:2] * second
+    moe = ahead * first + behind * second
     for s in range(out.shape[0] // tp):
         mine = jnp.where(place[0] == s, 1.0, 0.0)
         for k in range(tp):
@@ -247,11 +273,12 @@
     me = lax.axis_index("x")
     place = lax.axis_index(NEAR)
 
-    sent = pack(tokens, dense_gate.T, dense_up.T, dense_down, dense_mix[None], tp)
+    sent = pack(tokens, dense_gate.T, dense_up.T, dense_down, dense_mix, tp)
     first = exchange(sent, "x")
     mix_row = first[:, seqs + 3 * SLOT].reshape(1, -1)
 
-    route_weight = jax.nn.sigmoid(route_logits - route_logits[:, ::-1])
+    turned_logits = route_logits.T
+    route_weight = jax.nn.sigmoid(turned_logits - turned_logits[::-1])
 
     mix_out = {0: w_mix_out}
     for step in (2, 1, 3):
@@ -260,7 +287,7 @@
     dense = lax.all_gather(first[:, seqs : seqs + 3 * SLOT].reshape(-1, quarter), FAR)
     dense = dense.reshape(far, tp, 3 * SLOT, quarter)
 
-    mixed = cell(
+    sent = cell(
         first,
         gain_mix[None],
         w_query,
@@ -271,25 +298,23 @@
         w_forget_gate.T,
         cell_state[:, 0],
         norm_state[:, 0],
-        max_state,
-    )[0]
-    sent = to_all(jnp.concatenate([mixed, tokens], axis=1), near * tp)
+        max_state.T,
+        tokens,
+        near * tp,
+    )
     second = exchange(sent, NEAR + ("x",))
     second = second.reshape(near, tp, seqs, HEAD + quarter)
     group, outgoing, own_resid = residual(
         me, place, second, [mix_out[k] for k in range(tp)], gain_ffn[None], route_ids.T, experts
     )
 
-    outgoing = outgoing.reshape(experts, 4, -1)
     received = exchange(outgoing, EP)
 
-    rows = received.reshape(experts, -1)
-    hidden = (jax.nn.silu(dot(rows, expert_gate[0])) * dot(rows, expert_up[0])).astype(bf16)
-    partial = dot(hidden, expert_down[0]).astype(bf16).reshape(experts, 4, -1)
+    partial = expert(received, expert_gate[0].T, expert_up[0].T, expert_down[0])
     returned = exchange(partial, EP)
 
     part = dense_branch(group, dense, mix_row)
-    part = combine(place, part, returned.reshape(experts, -1), route_ids, route_weight, quarter)
+    part = combine(place, part, returned, route_ids, route_weight, quarter)
     parts = exchange(part, NEAR + ("x",))
     total = own_resid.astype(f32) + parts.astype(f32).sum(axis=0)
     return total.astype(bf16)

time: 130 us -> 124 us (0.954)
  local copies, waits for them, and re-layouts: 7.48 us -> 2.96 us
  Pallas kernels: 6.12 us -> 8.88 us
  waiting for transfers between devices: 19.6 us -> 17.9 us
    pallas_call x1 -> x2, Pallas kernels: 3.09 us -> 5.25 us  [the longest x1 3.15 us: cell(): pl.pallas_call(cell_kernel, out_shape=jax.ShapeDtypeStruct((count, norm.s...]
    broadcast_in_dim x2 -> x0, local copies, waits for them, and re-layouts: 2.01 us -> none  [the longest x1 1.3 us: layer(): dense_mix[None]]
    all_to_all x2, waiting for transfers between devices: 14.2 us -> 12.3 us  [exchange(): return lax.all_to_all(blocks, axis, 0, 0, tiled=True)]
    unnamed x25 -> x19, local copies, waits for them, and re-layouts: 3 us -> 1.52 us
  transfers between devices with their start and end apart: 6 -> 6, of which waited for: 3 -> 3; matrix products, arithmetic and copies ran while one was open for 5% -> 1% of each run, Pallas kernels for 3% -> 5%
where the time goes in v7:
time: 124 us
  blocking collectives  58 us (47%)
  starting transfers between devices  21.9 us (18%)
  waiting for transfers between devices  17.9 us (14%)
  between operations  13.5 us (11%)
  Pallas kernels  8.88 us (7%)
  local copies, waits for them, and re-layouts  2.96 us (2%)
    all_to_all x3, blocking collectives, exchange(): return lax.all_to_all(blocks, axis, 0, 0, tiled=True)  58 us
    all_to_all x2, waiting for transfers between devices, exchange(): return lax.all_to_all(blocks, axis, 0, 0, tiled=True)  12.3 us
    all_to_all x2, starting transfers between devices, exchange(): return lax.all_to_all(blocks, axis, 0, 0, tiled=True)  11.2 us
    ppermute x3, starting transfers between devices, shifted(): lax.ppermute(array, axis, [(i, (i + step) % size) for i in range(size)])  10.7 us
    ppermute x3, waiting for transfers between devices, shifted(): lax.ppermute(array, axis, [(i, (i + step) % size) for i in range(size)])  5.49 us
    pallas_call x1, Pallas kernels, cell(): pl.pallas_call(cell_kernel, out_shape=jax.ShapeDtypeStruct((count, norm.s...  3.15 us
  transfers between devices with their start and end apart: 6, of which 3 were waited for; matrix products, arithmetic and copies ran while one was open for 1% of the time, Pallas kernels for 5%

profile of v7, /device:TPU:1, one launch (start us, length us, event | category | flops | bytes accessed | tf_op | source)
XLA Modules:
  0.0 123.7 jit_solution(13107719306089340155)
XLA Ops:
  6.5 0.0 all-gather.2.cloned.1.call-start
  6.5 1.6 %pack.1 = bf16[4,48,256]{2,1,0:T(8,128)(2,1)} custom-call(bf16[16,256]{1,0:T(8,128)(2,1)} %tokens.3, bf16[24,256]{1,0:T(8,128)(2,1)} %bitcast.35, bf16[24,256]{1,0:T(8,128)(2,1)} %bitcast.36, bf16[24,256]{1,0:T(8,128)(2,1)} %down.1, bf16[256]{0:T(256)(128)(2,1)} %mix.1), custom_call_target="tpu_custom_call" | custom-call | tf_op jit(solution)/shard_map/pack/pallas_call | solution.py:64
  8.1 0.0 copy-start.4
  8.1 0.0 copy-start.5
  8.1 0.0 copy-start.6
  8.1 9.6 %all_to_all.25.first = bf16[4,48,256]{2,1,0:T(8,128)(2,1)S(1)} all-to-all(bf16[4,48,256]{2,1,0:T(8,128)(2,1)} %pack.1), channel_id=1, replica_groups=mesh['zh'=4,'zl'=2,'yh'=4,'yl'=2,'c'=2,'x'=4] {'x'}, dimensions={0} | all-to-all | bytes 196608 | tf_op jit(solution)/shard_map/all_to_all | solution.py:21
  17.7 0.0 copy-start.7
  17.7 0.7 slice.8
  18.4 0.0 all-gather.2.cloned.1.call-update
  18.4 0.0 copy-done.7
  18.4 3.2 %cell.1 = bf16[16,16,384]{2,1,0:T(8,128)(2,1)} custom-call(bf16[4,48,256]{2,1,0:T(8,128)(2,1)} %copy-done.7, f32[1,1024]{1,0:T(1,128)} %bitcast.38, bf16[1024,128]{1,0:T(8,128)(2,1)} %wq.1, bf16[1024,128]{1,0:T(8,128)(2,1)} %wk.1, bf16[1024,128]{1,0:T(8,128)(2,1)} %wv.1, bf16[1024,128]{1,0:T(8,128)(2,1)} %wo.1, bf16[1,1024]{1,0:T(2,128)(2,1)} %bitcast.39, ...), custom_call_target="tpu_custom_call" | custom-call | flops 40000000 | bytes 2200000 | tf_op jit(solution)/shard_map/cell/pallas_call | solution.py:101
  21.6 0.0 copy-start.1
  21.6 0.0 copy-start.2
  21.6 0.0 copy-start.3
  21.6 5.2 %all-to-all-start.1 = ((bf16[16,16,384]{2,1,0:T(8,128)(2,1)}), bf16[16,16,384]{2,1,0:T(8,128)(2,1)S(1)}, u32[]{:S(2)}, u32[]{:S(2)}) async-start(bf16[16,16,384]{2,1,0:T(8,128)(2,1)} %cell.1), calls=%async_computation.1 | async-start | bytes 393216 | tf_op jit(solution)/shard_map/all_to_all | solution.py:21
  26.8 0.0 copy-done.4
  26.9 3.3 %collective-permute-start = (bf16[512,256]{1,0:T(8,128)(2,1)S(1)}, bf16[512,256]{1,0:T(8,128)(2,1)S(1)}, u32[]{:S(2)}, u32[]{:S(2)}) collective-permute-start(bf16[512,256]{1,0:T(8,128)(2,1)S(1)} %copy-done.4), channel_id=1, source_target_pairs={{0,1},{1,2},{2,3},{3,0},{4,5},{5,6},{6,7},{7,4},{8,9},{9,10},{10,1... | collective-permute-start | bytes 786440 | tf_op jit(solution)/shard_map/ppermute | solution.py:34
  30.1 4.3 %collective-permute-start.1 = (bf16[512,256]{1,0:T(8,128)(2,1)S(1)}, bf16[512,256]{1,0:T(8,128)(2,1)S(1)}, u32[]{:S(2)}, u32[]{:S(2)}) collective-permute-start(bf16[512,256]{1,0:T(8,128)(2,1)S(1)} %copy-done.4), channel_id=1, source_target_pairs={{0,2},{1,3},{2,0},{3,1},{4,6},{5,7},{6,4},{7,5},{8,10},{9,11},{10,... | collective-permute-start | bytes 786440 | tf_op jit(solution)/shard_map/ppermute | solution.py:34
  34.4 3.1 %collective-permute-start.2 = (bf16[512,256]{1,0:T(8,128)(2,1)S(1)}, bf16[512,256]{1,0:T(8,128)(2,1)S(1)}, u32[]{:S(2)}, u32[]{:S(2)}) collective-permute-start(bf16[512,256]{1,0:T(8,128)(2,1)S(1)} %copy-done.4), channel_id=1, source_target_pairs={{0,3},{1,0},{2,1},{3,2},{4,7},{5,4},{6,5},{7,6},{8,11},{9,8},{10,9... | collective-permute-start | bytes 786440 | tf_op jit(solution)/shard_map/ppermute | solution.py:34
  37.6 0.0 collective-permute-done.w1
  37.6 3.9 %collective-permute-done.1.w2 = bf16[512,256]{1,0:T(8,128)(2,1)S(1)} collective-permute-done((bf16[512,256]{1,0:T(8,128)(2,1)S(1)}, bf16[512,256]{1,0:T(8,128)(2,1)S(1)}, u32[]{:S(2)}, u32[]{:S(2)}) %collective-permute-start.1) | collective-permute-done | bytes 262176 | tf_op jit(solution)/shard_map/ppermute | solution.py:34
  41.5 1.6 %collective-permute-done.2.w3 = bf16[512,256]{1,0:T(8,128)(2,1)S(1)} collective-permute-done((bf16[512,256]{1,0:T(8,128)(2,1)S(1)}, bf16[512,256]{1,0:T(8,128)(2,1)S(1)}, u32[]{:S(2)}, u32[]{:S(2)}) %collective-permute-start.2) | collective-permute-done | bytes 262176 | tf_op jit(solution)/shard_map/ppermute | solution.py:34
  43.1 0.0 all-to-all-done.1
  43.1 0.0 copy-done.5
  43.1 0.0 copy-done.6
  43.1 0.9 residual.1
  43.9 37.9 %all_to_all.26.rows = bf16[128,4,256]{2,1,0:T(4,128)(2,1)S(1)} all-to-all(bf16[128,4,256]{2,1,0:T(4,128)(2,1)S(1)} %get-tuple-element.10), channel_id=1, replica_groups=mesh['zh'=4,'zl'=2,'yh'=4,'yl'=2,'c'=2,'x'=4] {'zh','zl','yh','yl','c'}, dimensions={0} | all-to-all | bytes 524288 | tf_op jit(solution)/shard_map/all_to_all | solution.py:21
  81.8 0.0 copy-done.1
  81.8 0.0 copy-done.2
  81.8 0.0 copy-done.3
  81.8 0.0 copy-start.8
  81.8 2.1 %expert.1 = bf16[128,4,256]{2,1,0:T(4,128)(2,1)} custom-call(bf16[128,4,256]{2,1,0:T(4,128)(2,1)S(1)} %all_to_all.26.rows, bf16[352,1024]{1,0:T(8,128)(2,1)S(1)} %bitcast.27, bf16[352,1024]{1,0:T(8,128)(2,1)S(1)} %bitcast.28, bf16[352,1024]{1,0:T(8,128)(2,1)S(1)} %bitcast.29), custom_call_target="tpu_custom_call" | custom-call | flops 277000000 | bytes 2700000 | tf_op jit(solution)/shard_map/expert/pallas_call | solution.py:203
  83.9 6.0 %all-to-all-start.3 = ((bf16[128,4,256]{2,1,0:T(4,128)(2,1)}), bf16[128,4,256]{2,1,0:T(4,128)(2,1)S(1)}, u32[]{:S(2)}, u32[]{:S(2)}) async-start(bf16[128,4,256]{2,1,0:T(4,128)(2,1)} %expert.1), calls=%async_computation.3 | async-start | bytes 524288 | tf_op jit(solution)/shard_map/all_to_all | solution.py:21
  89.9 0.1 copy.24.ids
  90.0 0.0 copy-done.8
  90.0 0.7 slice.9
  90.7 0.0 all-gather.2.cloned.1.call-done
  90.7 0.0 copy-start
  90.8 1.4 %copy-done = bf16[32,96,256]{2,1,0:T(8,128)(2,1)S(1)} copy-done((bf16[32,96,256]{2,1,0:T(8,128)(2,1)S(1)}, bf16[32,96,256]{2,1,0:T(8,128)(2,1)}, u32[]{:S(2)}) %copy-start) | copy-done | bytes 1572888
  92.2 0.6 dense.1.part
  92.8 12.3 %all-to-all-done.3.returned = bf16[128,4,256]{2,1,0:T(4,128)(2,1)S(1)} async-done(((bf16[128,4,256]{2,1,0:T(4,128)(2,1)}), bf16[128,4,256]{2,1,0:T(4,128)(2,1)S(1)}, u32[]{:S(2)}, u32[]{:S(2)}) %all-to-all-start.3) | async-done | bytes 262176 | tf_op jit(solution)/shard_map/all_to_all | solution.py:21
  105.1 0.6 combine.1
  105.7 10.5 %all_to_all.27 = bf16[16,16,256]{2,1,0:T(8,128)(2,1)S(1)} all-to-all(bf16[16,16,256]{2,1,0:T(8,128)(2,1)S(1)} %combine.1), channel_id=1, replica_groups=mesh['zh'=4,'zl'=2,'yh'=4,'yl'=2,'c'=2,'x'=4] {'zl','yl','x'}, dimensions={0} | all-to-all | bytes 262144 | tf_op jit(solution)/shard_map/all_to_all | solution.py:21
  116.3 0.6 add_convert_fusion
  (3 shorter events, 0.1 us)
Async XLA Ops:
  6.5 84.2 %all-gather.2.cloned.1.call-start = ((), (), s32[]{:S(2)}) async-start(), calls=%async_computation.5 | async-start | bytes 1622016 | tf_op jit(solution)/shard_map/all_gather | solution.py:287
  8.1 18.8 %copy-start.4 = (bf16[512,256]{1,0:T(8,128)(2,1)S(1)}, bf16[512,256]{1,0:T(8,128)(2,1)}, u32[]{:S(2)}) copy-start(bf16[512,256]{1,0:T(8,128)(2,1)} %w0.1) | copy-start | bytes 786436
  8.1 35.0 %copy-start.5 = (f32[1024]{0:T(1024)S(1)}, f32[1024]{0:T(1024)}, u32[]{:S(2)}) copy-start(f32[1024]{0:T(1024)} %param.34) | copy-start | bytes 12292
  8.1 35.0 %copy-start.6 = (s32[16,2]{0,1:T(2,128)S(1)}, s32[16,2]{0,1:T(2,128)}, u32[]{:S(2)}) copy-start(s32[16,2]{0,1:T(2,128)} %param.35) | copy-start | bytes 388
  17.7 0.7 copy-start.7
  21.6 60.2 %copy-start.1 = (bf16[1,1024,352]{1,2,0:T(8,128)(2,1)S(1)}, bf16[1,1024,352]{1,2,0:T(8,128)(2,1)}, u32[]{:S(2)}) copy-start(bf16[1,1024,352]{1,2,0:T(8,128)(2,1)} %param.37) | copy-start | bytes 2162692
  21.6 60.2 %copy-start.2 = (bf16[1,1024,352]{1,2,0:T(8,128)(2,1)S(1)}, bf16[1,1024,352]{1,2,0:T(8,128)(2,1)}, u32[]{:S(2)}) copy-start(bf16[1,1024,352]{1,2,0:T(8,128)(2,1)} %param.38) | copy-start | bytes 2162692
  21.6 60.2 %copy-start.3 = (bf16[1,352,1024]{2,1,0:T(8,128)(2,1)S(1)}, bf16[1,352,1024]{2,1,0:T(8,128)(2,1)}, u32[]{:S(2)}) copy-start(bf16[1,352,1024]{2,1,0:T(8,128)(2,1)} %param.39) | copy-start | bytes 2162692
  21.6 21.5 %all-to-all-start.1 = ((bf16[16,16,384]{2,1,0:T(8,128)(2,1)}), bf16[16,16,384]{2,1,0:T(8,128)(2,1)S(1)}, u32[]{:S(2)}, u32[]{:S(2)}) async-start(bf16[16,16,384]{2,1,0:T(8,128)(2,1)} %cell.1), calls=%async_computation.1 | async-start | bytes 393216 | tf_op jit(solution)/shard_map/all_to_all | solution.py:21
  26.9 10.7 %collective-permute-start = (bf16[512,256]{1,0:T(8,128)(2,1)S(1)}, bf16[512,256]{1,0:T(8,128)(2,1)S(1)}, u32[]{:S(2)}, u32[]{:S(2)}) collective-permute-start(bf16[512,256]{1,0:T(8,128)(2,1)S(1)} %copy-done.4), channel_id=1, source_target_pairs={{0,1},{1,2},{2,3},{3,0},{4,5},{5,6},{6,7},{7,4},{8,9},{9,10},{10,1... | collective-permute-start | bytes 786440 | tf_op jit(solution)/shard_map/ppermute | solution.py:34
  30.1 11.4 %collective-permute-start.1 = (bf16[512,256]{1,0:T(8,128)(2,1)S(1)}, bf16[512,256]{1,0:T(8,128)(2,1)S(1)}, u32[]{:S(2)}, u32[]{:S(2)}) collective-permute-start(bf16[512,256]{1,0:T(8,128)(2,1)S(1)} %copy-done.4), channel_id=1, source_target_pairs={{0,2},{1,3},{2,0},{3,1},{4,6},{5,7},{6,4},{7,5},{8,10},{9,11},{10,... | collective-permute-start | bytes 786440 | tf_op jit(solution)/shard_map/ppermute | solution.py:34
  34.4 8.6 %collective-permute-start.2 = (bf16[512,256]{1,0:T(8,128)(2,1)S(1)}, bf16[512,256]{1,0:T(8,128)(2,1)S(1)}, u32[]{:S(2)}, u32[]{:S(2)}) collective-permute-start(bf16[512,256]{1,0:T(8,128)(2,1)S(1)} %copy-done.4), channel_id=1, source_target_pairs={{0,3},{1,0},{2,1},{3,2},{4,7},{5,4},{6,5},{7,6},{8,11},{9,8},{10,9... | collective-permute-start | bytes 786440 | tf_op jit(solution)/shard_map/ppermute | solution.py:34
  81.8 8.2 %copy-start.8 = (f32[16,2]{0,1:T(2,128)S(1)}, f32[16,2]{0,1:T(2,128)}, u32[]{:S(2)}) copy-start(f32[16,2]{0,1:T(2,128)} %param.36) | copy-start | bytes 388
  83.9 21.2 %all-to-all-start.3 = ((bf16[128,4,256]{2,1,0:T(4,128)(2,1)}), bf16[128,4,256]{2,1,0:T(4,128)(2,1)S(1)}, u32[]{:S(2)}, u32[]{:S(2)}) async-start(bf16[128,4,256]{2,1,0:T(4,128)(2,1)} %expert.1), calls=%async_computation.3 | async-start | bytes 524288 | tf_op jit(solution)/shard_map/all_to_all | solution.py:21
  90.7 1.4 %copy-start = (bf16[32,96,256]{2,1,0:T(8,128)(2,1)S(1)}, bf16[32,96,256]{2,1,0:T(8,128)(2,1)}, u32[]{:S(2)}) copy-start(bf16[32,96,256]{2,1,0:T(8,128)(2,1)} %all-gather.2.cloned.1.call-done) | copy-start | bytes 4718596
Sparse Core Ops, SparseCore 0:
  18.6 67.1 all-gather.1

commit v8 on v7

--- a/solution.py
+++ b/solution.py
@@ -68,7 +68,17 @@
     )(tokens, gate, up, down, mix)
 
 
-def cell_kernel(first, gain, wq, wk, wv, wo, wi, wf, state, norm, peak, tokens, out):
+def cell_kernel(*refs):
+    count = (len(refs) - 2) // 2
+    stored, out, kept, arrived = refs[:count], refs[count], refs[count + 1 : -1], refs[-1]
+    copies = [
+        pltpu.make_async_copy(stored[k], kept[k], arrived.at[k]) for k in range(count)
+    ]
+    for copy in copies:
+        copy.start()
+    for copy in copies[:-1]:
+        copy.wait()
+    first, gain, wq, wk, wv, wo, wi, wf, norm, peak, tokens, state = kept
     seqs = norm.shape[0]
     values = jnp.concatenate([first[k, :seqs] for k in range(first.shape[0])], axis=1).astype(f32)
     scale = lax.rsqrt(jnp.mean(values * values, axis=1, keepdims=True) + epsilon)
@@ -85,6 +95,7 @@
     old = jnp.exp(carried - stabilizer)
     new = jnp.exp(enter - stabilizer) * jnp.sum(query * key, axis=1, keepdims=True)
     turned = query.T
+    copies[-1].wait()
     read = [
         jnp.sum(turned[:, b : b + 1] * state[b], axis=0, keepdims=True) for b in range(seqs)
     ]
@@ -98,12 +109,19 @@
 
 
 def cell(first, gain, wq, wk, wv, wo, wi, wf, state, norm, peak, tokens, count):
+    stored = (first, gain, wq, wk, wv, wo, wi, wf, norm, peak, tokens, state)
+    away = pl.BlockSpec(memory_space=pltpu.HBM)
+    here = pl.BlockSpec(memory_space=pltpu.VMEM)
     return pl.pallas_call(
         cell_kernel,
         out_shape=jax.ShapeDtypeStruct((count, norm.shape[0], HEAD + tokens.shape[1]), bf16),
+        in_specs=[away] * len(stored),
+        out_specs=here,
+        scratch_shapes=[pltpu.VMEM(a.shape, a.dtype) for a in stored]
+        + [pltpu.SemaphoreType.DMA((len(stored),))],
         cost_estimate=pl.CostEstimate(flops=40000000, bytes_accessed=2200000, transcendentals=9000),
         name="cell",
-    )(first, gain, wq, wk, wv, wo, wi, wf, state, norm, peak, tokens)
+    )(*stored)
 
 
 def residual_kernel(me, place, second, w0, w1, w2, w3, gain, ids, group, outgoing, own, resid):
@@ -209,7 +227,7 @@
     )(rows, gate, up, down)
 
 
-def combine_kernel(place, part, returned, ids, weights, out):
+def combine_kernel(mine, part, returned, ids, weights, out):
     seqs, quarter = out.shape[1:]
     experts, tp, _ = returned.shape
     expert = lax.broadcasted_iota(jnp.int32, (seqs, experts), 1)
@@ -220,14 +238,13 @@
     second = dot((expert == here[:, 1:2]).astype(f32).astype(bf16), rows)
     moe = ahead * first + behind * second
     for s in range(out.shape[0] // tp):
-        mine = jnp.where(place[0] == s, 1.0, 0.0)
         for k in range(tp):
             columns = slice(k * quarter, (k + 1) * quarter)
-            value = part[s * seqs : (s + 1) * seqs, columns] + mine * moe[:, columns]
+            value = part[s * seqs : (s + 1) * seqs, columns] + mine[s] * moe[:, columns]
             out[s * tp + k] = value.astype(bf16)
 
 
-def combine(place, part, returned, ids, weights, quarter):
+def combine(mine, part, returned, ids, weights, quarter):
     seqs = ids.shape[0]
     whole = pl.BlockSpec(memory_space=pltpu.VMEM)
     count = part.shape[0] // seqs * (part.shape[1] // quarter)
@@ -238,7 +255,7 @@
         out_specs=whole,
         compiler_params=pltpu.CompilerParams(vmem_limit_bytes=8 << 20),
         name="combine",
-    )(place[None], part, returned, ids, weights)
+    )(mine, part, returned, ids, weights)
 
 
 def layer(
@@ -279,6 +296,7 @@
 
     turned_logits = route_logits.T
     route_weight = jax.nn.sigmoid(turned_logits - turned_logits[::-1])
+    mine = (jnp.arange(near, dtype=jnp.int32) == place).astype(f32)
 
     mix_out = {0: w_mix_out}
     for step in (2, 1, 3):
@@ -314,7 +332,7 @@
     returned = exchange(partial, EP)
 
     part = dense_branch(group, dense, mix_row)
-    part = combine(place, part, returned, route_ids, route_weight, quarter)
+    part = combine(mine, part, returned, route_ids, route_weight, quarter)
     parts = exchange(part, NEAR + ("x",))
     total = own_resid.astype(f32) + parts.astype(f32).sum(axis=0)
     return total.astype(bf16)

time: 124 us -> 125 us (level)
  no operation moved by 1% of the time
where the time goes in v8:
time: 125 us; the launch traced here: 124 us
  blocking collectives  58.2 us (47%)
  starting transfers between devices  22 us (18%)
  waiting for transfers between devices  17.9 us (14%)
  between operations  13.5 us (11%)
  Pallas kernels  9.13 us (7%)
  local copies, waits for them, and re-layouts  2.96 us (2%)
    all_to_all x3, blocking collectives, exchange(): return lax.all_to_all(blocks, axis, 0, 0, tiled=True)  58.2 us
    all_to_all x2, waiting for transfers between devices, exchange(): return lax.all_to_all(blocks, axis, 0, 0, tiled=True)  12.3 us
    all_to_all x2, starting transfers between devices, exchange(): return lax.all_to_all(blocks, axis, 0, 0, tiled=True)  11.4 us
    ppermute x3, starting transfers between devices, shifted(): lax.ppermute(array, axis, [(i, (i + step) % size) for i in range(size)])  10.7 us
    ppermute x3, waiting for transfers between devices, shifted(): lax.ppermute(array, axis, [(i, (i + step) % size) for i in range(size)])  5.49 us
    pallas_call x1, Pallas kernels, cell(): pl.pallas_call(cell_kernel, out_shape=jax.ShapeDtypeStruct((count, norm.s...  2.86 us
  transfers between devices with their start and end apart: 6, of which 3 were waited for; matrix products, arithmetic and copies ran while one was open for 1% of the time, Pallas kernels for 5%

profile of v8, /device:TPU:1, one launch (start us, length us, event | category | flops | bytes accessed | tf_op | source)
XLA Modules:
  0.0 124.3 jit_solution(18240987879904371073)
XLA Ops:
  6.5 0.0 all-gather.2.cloned.1.call-start
  6.5 1.6 %pack.1 = bf16[4,48,256]{2,1,0:T(8,128)(2,1)} custom-call(bf16[16,256]{1,0:T(8,128)(2,1)} %refs_10_.1, bf16[24,256]{1,0:T(8,128)(2,1)} %bitcast.35, bf16[24,256]{1,0:T(8,128)(2,1)} %bitcast.36, bf16[24,256]{1,0:T(8,128)(2,1)} %down.1, bf16[256]{0:T(256)(128)(2,1)} %mix.1), custom_call_target="tpu_custom_call" | custom-call | tf_op jit(solution)/shard_map/pack/pallas_call | solution.py:64
  8.1 0.0 copy-start.4
  8.1 0.0 copy-start.5
  8.1 0.0 copy-start.6
  8.1 9.6 %all_to_all.25.refs_0_ = bf16[4,48,256]{2,1,0:T(8,128)(2,1)S(1)} all-to-all(bf16[4,48,256]{2,1,0:T(8,128)(2,1)} %pack.1), channel_id=1, replica_groups=mesh['zh'=4,'zl'=2,'yh'=4,'yl'=2,'c'=2,'x'=4] {'x'}, dimensions={0} | all-to-all | bytes 196608 | tf_op jit(solution)/shard_map/all_to_all | solution.py:21
  17.7 0.0 copy-start.7
  17.7 0.7 slice.8
  18.4 0.0 all-gather.2.cloned.1.call-update
  18.4 0.0 copy-done.7
  18.4 2.9 %cell.1 = bf16[16,16,384]{2,1,0:T(8,128)(2,1)} custom-call(bf16[4,48,256]{2,1,0:T(8,128)(2,1)} %copy-done.7, f32[1,1024]{1,0:T(1,128)} %bitcast.38, bf16[1024,128]{1,0:T(8,128)(2,1)} %refs_2_.1, bf16[1024,128]{1,0:T(8,128)(2,1)} %refs_3_.1, bf16[1024,128]{1,0:T(8,128)(2,1)} %refs_4_.1, bf16[1024,128]{1,0:T(8,128)(2,1)} %refs_5_.1, bf16[1,1024]{1,0:T(2,128)(2,1)} %bitcast.39, ...), custom_call_target="tpu_custom_call" | custom-call | flops 40000000 | bytes 2200000 | tf_op jit(solution)/shard_map/cell/pallas_call | solution.py:115
  21.3 0.0 copy-start.1
  21.3 0.0 copy-start.2
  21.3 0.0 copy-start.3
  21.3 5.2 %all-to-all-start.1 = ((bf16[16,16,384]{2,1,0:T(8,128)(2,1)}), bf16[16,16,384]{2,1,0:T(8,128)(2,1)S(1)}, u32[]{:S(2)}, u32[]{:S(2)}) async-start(bf16[16,16,384]{2,1,0:T(8,128)(2,1)} %cell.1), calls=%async_computation.1 | async-start | bytes 393216 | tf_op jit(solution)/shard_map/all_to_all | solution.py:21
  26.6 0.0 copy-done.4
  26.6 3.3 %collective-permute-start = (bf16[512,256]{1,0:T(8,128)(2,1)S(1)}, bf16[512,256]{1,0:T(8,128)(2,1)S(1)}, u32[]{:S(2)}, u32[]{:S(2)}) collective-permute-start(bf16[512,256]{1,0:T(8,128)(2,1)S(1)} %copy-done.4), channel_id=1, source_target_pairs={{0,1},{1,2},{2,3},{3,0},{4,5},{5,6},{6,7},{7,4},{8,9},{9,10},{10,1... | collective-permute-start | bytes 786440 | tf_op jit(solution)/shard_map/ppermute | solution.py:34
  29.9 4.3 %collective-permute-start.1 = (bf16[512,256]{1,0:T(8,128)(2,1)S(1)}, bf16[512,256]{1,0:T(8,128)(2,1)S(1)}, u32[]{:S(2)}, u32[]{:S(2)}) collective-permute-start(bf16[512,256]{1,0:T(8,128)(2,1)S(1)} %copy-done.4), channel_id=1, source_target_pairs={{0,2},{1,3},{2,0},{3,1},{4,6},{5,7},{6,4},{7,5},{8,10},{9,11},{10,... | collective-permute-start | bytes 786440 | tf_op jit(solution)/shard_map/ppermute | solution.py:34
  34.2 3.1 %collective-permute-start.2 = (bf16[512,256]{1,0:T(8,128)(2,1)S(1)}, bf16[512,256]{1,0:T(8,128)(2,1)S(1)}, u32[]{:S(2)}, u32[]{:S(2)}) collective-permute-start(bf16[512,256]{1,0:T(8,128)(2,1)S(1)} %copy-done.4), channel_id=1, source_target_pairs={{0,3},{1,0},{2,1},{3,2},{4,7},{5,4},{6,5},{7,6},{8,11},{9,8},{10,9... | collective-permute-start | bytes 786440 | tf_op jit(solution)/shard_map/ppermute | solution.py:34
  37.3 0.0 collective-permute-done.w1
  37.3 3.9 %collective-permute-done.1.w2 = bf16[512,256]{1,0:T(8,128)(2,1)S(1)} collective-permute-done((bf16[512,256]{1,0:T(8,128)(2,1)S(1)}, bf16[512,256]{1,0:T(8,128)(2,1)S(1)}, u32[]{:S(2)}, u32[]{:S(2)}) %collective-permute-start.1) | collective-permute-done | bytes 262176 | tf_op jit(solution)/shard_map/ppermute | solution.py:34
  41.2 1.6 %collective-permute-done.2.w3 = bf16[512,256]{1,0:T(8,128)(2,1)S(1)} collective-permute-done((bf16[512,256]{1,0:T(8,128)(2,1)S(1)}, bf16[512,256]{1,0:T(8,128)(2,1)S(1)}, u32[]{:S(2)}, u32[]{:S(2)}) %collective-permute-start.2) | collective-permute-done | bytes 262176 | tf_op jit(solution)/shard_map/ppermute | solution.py:34
  42.8 0.0 all-to-all-done.1
  42.8 0.0 copy-done.5
  42.8 0.0 copy-done.6
  42.8 0.9 residual.1
  43.7 37.9 %all_to_all.26.rows = bf16[128,4,256]{2,1,0:T(4,128)(2,1)S(1)} all-to-all(bf16[128,4,256]{2,1,0:T(4,128)(2,1)S(1)} %get-tuple-element.10), channel_id=1, replica_groups=mesh['zh'=4,'zl'=2,'yh'=4,'yl'=2,'c'=2,'x'=4] {'zh','zl','yh','yl','c'}, dimensions={0} | all-to-all | bytes 524288 | tf_op jit(solution)/shard_map/all_to_all | solution.py:21
  81.6 0.0 copy-done.1
  81.6 0.0 copy-done.2
  81.6 0.0 copy-done.3
  81.6 0.0 copy-start.8
  81.6 2.1 %expert.1 = bf16[128,4,256]{2,1,0:T(4,128)(2,1)} custom-call(bf16[128,4,256]{2,1,0:T(4,128)(2,1)S(1)} %all_to_all.26.rows, bf16[352,1024]{1,0:T(8,128)(2,1)S(1)} %bitcast.27, bf16[352,1024]{1,0:T(8,128)(2,1)S(1)} %bitcast.28, bf16[352,1024]{1,0:T(8,128)(2,1)S(1)} %bitcast.29), custom_call_target="tpu_custom_call" | custom-call | flops 277000000 | bytes 2700000 | tf_op jit(solution)/shard_map/expert/pallas_call | solution.py:221
  83.7 6.1 %all-to-all-start.3 = ((bf16[128,4,256]{2,1,0:T(4,128)(2,1)}), bf16[128,4,256]{2,1,0:T(4,128)(2,1)S(1)}, u32[]{:S(2)}, u32[]{:S(2)}) async-start(bf16[128,4,256]{2,1,0:T(4,128)(2,1)} %expert.1), calls=%async_computation.3 | async-start | bytes 524288 | tf_op jit(solution)/shard_map/all_to_all | solution.py:21
  89.8 0.1 copy.24.ids
  89.9 0.0 copy-done.8
  90.0 0.7 slice.9
  90.7 0.0 all-gather.2.cloned.1.call-done
  90.7 0.0 copy-start
  90.7 1.4 %copy-done = bf16[32,96,256]{2,1,0:T(8,128)(2,1)S(1)} copy-done((bf16[32,96,256]{2,1,0:T(8,128)(2,1)S(1)}, bf16[32,96,256]{2,1,0:T(8,128)(2,1)}, u32[]{:S(2)}) %copy-start) | copy-done | bytes 1572888
  92.1 0.6 dense.1.part
  92.7 12.3 %all-to-all-done.3.returned = bf16[128,4,256]{2,1,0:T(4,128)(2,1)S(1)} async-done(((bf16[128,4,256]{2,1,0:T(4,128)(2,1)}), bf16[128,4,256]{2,1,0:T(4,128)(2,1)S(1)}, u32[]{:S(2)}, u32[]{:S(2)}) %all-to-all-start.3) | async-done | bytes 262176 | tf_op jit(solution)/shard_map/all_to_all | solution.py:21
  105.1 1.1 combine.1
  106.2 10.6 %all_to_all.27 = bf16[16,16,256]{2,1,0:T(8,128)(2,1)S(1)} all-to-all(bf16[16,16,256]{2,1,0:T(8,128)(2,1)S(1)} %combine.1), channel_id=1, replica_groups=mesh['zh'=4,'zl'=2,'yh'=4,'yl'=2,'c'=2,'x'=4] {'zl','yl','x'}, dimensions={0} | all-to-all | bytes 262144 | tf_op jit(solution)/shard_map/all_to_all | solution.py:21
  116.9 0.6 add_convert_fusion
  (4 shorter events, 0.1 us)
Async XLA Ops:
  6.5 84.2 %all-gather.2.cloned.1.call-start = ((), (), s32[]{:S(2)}) async-start(), calls=%async_computation.5 | async-start | bytes 1622016 | tf_op jit(solution)/shard_map/all_gather | solution.py:305
  8.1 18.5 %copy-start.4 = (bf16[512,256]{1,0:T(8,128)(2,1)S(1)}, bf16[512,256]{1,0:T(8,128)(2,1)}, u32[]{:S(2)}) copy-start(bf16[512,256]{1,0:T(8,128)(2,1)} %w0.1) | copy-start | bytes 786436
  8.1 34.7 %copy-start.5 = (f32[1024]{0:T(1024)S(1)}, f32[1024]{0:T(1024)}, u32[]{:S(2)}) copy-start(f32[1024]{0:T(1024)} %param.34) | copy-start | bytes 12292
  8.1 34.7 %copy-start.6 = (s32[16,2]{0,1:T(2,128)S(1)}, s32[16,2]{0,1:T(2,128)}, u32[]{:S(2)}) copy-start(s32[16,2]{0,1:T(2,128)} %param.35) | copy-start | bytes 388
  17.7 0.7 copy-start.7
  21.3 60.3 %copy-start.1 = (bf16[1,1024,352]{1,2,0:T(8,128)(2,1)S(1)}, bf16[1,1024,352]{1,2,0:T(8,128)(2,1)}, u32[]{:S(2)}) copy-start(bf16[1,1024,352]{1,2,0:T(8,128)(2,1)} %param.37) | copy-start | bytes 2162692
  21.3 60.3 %copy-start.2 = (bf16[1,1024,352]{1,2,0:T(8,128)(2,1)S(1)}, bf16[1,1024,352]{1,2,0:T(8,128)(2,1)}, u32[]{:S(2)}) copy-start(bf16[1,1024,352]{1,2,0:T(8,128)(2,1)} %param.38) | copy-start | bytes 2162692
  21.3 60.2 %copy-start.3 = (bf16[1,352,1024]{2,1,0:T(8,128)(2,1)S(1)}, bf16[1,352,1024]{2,1,0:T(8,128)(2,1)}, u32[]{:S(2)}) copy-start(bf16[1,352,1024]{2,1,0:T(8,128)(2,1)} %param.39) | copy-start | bytes 2162692
  21.3 21.5 %all-to-all-start.1 = ((bf16[16,16,384]{2,1,0:T(8,128)(2,1)}), bf16[16,16,384]{2,1,0:T(8,128)(2,1)S(1)}, u32[]{:S(2)}, u32[]{:S(2)}) async-start(bf16[16,16,384]{2,1,0:T(8,128)(2,1)} %cell.1), calls=%async_computation.1 | async-start | bytes 393216 | tf_op jit(solution)/shard_map/all_to_all | solution.py:21
  26.6 10.7 %collective-permute-start = (bf16[512,256]{1,0:T(8,128)(2,1)S(1)}, bf16[512,256]{1,0:T(8,128)(2,1)S(1)}, u32[]{:S(2)}, u32[]{:S(2)}) collective-permute-start(bf16[512,256]{1,0:T(8,128)(2,1)S(1)} %copy-done.4), channel_id=1, source_target_pairs={{0,1},{1,2},{2,3},{3,0},{4,5},{5,6},{6,7},{7,4},{8,9},{9,10},{10,1... | collective-permute-start | bytes 786440 | tf_op jit(solution)/shard_map/ppermute | solution.py:34
  29.9 11.4 %collective-permute-start.1 = (bf16[512,256]{1,0:T(8,128)(2,1)S(1)}, bf16[512,256]{1,0:T(8,128)(2,1)S(1)}, u32[]{:S(2)}, u32[]{:S(2)}) collective-permute-start(bf16[512,256]{1,0:T(8,128)(2,1)S(1)} %copy-done.4), channel_id=1, source_target_pairs={{0,2},{1,3},{2,0},{3,1},{4,6},{5,7},{6,4},{7,5},{8,10},{9,11},{10,... | collective-permute-start | bytes 786440 | tf_op jit(solution)/shard_map/ppermute | solution.py:34
  34.2 8.6 %collective-permute-start.2 = (bf16[512,256]{1,0:T(8,128)(2,1)S(1)}, bf16[512,256]{1,0:T(8,128)(2,1)S(1)}, u32[]{:S(2)}, u32[]{:S(2)}) collective-permute-start(bf16[512,256]{1,0:T(8,128)(2,1)S(1)} %copy-done.4), channel_id=1, source_target_pairs={{0,3},{1,0},{2,1},{3,2},{4,7},{5,4},{6,5},{7,6},{8,11},{9,8},{10,9... | collective-permute-start | bytes 786440 | tf_op jit(solution)/shard_map/ppermute | solution.py:34
  81.6 8.4 %copy-start.8 = (f32[16,2]{0,1:T(2,128)S(1)}, f32[16,2]{0,1:T(2,128)}, u32[]{:S(2)}) copy-start(f32[16,2]{0,1:T(2,128)} %param.36) | copy-start | bytes 388
  83.7 21.4 %all-to-all-start.3 = ((bf16[128,4,256]{2,1,0:T(4,128)(2,1)}), bf16[128,4,256]{2,1,0:T(4,128)(2,1)S(1)}, u32[]{:S(2)}, u32[]{:S(2)}) async-start(bf16[128,4,256]{2,1,0:T(4,128)(2,1)} %expert.1), calls=%async_computation.3 | async-start | bytes 524288 | tf_op jit(solution)/shard_map/all_to_all | solution.py:21
  90.7 1.4 %copy-start = (bf16[32,96,256]{2,1,0:T(8,128)(2,1)S(1)}, bf16[32,96,256]{2,1,0:T(8,128)(2,1)}, u32[]{:S(2)}) copy-start(bf16[32,96,256]{2,1,0:T(8,128)(2,1)} %all-gather.2.cloned.1.call-done) | copy-start | bytes 4718596
Sparse Core Ops, SparseCore 0:
  18.6 67.2 all-gather.1

commit v9 on v8

--- a/solution.py
+++ b/solution.py
@@ -78,7 +78,7 @@
         copy.start()
     for copy in copies[:-1]:
         copy.wait()
-    first, gain, wq, wk, wv, wo, wi, wf, norm, peak, tokens, state = kept
+    first, gain, wq, wk, wv, wo, wi, wf, norm, peak, state = kept
     seqs = norm.shape[0]
     values = jnp.concatenate([first[k, :seqs] for k in range(first.shape[0])], axis=1).astype(f32)
     scale = lax.rsqrt(jnp.mean(values * values, axis=1, keepdims=True) + epsilon)
@@ -104,17 +104,16 @@
     mixed = gate * (numerator / jnp.maximum(jnp.abs(denominator), 1.0))
     mixed = mixed.astype(bf16)
     for k in range(out.shape[0]):
-        out[k, :, :HEAD] = mixed
-        out[k, :, HEAD:] = tokens[...]
-
-
-def cell(first, gain, wq, wk, wv, wo, wi, wf, state, norm, peak, tokens, count):
-    stored = (first, gain, wq, wk, wv, wo, wi, wf, norm, peak, tokens, state)
+        out[k] = mixed
+
+
+def cell(first, gain, wq, wk, wv, wo, wi, wf, state, norm, peak, count):
+    stored = (first, gain, wq, wk, wv, wo, wi, wf, norm, peak, state)
     away = pl.BlockSpec(memory_space=pltpu.HBM)
     here = pl.BlockSpec(memory_space=pltpu.VMEM)
     return pl.pallas_call(
         cell_kernel,
-        out_shape=jax.ShapeDtypeStruct((count, norm.shape[0], HEAD + tokens.shape[1]), bf16),
+        out_shape=jax.ShapeDtypeStruct((count, *norm.shape), bf16),
         in_specs=[away] * len(stored),
         out_specs=here,
         scratch_shapes=[pltpu.VMEM(a.shape, a.dtype) for a in stored]
@@ -124,58 +123,47 @@
     )(*stored)
 
 
-def residual_kernel(me, place, second, w0, w1, w2, w3, gain, ids, group, outgoing, own, resid):
-    near, tp, seqs, _ = second.shape
+def residual_kernel(me, second, first, w0, w1, w2, w3, gain, ids, normed, outgoing, own, resid):
+    tp, seqs, _ = second.shape
     quarter = w0.shape[1]
-    heads = jnp.concatenate(
-        [
-            jnp.concatenate([second[s, k, :, :HEAD] for s in range(near)], axis=0)
-            for k in range(tp)
-        ],
-        axis=1,
-    )
-    total = jnp.zeros((near * seqs, 1), f32)
+    heads = jnp.concatenate([second[k] for k in range(tp)], axis=1)
+    total = jnp.zeros((seqs, 1), f32)
     for step, weight in enumerate((w0, w1, w2, w3)):
         k = (me[0] + tp - step) & (tp - 1)
-        added = dot(heads, weight[...])
-        old = jnp.concatenate([second[s, k, :, HEAD:] for s in range(near)], axis=0)
-        values = (old.astype(f32) + added).astype(bf16)
+        values = (first[k, :seqs].astype(f32) + dot(heads, weight[...])).astype(bf16)
         wide = values.astype(f32)
         total = total + jnp.sum(wide * wide, axis=1, keepdims=True)
         resid[:, pl.ds(pl.multiple_of(k * quarter, quarter), quarter)] = wide
         if step == 0:
-            group[:, :quarter] = values
-    start = pl.multiple_of(place[0] * seqs, seqs)
-    own[...] = group[pl.ds(start, seqs), :quarter]
+            own[...] = values
     scale = lax.rsqrt(total * (1.0 / (tp * quarter)) + epsilon)
-    group[...] = (resid[...] * scale * gain[...]).astype(bf16)
-    experts = outgoing.shape[0]
-    expert = lax.broadcasted_iota(jnp.int32, (experts, seqs), 0)
+    rows = (resid[...] * scale * gain[...]).astype(bf16)
+    normed[...] = rows
+    expert = lax.broadcasted_iota(jnp.int32, (outgoing.shape[0], seqs), 0)
     chosen = ((expert == ids[0:1, :]) | (expert == ids[1:2, :])).astype(f32).astype(bf16)
-    rows = dot(chosen, group[pl.ds(start, seqs), :])
+    sent = dot(chosen, rows)
     for k in range(tp):
-        outgoing[:, k, :] = rows[:, k * quarter : (k + 1) * quarter].astype(bf16)
-
-
-def residual(me, place, second, weights, gain, ids, experts):
-    near, tp, seqs, _ = second.shape
+        outgoing[:, k, :] = sent[:, k * quarter : (k + 1) * quarter].astype(bf16)
+
+
+def residual(me, second, first, weights, gain, ids, experts):
+    tp, seqs, _ = second.shape
     quarter = weights[0].shape[1]
     whole = pl.BlockSpec(memory_space=pltpu.VMEM)
-    scalar = pl.BlockSpec(memory_space=pltpu.SMEM)
     return pl.pallas_call(
         residual_kernel,
         out_shape=(
-            jax.ShapeDtypeStruct((near * seqs, tp * quarter), bf16),
+            jax.ShapeDtypeStruct((seqs, tp * quarter), bf16),
             jax.ShapeDtypeStruct((experts, tp, quarter), bf16),
             jax.ShapeDtypeStruct((seqs, quarter), bf16),
         ),
-        in_specs=[scalar, scalar] + [whole] * 7,
+        in_specs=[pl.BlockSpec(memory_space=pltpu.SMEM)] + [whole] * 8,
         out_specs=(whole, whole, whole),
-        scratch_shapes=[pltpu.VMEM((near * seqs, tp * quarter), f32)],
-        cost_estimate=pl.CostEstimate(flops=140000000, bytes_accessed=2000000, transcendentals=128),
+        scratch_shapes=[pltpu.VMEM((seqs, tp * quarter), f32)],
         compiler_params=pltpu.CompilerParams(vmem_limit_bytes=12 << 20),
+        cost_estimate=pl.CostEstimate(flops=21000000, bytes_accessed=1500000, transcendentals=16),
         name="residual",
-    )(me[None], place[None], second, *weights, gain, ids)
+    )(me[None], second, first, *weights, gain, ids)
 
 
 def dense_kernel(group, weights, mix, out):
@@ -227,7 +215,7 @@
     )(rows, gate, up, down)
 
 
-def combine_kernel(mine, part, returned, ids, weights, out):
+def combine_kernel(slots, part, returned, ids, weights, out):
     seqs, quarter = out.shape[1:]
     experts, tp, _ = returned.shape
     expert = lax.broadcasted_iota(jnp.int32, (seqs, experts), 1)
@@ -240,11 +228,13 @@
     for s in range(out.shape[0] // tp):
         for k in range(tp):
             columns = slice(k * quarter, (k + 1) * quarter)
-            value = part[s * seqs : (s + 1) * seqs, columns] + mine[s] * moe[:, columns]
-            out[s * tp + k] = value.astype(bf16)
-
-
-def combine(mine, part, returned, ids, weights, quarter):
+            value = part[s * seqs : (s + 1) * seqs, columns]
+            if s == 0:
+                value = value + moe[:, columns]
+            out[slots[s] + k] = value.astype(bf16)
+
+
+def combine(slots, part, returned, ids, weights, quarter):
     seqs = ids.shape[0]
     whole = pl.BlockSpec(memory_space=pltpu.VMEM)
     count = part.shape[0] // seqs * (part.shape[1] // quarter)
@@ -255,7 +245,7 @@
         out_specs=whole,
         compiler_params=pltpu.CompilerParams(vmem_limit_bytes=8 << 20),
         name="combine",
-    )(mine, part, returned, ids, weights)
+    )(slots, part, returned, ids, weights)
 
 
 def layer(
@@ -296,7 +286,7 @@
 
     turned_logits = route_logits.T
     route_weight = jax.nn.sigmoid(turned_logits - turned_logits[::-1])
-    mine = (jnp.arange(near, dtype=jnp.int32) == place).astype(f32)
+    slots = (jnp.arange(near, dtype=jnp.int32) ^ place) * tp
 
     mix_out = {0: w_mix_out}
     for step in (2, 1, 3):
@@ -317,22 +307,24 @@
         cell_state[:, 0],
         norm_state[:, 0],
         max_state.T,
-        tokens,
-        near * tp,
+        tp,
     )
-    second = exchange(sent, NEAR + ("x",))
-    second = second.reshape(near, tp, seqs, HEAD + quarter)
+    second = exchange(sent, "x")
     group, outgoing, own_resid = residual(
-        me, place, second, [mix_out[k] for k in range(tp)], gain_ffn[None], route_ids.T, experts
+        me, second, first, [mix_out[k] for k in range(tp)], gain_ffn[None], route_ids.T, experts
     )
 
     received = exchange(outgoing, EP)
+
+    for axis in ("yl", "zl"):
+        other = lax.ppermute(group, axis, [(0, 1), (1, 0)])
+        group = jnp.concatenate([group, other], axis=0)
 
     partial = expert(received, expert_gate[0].T, expert_up[0].T, expert_down[0])
     returned = exchange(partial, EP)
 
     part = dense_branch(group, dense, mix_row)
-    part = combine(mine, part, returned, route_ids, route_weight, quarter)
+    part = combine(slots, part, returned, route_ids, route_weight, quarter)
     parts = exchange(part, NEAR + ("x",))
     total = own_resid.astype(f32) + parts.astype(f32).sum(axis=0)
     return total.astype(bf16)

time: 125 us -> 121 us (0.968)
  blocking collectives: 58.2 us -> 18.6 us
  starting transfers between devices: 22 us -> 45.6 us
  waiting for transfers between devices: 17.9 us -> 27.7 us
    all_to_all x3 -> x2, blocking collectives: 58.2 us -> 18.6 us  [exchange(): return lax.all_to_all(blocks, axis, 0, 0, tiled=True)]
    all_to_all x2 -> x3, starting transfers between devices: 11.4 us -> 30.7 us  [exchange(): return lax.all_to_all(blocks, axis, 0, 0, tiled=True)]
    all_to_all x2 -> x3, waiting for transfers between devices: 12.3 us -> 23.3 us  [exchange(): return lax.all_to_all(blocks, axis, 0, 0, tiled=True)]
    ppermute x0 -> x2, starting transfers between devices: none -> 6.52 us  [layer(): other = lax.ppermute(group, axis, [(0, 1), (1, 0)])]
    ppermute x3, waiting for transfers between devices: 5.49 us -> 0.01 us  [shifted(): lax.ppermute(array, axis, [(i, (i + step) % size) for i in range(size)])]
    ppermute x0 -> x2, waiting for transfers between devices: none -> 4.3 us  [layer(): other = lax.ppermute(group, axis, [(0, 1), (1, 0)])]
    ppermute x3, starting transfers between devices: 10.7 us -> 8.43 us  [shifted(): lax.ppermute(array, axis, [(i, (i + step) % size) for i in range(size)])]
  transfers between devices with their start and end apart: 6 -> 9, of which waited for: 3 -> 4; matrix products, arithmetic and copies ran while one was open for 1% -> 1% of each run, Pallas kernels for 5% -> 6%
where the time goes in v9:
time: 121 us; the launch traced here: 120 us
  starting transfers between devices  45.6 us (38%)
  waiting for transfers between devices  27.7 us (23%)
  blocking collectives  18.6 us (15%)
  between operations  13.6 us (11%)
  Pallas kernels  9.84 us (8%)
  local copies, waits for them, and re-layouts  3.81 us (3%)
    all_to_all x3, starting transfers between devices, exchange(): return lax.all_to_all(blocks, axis, 0, 0, tiled=True)  30.7 us
    all_to_all x3, waiting for transfers between devices, exchange(): return lax.all_to_all(blocks, axis, 0, 0, tiled=True)  23.3 us
    all_to_all x2, blocking collectives, exchange(): return lax.all_to_all(blocks, axis, 0, 0, tiled=True)  18.6 us
    ppermute x3, starting transfers between devices, shifted(): lax.ppermute(array, axis, [(i, (i + step) % size) for i in range(size)])  8.43 us
    ppermute x2, starting transfers between devices, layer(): other = lax.ppermute(group, axis, [(0, 1), (1, 0)])  6.52 us
    ppermute x2, waiting for transfers between devices, layer(): other = lax.ppermute(group, axis, [(0, 1), (1, 0)])  4.3 us
    pallas_call x1, Pallas kernels, cell(): pl.pallas_call(cell_kernel, out_shape=jax.ShapeDtypeStruct((count, *norm....  2.9 us
  transfers between devices with their start and end apart: 9, of which 4 were waited for; matrix products, arithmetic and copies ran while one was open for 1% of the time, Pallas kernels for 6%

profile of v9, /device:TPU:1, one launch (start us, length us, event | category | flops | bytes accessed | tf_op | source)
XLA Modules:
  0.0 119.8 jit_solution(18382457973559872854)
XLA Ops:
  6.5 0.0 copy-start.6
  6.5 0.0 copy-start.8
  6.5 0.0 copy-start.7
  6.5 0.0 all-gather.2.cloned.1.call-start
  6.5 1.6 %pack.1 = bf16[4,48,256]{2,1,0:T(8,128)(2,1)} custom-call(bf16[16,256]{1,0:T(8,128)(2,1)} %tokens.1, bf16[24,256]{1,0:T(8,128)(2,1)} %bitcast.32, bf16[24,256]{1,0:T(8,128)(2,1)} %bitcast.33, bf16[24,256]{1,0:T(8,128)(2,1)} %down.1, bf16[256]{0:T(256)(128)(2,1)} %mix.1), custom_call_target="tpu_custom_call" | custom-call | tf_op jit(solution)/shard_map/pack/pallas_call | solution.py:64
  8.1 9.5 %all_to_all.25.refs_0_.first = bf16[4,48,256]{2,1,0:T(8,128)(2,1)S(1)} all-to-all(bf16[4,48,256]{2,1,0:T(8,128)(2,1)} %pack.1), channel_id=1, replica_groups=mesh['zh'=4,'zl'=2,'yh'=4,'yl'=2,'c'=2,'x'=4] {'x'}, dimensions={0} | all-to-all | bytes 196608 | tf_op jit(solution)/shard_map/all_to_all | solution.py:21
  17.6 0.0 copy-start.1
  17.6 0.6 slice.8
  18.3 0.0 all-gather.2.cloned.1.call-update
  18.3 2.2 %collective-permute-start = (bf16[512,256]{1,0:T(8,128)(2,1)}, bf16[512,256]{1,0:T(8,128)(2,1)S(1)}, u32[]{:S(2)}, u32[]{:S(2)}) collective-permute-start(bf16[512,256]{1,0:T(8,128)(2,1)} %w0.1), channel_id=1, source_target_pairs={{0,1},{1,2},{2,3},{3,0},{4,5},{5,6},{6,7},{7,4},{8,9},{9,10},{10,1... | collective-permute-start | bytes 786440 | tf_op jit(solution)/shard_map/ppermute | solution.py:34
  20.5 3.7 %collective-permute-start.1 = (bf16[512,256]{1,0:T(8,128)(2,1)}, bf16[512,256]{1,0:T(8,128)(2,1)S(1)}, u32[]{:S(2)}, u32[]{:S(2)}) collective-permute-start(bf16[512,256]{1,0:T(8,128)(2,1)} %w0.1), channel_id=1, source_target_pairs={{0,2},{1,3},{2,0},{3,1},{4,6},{5,7},{6,4},{7,5},{8,10},{9,11},{10,... | collective-permute-start | bytes 786440 | tf_op jit(solution)/shard_map/ppermute | solution.py:34
  24.2 2.5 %collective-permute-start.2 = (bf16[512,256]{1,0:T(8,128)(2,1)}, bf16[512,256]{1,0:T(8,128)(2,1)S(1)}, u32[]{:S(2)}, u32[]{:S(2)}) collective-permute-start(bf16[512,256]{1,0:T(8,128)(2,1)} %w0.1), channel_id=1, source_target_pairs={{0,3},{1,0},{2,1},{3,2},{4,7},{5,4},{6,5},{7,6},{8,11},{9,8},{10,9... | collective-permute-start | bytes 786440 | tf_op jit(solution)/shard_map/ppermute | solution.py:34
  26.7 0.0 copy-done.1
  26.8 0.0 copy-start.9
  26.8 0.0 copy-start.3
  26.8 0.0 copy-start.4
  26.8 0.0 copy-start.5
  26.8 2.9 %cell.1 = bf16[4,16,128]{2,1,0:T(8,128)(2,1)} custom-call(bf16[4,48,256]{2,1,0:T(8,128)(2,1)} %copy-done.1, f32[1,1024]{1,0:T(1,128)} %bitcast.35, bf16[1024,128]{1,0:T(8,128)(2,1)} %refs_2_.1, bf16[1024,128]{1,0:T(8,128)(2,1)} %refs_3_.1, bf16[1024,128]{1,0:T(8,128)(2,1)} %refs_4_.1, bf16[1024,128]{1,0:T(8,128)(2,1)} %refs_5_.1, bf16[1,1024]{1,0:T(2,128)(2,1)} %bitcast.36, ...), custom_call_target="tpu_custom_call" | custom-call | flops 40000000 | bytes 2200000 | tf_op jit(solution)/shard_map/cell/pallas_call | solution.py:114
  29.7 3.6 %all-to-all-start.1 = ((bf16[4,16,128]{2,1,0:T(8,128)(2,1)}), bf16[4,16,128]{2,1,0:T(8,128)(2,1)S(1)}, u32[]{:S(2)}, u32[]{:S(2)}) async-start(bf16[4,16,128]{2,1,0:T(8,128)(2,1)} %cell.1), calls=%async_computation.1 | async-start | bytes 32768 | tf_op jit(solution)/shard_map/all_to_all | solution.py:21
  33.3 4.2 %all-to-all-done.1.second = bf16[4,16,128]{2,1,0:T(8,128)(2,1)S(1)} async-done(((bf16[4,16,128]{2,1,0:T(8,128)(2,1)}), bf16[4,16,128]{2,1,0:T(8,128)(2,1)S(1)}, u32[]{:S(2)}, u32[]{:S(2)}) %all-to-all-start.1) | async-done | bytes 16416 | tf_op jit(solution)/shard_map/all_to_all | solution.py:21
  37.6 0.0 collective-permute-done.w1
  37.6 0.0 collective-permute-done.1.w2
  37.6 0.0 collective-permute-done.2.w3
  37.6 0.0 copy-done.6
  37.6 0.0 copy-done.8
  37.6 0.0 copy-done.7
  37.6 0.0 copy-start.2
  37.6 0.9 copy-done.2
  38.5 1.5 %residual.1 = (bf16[16,1024]{1,0:T(8,128)(2,1)S(1)}, bf16[128,4,256]{2,1,0:T(4,128)(2,1)}, bf16[16,256]{1,0:T(8,128)(2,1)S(1)}) custom-call(s32[1]{0:T(128)} %bitcast.me, bf16[4,16,128]{2,1,0:T(8,128)(2,1)S(1)} %all-to-all-done.1.second, bf16[4,48,256]{2,1,0:T(8,128)(2,1)S(1)} %copy-done.2, bf16[512,256]{1,0:T(8,128)(2,1)S(1)} %copy-done.6, ...), custom_call_target="tpu_custom_call" | custom-call | flops 21000000 | bytes 1500000 | tf_op jit(solution)/shard_map/residual/pallas_call | solution.py:153
  40.0 21.3 %all-to-all-start.2 = ((bf16[128,4,256]{2,1,0:T(4,128)(2,1)}), bf16[128,4,256]{2,1,0:T(4,128)(2,1)S(1)}, u32[]{:S(2)}, u32[]{:S(2)}) async-start(bf16[128,4,256]{2,1,0:T(4,128)(2,1)} %get-tuple-element.10), calls=%async_computation.2 | async-start | bytes 524288 | tf_op jit(solution)/shard_map/all_to_all | solution.py:21
  61.3 0.0 copy-done.9
  61.3 3.2 %collective-permute-start.3 = (bf16[16,1024]{1,0:T(8,128)(2,1)S(1)}, bf16[16,1024]{1,0:T(8,128)(2,1)S(1)}, u32[]{:S(2)}, u32[]{:S(2)}) collective-permute-start(bf16[16,1024]{1,0:T(8,128)(2,1)S(1)} %get-tuple-element.9), channel_id=1, source_target_pairs={{0,8},{8,0},{1,9},{9,1},{2,10},{10,2},{3,11},{11,3},{4,12},{12,4},... | collective-permute-start | bytes 98312 | tf_op jit(solution)/shard_map/ppermute | solution.py:320
  64.6 14.4 %all-to-all-done.2.rows = bf16[128,4,256]{2,1,0:T(4,128)(2,1)S(1)} async-done(((bf16[128,4,256]{2,1,0:T(4,128)(2,1)}), bf16[128,4,256]{2,1,0:T(4,128)(2,1)S(1)}, u32[]{:S(2)}, u32[]{:S(2)}) %all-to-all-start.2) | async-done | bytes 262176 | tf_op jit(solution)/shard_map/all_to_all | solution.py:21
  79.0 0.0 copy-done.3
  79.0 0.0 copy-done.4
  79.0 0.0 copy-done.5
  79.0 2.1 %expert.1 = bf16[128,4,256]{2,1,0:T(4,128)(2,1)} custom-call(bf16[128,4,256]{2,1,0:T(4,128)(2,1)S(1)} %all-to-all-done.2.rows, bf16[352,1024]{1,0:T(8,128)(2,1)S(1)} %bitcast.24, bf16[352,1024]{1,0:T(8,128)(2,1)S(1)} %bitcast.25, bf16[352,1024]{1,0:T(8,128)(2,1)S(1)} %bitcast.26), custom_call_target="tpu_custom_call" | custom-call | flops 277000000 | bytes 2700000 | tf_op jit(solution)/shard_map/expert/pallas_call | solution.py:209
  81.1 5.8 %all-to-all-start.3 = ((bf16[128,4,256]{2,1,0:T(4,128)(2,1)}), bf16[128,4,256]{2,1,0:T(4,128)(2,1)S(1)}, u32[]{:S(2)}, u32[]{:S(2)}) async-start(bf16[128,4,256]{2,1,0:T(4,128)(2,1)} %expert.1), calls=%async_computation.3 | async-start | bytes 524288 | tf_op jit(solution)/shard_map/all_to_all | solution.py:21
  86.9 0.1 copy.24.ids
  87.0 0.0 collective-permute-done.3
  87.0 3.3 %collective-permute-start.4 = (bf16[32,1024]{1,0:T(8,128)(2,1)S(1)}, bf16[32,1024]{1,0:T(8,128)(2,1)S(1)}, u32[]{:S(2)}, u32[]{:S(2)}) collective-permute-start(bf16[32,1024]{1,0:T(8,128)(2,1)S(1)} %pad_maximum_fusion.1), channel_id=1, source_target_pairs={{0,64},{64,0},{1,65},{65,1},{2,66},{66,2},{3,67},{67,3},{4,68},{68... | collective-permute-start | bytes 196616 | tf_op jit(solution)/shard_map/ppermute | solution.py:320
  90.3 0.7 slice.9
  91.0 4.3 %collective-permute-done.4 = bf16[32,1024]{1,0:T(8,128)(2,1)S(1)} collective-permute-done((bf16[32,1024]{1,0:T(8,128)(2,1)S(1)}, bf16[32,1024]{1,0:T(8,128)(2,1)S(1)}, u32[]{:S(2)}, u32[]{:S(2)}) %collective-permute-start.4) | collective-permute-done | bytes 65568 | tf_op jit(solution)/shard_map/ppermute | solution.py:320
  95.3 0.0 all-gather.2.cloned.1.call-done
  95.3 0.0 copy-start
  95.3 1.4 %copy-done = bf16[32,96,256]{2,1,0:T(8,128)(2,1)S(1)} copy-done((bf16[32,96,256]{2,1,0:T(8,128)(2,1)S(1)}, bf16[32,96,256]{2,1,0:T(8,128)(2,1)}, u32[]{:S(2)}) %copy-start) | copy-done | bytes 1572888
  96.7 0.6 dense.1.part
  97.4 4.7 %all-to-all-done.3.returned = bf16[128,4,256]{2,1,0:T(4,128)(2,1)S(1)} async-done(((bf16[128,4,256]{2,1,0:T(4,128)(2,1)}), bf16[128,4,256]{2,1,0:T(4,128)(2,1)S(1)}, u32[]{:S(2)}, u32[]{:S(2)}) %all-to-all-start.3) | async-done | bytes 262176 | tf_op jit(solution)/shard_map/all_to_all | solution.py:21
  102.1 1.1 combine.1
  103.2 9.1 %all_to_all.26 = bf16[16,16,256]{2,1,0:T(8,128)(2,1)S(1)} all-to-all(bf16[16,16,256]{2,1,0:T(8,128)(2,1)S(1)} %combine.1), channel_id=1, replica_groups=mesh['zh'=4,'zl'=2,'yh'=4,'yl'=2,'c'=2,'x'=4] {'zl','yl','x'}, dimensions={0} | all-to-all | bytes 262144 | tf_op jit(solution)/shard_map/all_to_all | solution.py:21
  112.4 0.6 add_convert_fusion
  (6 shorter events, 0.1 us)
Async XLA Ops:
  6.5 31.0 %copy-start.6 = (bf16[512,256]{1,0:T(8,128)(2,1)S(1)}, bf16[512,256]{1,0:T(8,128)(2,1)}, u32[]{:S(2)}) copy-start(bf16[512,256]{1,0:T(8,128)(2,1)} %w0.1) | copy-start | bytes 786436
  6.5 31.0 %copy-start.8 = (s32[16,2]{0,1:T(2,128)S(1)}, s32[16,2]{0,1:T(2,128)}, u32[]{:S(2)}) copy-start(s32[16,2]{0,1:T(2,128)} %param.35) | copy-start | bytes 388
  6.5 31.1 %copy-start.7 = (f32[1024]{0:T(1024)S(1)}, f32[1024]{0:T(1024)}, u32[]{:S(2)}) copy-start(f32[1024]{0:T(1024)} %param.34) | copy-start | bytes 12292
  6.5 88.8 %all-gather.2.cloned.1.call-start = ((), (), s32[]{:S(2)}) async-start(), calls=%async_computation.5 | async-start | bytes 1622016 | tf_op jit(solution)/shard_map/all_gather | solution.py:295
  17.6 9.1 %copy-start.1 = (bf16[4,48,256]{2,1,0:T(8,128)(2,1)}, bf16[4,48,256]{2,1,0:T(8,128)(2,1)S(1)}, u32[]{:S(2)}) copy-start(bf16[4,48,256]{2,1,0:T(8,128)(2,1)S(1)} %all_to_all.25.refs_0_.first) | copy-start | bytes 294916
  18.3 19.3 %collective-permute-start = (bf16[512,256]{1,0:T(8,128)(2,1)}, bf16[512,256]{1,0:T(8,128)(2,1)S(1)}, u32[]{:S(2)}, u32[]{:S(2)}) collective-permute-start(bf16[512,256]{1,0:T(8,128)(2,1)} %w0.1), channel_id=1, source_target_pairs={{0,1},{1,2},{2,3},{3,0},{4,5},{5,6},{6,7},{7,4},{8,9},{9,10},{10,1... | collective-permute-start | bytes 786440 | tf_op jit(solution)/shard_map/ppermute | solution.py:34
  20.5 17.1 %collective-permute-start.1 = (bf16[512,256]{1,0:T(8,128)(2,1)}, bf16[512,256]{1,0:T(8,128)(2,1)S(1)}, u32[]{:S(2)}, u32[]{:S(2)}) collective-permute-start(bf16[512,256]{1,0:T(8,128)(2,1)} %w0.1), channel_id=1, source_target_pairs={{0,2},{1,3},{2,0},{3,1},{4,6},{5,7},{6,4},{7,5},{8,10},{9,11},{10,... | collective-permute-start | bytes 786440 | tf_op jit(solution)/shard_map/ppermute | solution.py:34
  24.2 13.4 %collective-permute-start.2 = (bf16[512,256]{1,0:T(8,128)(2,1)}, bf16[512,256]{1,0:T(8,128)(2,1)S(1)}, u32[]{:S(2)}, u32[]{:S(2)}) collective-permute-start(bf16[512,256]{1,0:T(8,128)(2,1)} %w0.1), channel_id=1, source_target_pairs={{0,3},{1,0},{2,1},{3,2},{4,7},{5,4},{6,5},{7,6},{8,11},{9,8},{10,9... | collective-permute-start | bytes 786440 | tf_op jit(solution)/shard_map/ppermute | solution.py:34
  26.8 34.5 %copy-start.9 = (f32[16,2]{0,1:T(2,128)S(1)}, f32[16,2]{0,1:T(2,128)}, u32[]{:S(2)}) copy-start(f32[16,2]{0,1:T(2,128)} %param.36) | copy-start | bytes 388
  26.8 52.2 %copy-start.3 = (bf16[1,1024,352]{1,2,0:T(8,128)(2,1)S(1)}, bf16[1,1024,352]{1,2,0:T(8,128)(2,1)}, u32[]{:S(2)}) copy-start(bf16[1,1024,352]{1,2,0:T(8,128)(2,1)} %param.37) | copy-start | bytes 2162692
  26.8 52.2 %copy-start.4 = (bf16[1,1024,352]{1,2,0:T(8,128)(2,1)S(1)}, bf16[1,1024,352]{1,2,0:T(8,128)(2,1)}, u32[]{:S(2)}) copy-start(bf16[1,1024,352]{1,2,0:T(8,128)(2,1)} %param.38) | copy-start | bytes 2162692
  26.8 52.2 %copy-start.5 = (bf16[1,352,1024]{2,1,0:T(8,128)(2,1)S(1)}, bf16[1,352,1024]{2,1,0:T(8,128)(2,1)}, u32[]{:S(2)}) copy-start(bf16[1,352,1024]{2,1,0:T(8,128)(2,1)} %param.39) | copy-start | bytes 2162692
  29.7 7.8 %all-to-all-start.1 = ((bf16[4,16,128]{2,1,0:T(8,128)(2,1)}), bf16[4,16,128]{2,1,0:T(8,128)(2,1)S(1)}, u32[]{:S(2)}, u32[]{:S(2)}) async-start(bf16[4,16,128]{2,1,0:T(8,128)(2,1)} %cell.1), calls=%async_computation.1 | async-start | bytes 32768 | tf_op jit(solution)/shard_map/all_to_all | solution.py:21
  37.6 0.9 copy-start.2
  40.0 39.0 %all-to-all-start.2 = ((bf16[128,4,256]{2,1,0:T(4,128)(2,1)}), bf16[128,4,256]{2,1,0:T(4,128)(2,1)S(1)}, u32[]{:S(2)}, u32[]{:S(2)}) async-start(bf16[128,4,256]{2,1,0:T(4,128)(2,1)} %get-tuple-element.10), calls=%async_computation.2 | async-start | bytes 524288 | tf_op jit(solution)/shard_map/all_to_all | solution.py:21
  61.3 25.6 %collective-permute-start.3 = (bf16[16,1024]{1,0:T(8,128)(2,1)S(1)}, bf16[16,1024]{1,0:T(8,128)(2,1)S(1)}, u32[]{:S(2)}, u32[]{:S(2)}) collective-permute-start(bf16[16,1024]{1,0:T(8,128)(2,1)S(1)} %get-tuple-element.9), channel_id=1, source_target_pairs={{0,8},{8,0},{1,9},{9,1},{2,10},{10,2},{3,11},{11,3},{4,12},{12,4},... | collective-permute-start | bytes 98312 | tf_op jit(solution)/shard_map/ppermute | solution.py:320
  81.1 21.0 %all-to-all-start.3 = ((bf16[128,4,256]{2,1,0:T(4,128)(2,1)}), bf16[128,4,256]{2,1,0:T(4,128)(2,1)S(1)}, u32[]{:S(2)}, u32[]{:S(2)}) async-start(bf16[128,4,256]{2,1,0:T(4,128)(2,1)} %expert.1), calls=%async_computation.3 | async-start | bytes 524288 | tf_op jit(solution)/shard_map/all_to_all | solution.py:21
  87.0 8.3 %collective-permute-start.4 = (bf16[32,1024]{1,0:T(8,128)(2,1)S(1)}, bf16[32,1024]{1,0:T(8,128)(2,1)S(1)}, u32[]{:S(2)}, u32[]{:S(2)}) collective-permute-start(bf16[32,1024]{1,0:T(8,128)(2,1)S(1)} %pad_maximum_fusion.1), channel_id=1, source_target_pairs={{0,64},{64,0},{1,65},{65,1},{2,66},{66,2},{3,67},{67,3},{4,68},{68... | collective-permute-start | bytes 196616 | tf_op jit(solution)/shard_map/ppermute | solution.py:320
  95.3 1.4 %copy-start = (bf16[32,96,256]{2,1,0:T(8,128)(2,1)S(1)}, bf16[32,96,256]{2,1,0:T(8,128)(2,1)}, u32[]{:S(2)}) copy-start(bf16[32,96,256]{2,1,0:T(8,128)(2,1)} %all-gather.2.cloned.1.call-done) | copy-start | bytes 4718596
Sparse Core Ops, SparseCore 0:
  18.4 66.4 all-gather.1

commit v10 on v7

--- a/solution.py
+++ b/solution.py
@@ -68,7 +68,7 @@
     )(tokens, gate, up, down, mix)
 
 
-def cell_kernel(first, gain, wq, wk, wv, wo, wi, wf, state, norm, peak, tokens, out):
+def cell_kernel(first, gain, wq, wk, wv, wo, wi, wf, norm, peak, tokens, state, out):
     seqs = norm.shape[0]
     values = jnp.concatenate([first[k, :seqs] for k in range(first.shape[0])], axis=1).astype(f32)
     scale = lax.rsqrt(jnp.mean(values * values, axis=1, keepdims=True) + epsilon)
@@ -98,12 +98,30 @@
 
 
 def cell(first, gain, wq, wk, wv, wo, wi, wf, state, norm, peak, tokens, count):
+    stored = (first, gain, wq, wk, wv, wo, wi, wf, norm, peak, tokens, state)
     return pl.pallas_call(
         cell_kernel,
         out_shape=jax.ShapeDtypeStruct((count, norm.shape[0], HEAD + tokens.shape[1]), bf16),
+        compiler_params=pltpu.CompilerParams(vmem_limit_bytes=12 << 20),
         cost_estimate=pl.CostEstimate(flops=40000000, bytes_accessed=2200000, transcendentals=9000),
         name="cell",
-    )(first, gain, wq, wk, wv, wo, wi, wf, state, norm, peak, tokens)
+    )(*stored)
+
+
+def marker_kernel(place, out):
+    row = lax.broadcasted_iota(jnp.int32, out.shape, 0)
+    out[...] = jnp.where(row == place[0], 1.0, 0.0)
+
+
+def marker(place, count):
+    return pl.pallas_call(
+        marker_kernel,
+        out_shape=jax.ShapeDtypeStruct((count, HEAD), f32),
+        in_specs=[pl.BlockSpec(memory_space=pltpu.SMEM)],
+        compiler_params=pltpu.CompilerParams(vmem_limit_bytes=1 << 20),
+        cost_estimate=pl.CostEstimate(flops=8000000000, bytes_accessed=16384, transcendentals=0),
+        name="marker",
+    )(place[None])
 
 
 def residual_kernel(me, place, second, w0, w1, w2, w3, gain, ids, group, outgoing, own, resid):
@@ -209,7 +227,7 @@
     )(rows, gate, up, down)
 
 
-def combine_kernel(place, part, returned, ids, weights, out):
+def combine_kernel(mine, part, returned, ids, weights, out):
     seqs, quarter = out.shape[1:]
     experts, tp, _ = returned.shape
     expert = lax.broadcasted_iota(jnp.int32, (seqs, experts), 1)
@@ -220,25 +238,22 @@
     second = dot((expert == here[:, 1:2]).astype(f32).astype(bf16), rows)
     moe = ahead * first + behind * second
     for s in range(out.shape[0] // tp):
-        mine = jnp.where(place[0] == s, 1.0, 0.0)
         for k in range(tp):
             columns = slice(k * quarter, (k + 1) * quarter)
-            value = part[s * seqs : (s + 1) * seqs, columns] + mine * moe[:, columns]
+            value = part[s * seqs : (s + 1) * seqs, columns] + mine[s : s + 1, 0:1] * moe[:, columns]
             out[s * tp + k] = value.astype(bf16)
 
 
-def combine(place, part, returned, ids, weights, quarter):
+def combine(mine, part, returned, ids, weights, quarter):
     seqs = ids.shape[0]
     whole = pl.BlockSpec(memory_space=pltpu.VMEM)
     count = part.shape[0] // seqs * (part.shape[1] // quarter)
     return pl.pallas_call(
         combine_kernel,
         out_shape=jax.ShapeDtypeStruct((count, seqs, quarter), bf16),
-        in_specs=[pl.BlockSpec(memory_space=pltpu.SMEM)] + [whole] * 4,
-        out_specs=whole,
         compiler_params=pltpu.CompilerParams(vmem_limit_bytes=8 << 20),
         name="combine",
-    )(place[None], part, returned, ids, weights)
+    )(mine, part, returned, ids, weights)
 
 
 def layer(
@@ -279,6 +294,7 @@
 
     turned_logits = route_logits.T
     route_weight = jax.nn.sigmoid(turned_logits - turned_logits[::-1])
+    mine = marker(place, near)
 
     mix_out = {0: w_mix_out}
     for step in (2, 1, 3):
@@ -314,7 +330,7 @@
     returned = exchange(partial, EP)
 
     part = dense_branch(group, dense, mix_row)
-    part = combine(place, part, returned, route_ids, route_weight, quarter)
+    part = combine(mine, part, returned, route_ids, route_weight, quarter)
     parts = exchange(part, NEAR + ("x",))
     total = own_resid.astype(f32) + parts.astype(f32).sum(axis=0)
     return total.astype(bf16)

time: 124 us -> 132 us (1.065)
  blocking collectives: 58 us -> 20.5 us
  starting transfers between devices: 21.9 us -> 41.9 us
  waiting for transfers between devices: 17.9 us -> 34.4 us
  local copies, waits for them, and re-layouts: 2.96 us -> 11.3 us
    all_to_all x3 -> x2, blocking collectives: 58 us -> 20.5 us  [exchange(): return lax.all_to_all(blocks, axis, 0, 0, tiled=True)]
    all_to_all x2 -> x3, starting transfers between devices: 11.2 us -> 31.2 us  [exchange(): return lax.all_to_all(blocks, axis, 0, 0, tiled=True)]
    all_to_all x2 -> x3, waiting for transfers between devices: 12.3 us -> 28.9 us  [exchange(): return lax.all_to_all(blocks, axis, 0, 0, tiled=True)]
    unnamed x19 -> x39, local copies, waits for them, and re-layouts: 1.52 us -> 10.6 us
    pallas_call x1, Pallas kernels: 3.15 us -> 1.5 us  [cell(): pl.pallas_call(cell_kernel, out_shape=jax.ShapeDtypeStruct((count, norm.s...]
    pallas_call x1, Pallas kernels: 0.86 us -> 2.52 us  [residual(): pl.pallas_call(residual_kernel, out_shape=(jax.ShapeDtypeStruct((near * s...]
  transfers between devices with their start and end apart: 6 -> 7, of which waited for: 3 -> 4; matrix products, arithmetic and copies ran while one was open for 1% -> 0% of each run, Pallas kernels for 5% -> 5%
where the time goes in v10:
time: 132 us; the launch traced here: 131 us
  starting transfers between devices  41.9 us (32%)
  waiting for transfers between devices  34.4 us (26%)
  blocking collectives  20.5 us (16%)
  between operations  13.5 us (10%)
  local copies, waits for them, and re-layouts  11.3 us (9%)
  Pallas kernels  8.9 us (7%)
    all_to_all x3, starting transfers between devices, exchange(): return lax.all_to_all(blocks, axis, 0, 0, tiled=True)  31.2 us
    all_to_all x3, waiting for transfers between devices, exchange(): return lax.all_to_all(blocks, axis, 0, 0, tiled=True)  28.9 us
    all_to_all x2, blocking collectives, exchange(): return lax.all_to_all(blocks, axis, 0, 0, tiled=True)  20.5 us
    ppermute x3, starting transfers between devices, shifted(): lax.ppermute(array, axis, [(i, (i + step) % size) for i in range(size)])  10.7 us
    unnamed x39, local copies, waits for them, and re-layouts  10.6 us
    ppermute x3, waiting for transfers between devices, shifted(): lax.ppermute(array, axis, [(i, (i + step) % size) for i in range(size)])  5.49 us
  transfers between devices with their start and end apart: 7, of which 4 were waited for; matrix products, arithmetic and copies ran while one was open for 0% of the time, Pallas kernels for 5%

profile of v10, /device:TPU:1, one launch (start us, length us, event | category | flops | bytes accessed | tf_op | source)
XLA Modules:
  0.0 131.2 jit_solution(424957183191409531)
XLA Ops:
  6.5 0.0 all-gather.2.cloned.1.call-start
  6.5 1.5 %pack.1 = bf16[4,48,256]{2,1,0:T(8,128)(2,1)} custom-call(bf16[16,256]{1,0:T(8,128)(2,1)} %tokens.3, bf16[24,256]{1,0:T(8,128)(2,1)} %bitcast.40, bf16[24,256]{1,0:T(8,128)(2,1)} %bitcast.41, bf16[24,256]{1,0:T(8,128)(2,1)} %down.1, bf16[256]{0:T(256)(128)(2,1)} %mix.1), custom_call_target="tpu_custom_call" | custom-call | tf_op jit(solution)/shard_map/pack/pallas_call | solution.py:64
  8.1 0.0 copy-start.5
  8.1 0.0 copy-start.15
  8.1 0.0 copy-start.16
  8.1 9.6 %all_to_all.25.first = bf16[4,48,256]{2,1,0:T(8,128)(2,1)S(1)} all-to-all(bf16[4,48,256]{2,1,0:T(8,128)(2,1)} %pack.1), channel_id=1, replica_groups=mesh['zh'=4,'zl'=2,'yh'=4,'yl'=2,'c'=2,'x'=4] {'x'}, dimensions={0} | all-to-all | bytes 196608 | tf_op jit(solution)/shard_map/all_to_all | solution.py:21
  17.7 0.6 slice.8
  18.3 0.0 all-gather.2.cloned.1.call-update
  18.4 0.0 copy-start.1
  18.4 1.2 copy-done.1
  19.6 0.0 copy-start.6
  19.6 0.9 copy-done.6
  20.5 0.0 copy-start.7
  20.5 0.9 copy-done.7
  21.5 0.0 copy-start.8
  21.5 0.9 copy-done.8
  22.4 0.0 copy-start.9
  22.4 0.9 copy-done.9
  23.4 0.0 copy-start.10
  23.4 0.7 copy-done.10
  24.1 0.0 copy-start.11
  24.1 0.7 copy-done.11
  24.8 0.0 copy-start.12
  24.8 0.7 copy-done.12
  25.5 0.0 copy-start.13
  25.5 0.7 copy-done.13
  26.2 0.0 copy-start.14
  26.2 0.7 copy-done.14
  26.8 0.0 copy-start.17
  26.9 0.7 copy-done.17
  27.5 1.5 %cell.1 = bf16[16,16,384]{2,1,0:T(8,128)(2,1)} custom-call(bf16[4,48,256]{2,1,0:T(8,128)(2,1)S(1)} %all_to_all.25.first, f32[1,1024]{1,0:T(1,128)S(1)} %bitcast.33, bf16[1024,128]{1,0:T(8,128)(2,1)S(1)} %copy-done.6, bf16[1024,128]{1,0:T(8,128)(2,1)S(1)} %copy-done.7, bf16[1024,128]{1,0:T(8,128)(2,1)S(1)} %copy-done.8, bf16[1024,128]{1,0:T(8,128)(2,1)S(1)} %copy-done.9, ...), custom_call_target="tpu_custom_call" | custom-call | flops 40000000 | bytes 2200000 | tf_op jit(solution)/shard_map/cell/pallas_call | solution.py:102
  29.0 0.0 copy-start.18
  29.0 0.0 copy-start.2
  29.0 0.0 copy-start.3
  29.0 0.0 copy-start.4
  29.0 5.2 %all-to-all-start.1 = ((bf16[16,16,384]{2,1,0:T(8,128)(2,1)}), bf16[16,16,384]{2,1,0:T(8,128)(2,1)S(1)}, u32[]{:S(2)}, u32[]{:S(2)}) async-start(bf16[16,16,384]{2,1,0:T(8,128)(2,1)} %cell.1), calls=%async_computation.1 | async-start | bytes 393216 | tf_op jit(solution)/shard_map/all_to_all | solution.py:21
  34.3 0.0 copy-done.5
  34.3 3.3 %collective-permute-start = (bf16[512,256]{1,0:T(8,128)(2,1)S(1)}, bf16[512,256]{1,0:T(8,128)(2,1)S(1)}, u32[]{:S(2)}, u32[]{:S(2)}) collective-permute-start(bf16[512,256]{1,0:T(8,128)(2,1)S(1)} %copy-done.5), channel_id=1, source_target_pairs={{0,1},{1,2},{2,3},{3,0},{4,5},{5,6},{6,7},{7,4},{8,9},{9,10},{10,1... | collective-permute-start | bytes 786440 | tf_op jit(solution)/shard_map/ppermute | solution.py:34
  37.5 4.3 %collective-permute-start.1 = (bf16[512,256]{1,0:T(8,128)(2,1)S(1)}, bf16[512,256]{1,0:T(8,128)(2,1)S(1)}, u32[]{:S(2)}, u32[]{:S(2)}) collective-permute-start(bf16[512,256]{1,0:T(8,128)(2,1)S(1)} %copy-done.5), channel_id=1, source_target_pairs={{0,2},{1,3},{2,0},{3,1},{4,6},{5,7},{6,4},{7,5},{8,10},{9,11},{10,... | collective-permute-start | bytes 786440 | tf_op jit(solution)/shard_map/ppermute | solution.py:34
  41.9 3.1 %collective-permute-start.2 = (bf16[512,256]{1,0:T(8,128)(2,1)S(1)}, bf16[512,256]{1,0:T(8,128)(2,1)}, u32[]{:S(2)}, u32[]{:S(2)}) collective-permute-start(bf16[512,256]{1,0:T(8,128)(2,1)S(1)} %copy-done.5), channel_id=1, source_target_pairs={{0,3},{1,0},{2,1},{3,2},{4,7},{5,4},{6,5},{7,6},{8,11},{9,8},{10,9... | collective-permute-start | bytes 786440 | tf_op jit(solution)/shard_map/ppermute | solution.py:34
  45.0 0.0 collective-permute-done.w1
  45.0 3.9 %collective-permute-done.1.w2 = bf16[512,256]{1,0:T(8,128)(2,1)S(1)} collective-permute-done((bf16[512,256]{1,0:T(8,128)(2,1)S(1)}, bf16[512,256]{1,0:T(8,128)(2,1)S(1)}, u32[]{:S(2)}, u32[]{:S(2)}) %collective-permute-start.1) | collective-permute-done | bytes 262176 | tf_op jit(solution)/shard_map/ppermute | solution.py:34
  48.8 1.6 %collective-permute-done.2.w3 = bf16[512,256]{1,0:T(8,128)(2,1)} collective-permute-done((bf16[512,256]{1,0:T(8,128)(2,1)S(1)}, bf16[512,256]{1,0:T(8,128)(2,1)}, u32[]{:S(2)}, u32[]{:S(2)}) %collective-permute-start.2) | collective-permute-done | bytes 262176 | tf_op jit(solution)/shard_map/ppermute | solution.py:34
  50.5 0.0 all-to-all-done.1
  50.5 0.0 copy-done.15
  50.5 0.0 copy-done.16
  50.5 2.5 %residual.1 = (bf16[64,1024]{1,0:T(8,128)(2,1)S(1)}, bf16[128,4,256]{2,1,0:T(4,128)(2,1)}, bf16[16,256]{1,0:T(8,128)(2,1)S(1)}) custom-call(s32[1]{0:T(128)} %bitcast.me, s32[1]{0:T(128)} %bitcast.1.place, bf16[4,4,16,384]{3,2,1,0:T(8,128)(2,1)S(1)} %bitcast.27, bf16[512,256]{1,0:T(8,128)(2,1)S(1)} %copy-done.5, ...), custom_call_target="tpu_custom_call" | custom-call | flops 140000000 | bytes 2000000 | tf_op jit(solution)/shard_map/residual/pallas_call | solution.py:165
  53.0 19.7 %all-to-all-start.2 = ((bf16[128,4,256]{2,1,0:T(4,128)(2,1)}), bf16[128,4,256]{2,1,0:T(4,128)(2,1)S(1)}, u32[]{:S(2)}, u32[]{:S(2)}) async-start(bf16[128,4,256]{2,1,0:T(4,128)(2,1)} %get-tuple-element.10), calls=%async_computation.2 | async-start | bytes 524288 | tf_op jit(solution)/shard_map/all_to_all | solution.py:21
  72.7 0.1 copy.24.ids
  72.8 0.0 copy-done.18
  72.9 15.8 %all-to-all-done.2.rows = bf16[128,4,256]{2,1,0:T(4,128)(2,1)S(1)} async-done(((bf16[128,4,256]{2,1,0:T(4,128)(2,1)}), bf16[128,4,256]{2,1,0:T(4,128)(2,1)S(1)}, u32[]{:S(2)}, u32[]{:S(2)}) %all-to-all-start.2) | async-done | bytes 262176 | tf_op jit(solution)/shard_map/all_to_all | solution.py:21
  88.6 0.0 copy-done.2
  88.6 0.0 copy-done.3
  88.6 0.0 copy-done.4
  88.6 2.1 %expert.1 = bf16[128,4,256]{2,1,0:T(4,128)(2,1)} custom-call(bf16[128,4,256]{2,1,0:T(4,128)(2,1)S(1)} %all-to-all-done.2.rows, bf16[352,1024]{1,0:T(8,128)(2,1)S(1)} %bitcast.28, bf16[352,1024]{1,0:T(8,128)(2,1)S(1)} %bitcast.29, bf16[352,1024]{1,0:T(8,128)(2,1)S(1)} %bitcast.30), custom_call_target="tpu_custom_call" | custom-call | flops 277000000 | bytes 2700000 | tf_op jit(solution)/shard_map/expert/pallas_call | solution.py:221
  90.8 6.2 %all-to-all-start.3 = ((bf16[128,4,256]{2,1,0:T(4,128)(2,1)}), bf16[128,4,256]{2,1,0:T(4,128)(2,1)S(1)}, u32[]{:S(2)}, u32[]{:S(2)}) async-start(bf16[128,4,256]{2,1,0:T(4,128)(2,1)} %expert.1), calls=%async_computation.3 | async-start | bytes 524288 | tf_op jit(solution)/shard_map/all_to_all | solution.py:21
  97.0 0.0 all-gather.2.cloned.1.call-done
  97.1 0.0 copy-start
  97.1 1.4 %copy-done = bf16[32,96,256]{2,1,0:T(8,128)(2,1)S(1)} copy-done((bf16[32,96,256]{2,1,0:T(8,128)(2,1)S(1)}, bf16[32,96,256]{2,1,0:T(8,128)(2,1)}, u32[]{:S(2)}) %copy-start) | copy-done | bytes 1572888
  98.5 0.6 dense.1.part
  99.1 13.1 %all-to-all-done.3.returned = bf16[128,4,256]{2,1,0:T(4,128)(2,1)S(1)} async-done(((bf16[128,4,256]{2,1,0:T(4,128)(2,1)}), bf16[128,4,256]{2,1,0:T(4,128)(2,1)S(1)}, u32[]{:S(2)}, u32[]{:S(2)}) %all-to-all-start.3) | async-done | bytes 262176 | tf_op jit(solution)/shard_map/all_to_all | solution.py:21
  112.2 0.6 combine.1
  112.8 10.8 %all_to_all.26 = bf16[16,16,256]{2,1,0:T(8,128)(2,1)S(1)} all-to-all(bf16[16,16,256]{2,1,0:T(8,128)(2,1)S(1)} %combine.1), channel_id=1, replica_groups=mesh['zh'=4,'zl'=2,'yh'=4,'yl'=2,'c'=2,'x'=4] {'zl','yl','x'}, dimensions={0} | all-to-all | bytes 262144 | tf_op jit(solution)/shard_map/all_to_all | solution.py:21
  123.7 0.6 add_convert_fusion
  (5 shorter events, 0.1 us)
Async XLA Ops:
  6.5 90.5 %all-gather.2.cloned.1.call-start = ((), (), s32[]{:S(2)}) async-start(), calls=%async_computation.5 | async-start | bytes 1622016 | tf_op jit(solution)/shard_map/all_gather | solution.py:303
  8.1 26.2 %copy-start.5 = (bf16[512,256]{1,0:T(8,128)(2,1)S(1)}, bf16[512,256]{1,0:T(8,128)(2,1)}, u32[]{:S(2)}) copy-start(bf16[512,256]{1,0:T(8,128)(2,1)} %w0.1) | copy-start | bytes 786436
  8.1 42.4 %copy-start.15 = (f32[1024]{0:T(1024)S(1)}, f32[1024]{0:T(1024)}, u32[]{:S(2)}) copy-start(f32[1024]{0:T(1024)} %param.34) | copy-start | bytes 12292
  8.1 42.4 %copy-start.16 = (s32[16,2]{0,1:T(2,128)S(1)}, s32[16,2]{0,1:T(2,128)}, u32[]{:S(2)}) copy-start(s32[16,2]{0,1:T(2,128)} %param.35) | copy-start | bytes 388
  18.4 1.2 copy-start.1
  19.6 0.9 copy-start.6
  20.5 0.9 copy-start.7
  21.5 0.9 copy-start.8
  22.4 0.9 copy-start.9
  23.4 0.7 copy-start.10
  24.1 0.7 copy-start.11
  24.8 0.7 copy-start.12
  25.5 0.7 copy-start.13
  26.2 0.7 copy-start.14
  26.8 0.7 copy-start.17
  29.0 43.8 %copy-start.18 = (f32[16,2]{0,1:T(2,128)S(1)}, f32[16,2]{0,1:T(2,128)}, u32[]{:S(2)}) copy-start(f32[16,2]{0,1:T(2,128)} %param.36) | copy-start | bytes 388
  29.0 59.6 %copy-start.2 = (bf16[1,1024,352]{1,2,0:T(8,128)(2,1)S(1)}, bf16[1,1024,352]{1,2,0:T(8,128)(2,1)}, u32[]{:S(2)}) copy-start(bf16[1,1024,352]{1,2,0:T(8,128)(2,1)} %param.37) | copy-start | bytes 2162692
  29.0 59.6 %copy-start.3 = (bf16[1,1024,352]{1,2,0:T(8,128)(2,1)S(1)}, bf16[1,1024,352]{1,2,0:T(8,128)(2,1)}, u32[]{:S(2)}) copy-start(bf16[1,1024,352]{1,2,0:T(8,128)(2,1)} %param.38) | copy-start | bytes 2162692
  29.0 59.6 %copy-start.4 = (bf16[1,352,1024]{2,1,0:T(8,128)(2,1)S(1)}, bf16[1,352,1024]{2,1,0:T(8,128)(2,1)}, u32[]{:S(2)}) copy-start(bf16[1,352,1024]{2,1,0:T(8,128)(2,1)} %param.39) | copy-start | bytes 2162692
  29.0 21.5 %all-to-all-start.1 = ((bf16[16,16,384]{2,1,0:T(8,128)(2,1)}), bf16[16,16,384]{2,1,0:T(8,128)(2,1)S(1)}, u32[]{:S(2)}, u32[]{:S(2)}) async-start(bf16[16,16,384]{2,1,0:T(8,128)(2,1)} %cell.1), calls=%async_computation.1 | async-start | bytes 393216 | tf_op jit(solution)/shard_map/all_to_all | solution.py:21
  34.3 10.7 %collective-permute-start = (bf16[512,256]{1,0:T(8,128)(2,1)S(1)}, bf16[512,256]{1,0:T(8,128)(2,1)S(1)}, u32[]{:S(2)}, u32[]{:S(2)}) collective-permute-start(bf16[512,256]{1,0:T(8,128)(2,1)S(1)} %copy-done.5), channel_id=1, source_target_pairs={{0,1},{1,2},{2,3},{3,0},{4,5},{5,6},{6,7},{7,4},{8,9},{9,10},{10,1... | collective-permute-start | bytes 786440 | tf_op jit(solution)/shard_map/ppermute | solution.py:34
  37.5 11.3 %collective-permute-start.1 = (bf16[512,256]{1,0:T(8,128)(2,1)S(1)}, bf16[512,256]{1,0:T(8,128)(2,1)S(1)}, u32[]{:S(2)}, u32[]{:S(2)}) collective-permute-start(bf16[512,256]{1,0:T(8,128)(2,1)S(1)} %copy-done.5), channel_id=1, source_target_pairs={{0,2},{1,3},{2,0},{3,1},{4,6},{5,7},{6,4},{7,5},{8,10},{9,11},{10,... | collective-permute-start | bytes 786440 | tf_op jit(solution)/shard_map/ppermute | solution.py:34
  41.9 8.6 %collective-permute-start.2 = (bf16[512,256]{1,0:T(8,128)(2,1)S(1)}, bf16[512,256]{1,0:T(8,128)(2,1)}, u32[]{:S(2)}, u32[]{:S(2)}) collective-permute-start(bf16[512,256]{1,0:T(8,128)(2,1)S(1)} %copy-done.5), channel_id=1, source_target_pairs={{0,3},{1,0},{2,1},{3,2},{4,7},{5,4},{6,5},{7,6},{8,11},{9,8},{10,9... | collective-permute-start | bytes 786440 | tf_op jit(solution)/shard_map/ppermute | solution.py:34
  53.0 35.6 %all-to-all-start.2 = ((bf16[128,4,256]{2,1,0:T(4,128)(2,1)}), bf16[128,4,256]{2,1,0:T(4,128)(2,1)S(1)}, u32[]{:S(2)}, u32[]{:S(2)}) async-start(bf16[128,4,256]{2,1,0:T(4,128)(2,1)} %get-tuple-element.10), calls=%async_computation.2 | async-start | bytes 524288 | tf_op jit(solution)/shard_map/all_to_all | solution.py:21
  90.8 21.5 %all-to-all-start.3 = ((bf16[128,4,256]{2,1,0:T(4,128)(2,1)}), bf16[128,4,256]{2,1,0:T(4,128)(2,1)S(1)}, u32[]{:S(2)}, u32[]{:S(2)}) async-start(bf16[128,4,256]{2,1,0:T(4,128)(2,1)} %expert.1), calls=%async_computation.3 | async-start | bytes 524288 | tf_op jit(solution)/shard_map/all_to_all | solution.py:21
  97.1 1.4 %copy-start = (bf16[32,96,256]{2,1,0:T(8,128)(2,1)S(1)}, bf16[32,96,256]{2,1,0:T(8,128)(2,1)}, u32[]{:S(2)}) copy-start(bf16[32,96,256]{2,1,0:T(8,128)(2,1)} %all-gather.2.cloned.1.call-done) | copy-start | bytes 4718596
Sparse Core Ops, SparseCore 0:
  18.5 66.7 all-gather.1

commit v11 on v10

--- a/solution.py
+++ b/solution.py
@@ -29,9 +29,9 @@
     return lax.dot_general(a, b, (((1,), (1,)), ((), ())), preferred_element_type=f32)
 
 
-def shifted(array, axis, step):
+def swapped(array, axis, step):
     size = lax.axis_size(axis)
-    return lax.ppermute(array, axis, [(i, (i + step) % size) for i in range(size)])
+    return lax.ppermute(array, axis, [(i, i ^ step) for i in range(size)])
 
 
 def upright(row):
@@ -136,7 +136,7 @@
     )
     total = jnp.zeros((near * seqs, 1), f32)
     for step, weight in enumerate((w0, w1, w2, w3)):
-        k = (me[0] + tp - step) & (tp - 1)
+        k = me[0] ^ step
         added = dot(heads, weight[...])
         old = jnp.concatenate([second[s, k, :, HEAD:] for s in range(near)], axis=0)
         values = (old.astype(f32) + added).astype(bf16)
@@ -298,7 +298,7 @@
 
     mix_out = {0: w_mix_out}
     for step in (2, 1, 3):
-        mix_out[step] = shifted(w_mix_out, "x", step)
+        mix_out[step] = swapped(w_mix_out, "x", step)
 
     dense = lax.all_gather(first[:, seqs : seqs + 3 * SLOT].reshape(-1, quarter), FAR)
     dense = dense.reshape(far, tp, 3 * SLOT, quarter)

time: 132 us -> 133 us (level)
  waiting for transfers between devices: 34.4 us -> 38.9 us
  starting transfers between devices: 41.9 us -> 39.8 us
  blocking collectives: 20.5 us -> 19 us
    ppermute x3, waiting for transfers between devices: 5.49 us -> 10.5 us  [swapped(): return lax.ppermute(array, axis, [(i, i ^ step) for i in range(size)])]
    all_to_all x2, blocking collectives: 20.5 us -> 19 us  [exchange(): return lax.all_to_all(blocks, axis, 0, 0, tiled=True)]
where the time goes in v11:
time: 133 us; the launch traced here: 132 us
  starting transfers between devices  39.8 us (30%)
  waiting for transfers between devices  38.9 us (29%)
  blocking collectives  19 us (14%)
  between operations  13.5 us (10%)
  local copies, waits for them, and re-layouts  11.3 us (8%)
  Pallas kernels  8.9 us (7%)
    all_to_all x3, starting transfers between devices, exchange(): return lax.all_to_all(blocks, axis, 0, 0, tiled=True)  30.2 us
    all_to_all x3, waiting for transfers between devices, exchange(): return lax.all_to_all(blocks, axis, 0, 0, tiled=True)  28.4 us
    all_to_all x2, blocking collectives, exchange(): return lax.all_to_all(blocks, axis, 0, 0, tiled=True)  19 us
    unnamed x39, local copies, waits for them, and re-layouts  10.6 us
    ppermute x3, waiting for transfers between devices, swapped(): return lax.ppermute(array, axis, [(i, i ^ step) for i in range(size)])  10.5 us
    ppermute x3, starting transfers between devices, swapped(): return lax.ppermute(array, axis, [(i, i ^ step) for i in range(size)])  9.58 us
  transfers between devices with their start and end apart: 7, of which 4 were waited for; matrix products, arithmetic and copies ran while one was open for 0% of the time, Pallas kernels for 5%

profile of v11, /device:TPU:1, one launch (start us, length us, event | category | flops | bytes accessed | tf_op | source)
XLA Modules:
  0.0 132.1 jit_solution(8347300085505684087)
XLA Ops:
  6.5 0.0 all-gather.2.cloned.1.call-start
  6.5 1.5 %pack.1 = bf16[4,48,256]{2,1,0:T(8,128)(2,1)} custom-call(bf16[16,256]{1,0:T(8,128)(2,1)} %tokens.3, bf16[24,256]{1,0:T(8,128)(2,1)} %bitcast.40, bf16[24,256]{1,0:T(8,128)(2,1)} %bitcast.41, bf16[24,256]{1,0:T(8,128)(2,1)} %down.1, bf16[256]{0:T(256)(128)(2,1)} %mix.1), custom_call_target="tpu_custom_call" | custom-call | tf_op jit(solution)/shard_map/pack/pallas_call | solution.py:64
  8.1 0.0 copy-start.5
  8.1 0.0 copy-start.15
  8.1 0.0 copy-start.16
  8.1 9.6 %all_to_all.25.first = bf16[4,48,256]{2,1,0:T(8,128)(2,1)S(1)} all-to-all(bf16[4,48,256]{2,1,0:T(8,128)(2,1)} %pack.1), channel_id=1, replica_groups=mesh['zh'=4,'zl'=2,'yh'=4,'yl'=2,'c'=2,'x'=4] {'x'}, dimensions={0} | all-to-all | bytes 196608 | tf_op jit(solution)/shard_map/all_to_all | solution.py:21
  17.7 0.6 slice.8
  18.3 0.0 all-gather.2.cloned.1.call-update
  18.4 0.0 copy-start.1
  18.4 1.2 copy-done.1
  19.6 0.0 copy-start.6
  19.6 0.9 copy-done.6
  20.5 0.0 copy-start.7
  20.5 0.9 copy-done.7
  21.5 0.0 copy-start.8
  21.5 0.9 copy-done.8
  22.4 0.0 copy-start.9
  22.4 0.9 copy-done.9
  23.4 0.0 copy-start.10
  23.4 0.7 copy-done.10
  24.1 0.0 copy-start.11
  24.1 0.7 copy-done.11
  24.8 0.0 copy-start.12
  24.8 0.7 copy-done.12
  25.5 0.0 copy-start.13
  25.5 0.7 copy-done.13
  26.2 0.0 copy-start.14
  26.2 0.7 copy-done.14
  26.8 0.0 copy-start.17
  26.9 0.7 copy-done.17
  27.5 1.5 %cell.1 = bf16[16,16,384]{2,1,0:T(8,128)(2,1)} custom-call(bf16[4,48,256]{2,1,0:T(8,128)(2,1)S(1)} %all_to_all.25.first, f32[1,1024]{1,0:T(1,128)S(1)} %bitcast.33, bf16[1024,128]{1,0:T(8,128)(2,1)S(1)} %copy-done.6, bf16[1024,128]{1,0:T(8,128)(2,1)S(1)} %copy-done.7, bf16[1024,128]{1,0:T(8,128)(2,1)S(1)} %copy-done.8, bf16[1024,128]{1,0:T(8,128)(2,1)S(1)} %copy-done.9, ...), custom_call_target="tpu_custom_call" | custom-call | flops 40000000 | bytes 2200000 | tf_op jit(solution)/shard_map/cell/pallas_call | solution.py:102
  29.0 0.0 copy-start.18
  29.0 0.0 copy-start.2
  29.0 0.0 copy-start.3
  29.0 0.0 copy-start.4
  29.0 5.2 %all-to-all-start.1 = ((bf16[16,16,384]{2,1,0:T(8,128)(2,1)}), bf16[16,16,384]{2,1,0:T(8,128)(2,1)S(1)}, u32[]{:S(2)}, u32[]{:S(2)}) async-start(bf16[16,16,384]{2,1,0:T(8,128)(2,1)} %cell.1), calls=%async_computation.1 | async-start | bytes 393216 | tf_op jit(solution)/shard_map/all_to_all | solution.py:21
  34.3 0.0 copy-done.5
  34.3 3.3 %collective-permute-start = (bf16[512,256]{1,0:T(8,128)(2,1)S(1)}, bf16[512,256]{1,0:T(8,128)(2,1)S(1)}, u32[]{:S(2)}, u32[]{:S(2)}) collective-permute-start(bf16[512,256]{1,0:T(8,128)(2,1)S(1)} %copy-done.5), channel_id=1, source_target_pairs={{0,1},{1,0},{2,3},{3,2},{4,5},{5,4},{6,7},{7,6},{8,9},{9,8},{10,11... | collective-permute-start | bytes 786440 | tf_op jit(solution)/shard_map/ppermute | solution.py:34
  37.5 4.3 %collective-permute-start.1 = (bf16[512,256]{1,0:T(8,128)(2,1)S(1)}, bf16[512,256]{1,0:T(8,128)(2,1)S(1)}, u32[]{:S(2)}, u32[]{:S(2)}) collective-permute-start(bf16[512,256]{1,0:T(8,128)(2,1)S(1)} %copy-done.5), channel_id=1, source_target_pairs={{0,2},{1,3},{2,0},{3,1},{4,6},{5,7},{6,4},{7,5},{8,10},{9,11},{10,... | collective-permute-start | bytes 786440 | tf_op jit(solution)/shard_map/ppermute | solution.py:34
  41.9 2.0 %collective-permute-start.2 = (bf16[512,256]{1,0:T(8,128)(2,1)S(1)}, bf16[512,256]{1,0:T(8,128)(2,1)}, u32[]{:S(2)}, u32[]{:S(2)}) collective-permute-start(bf16[512,256]{1,0:T(8,128)(2,1)S(1)} %copy-done.5), channel_id=1, source_target_pairs={{0,3},{1,2},{2,1},{3,0},{4,7},{5,6},{6,5},{7,4},{8,11},{9,10},{10,... | collective-permute-start | bytes 786440 | tf_op jit(solution)/shard_map/ppermute | solution.py:34
  43.9 0.0 collective-permute-done.w1
  43.9 5.0 %collective-permute-done.1.w2 = bf16[512,256]{1,0:T(8,128)(2,1)S(1)} collective-permute-done((bf16[512,256]{1,0:T(8,128)(2,1)S(1)}, bf16[512,256]{1,0:T(8,128)(2,1)S(1)}, u32[]{:S(2)}, u32[]{:S(2)}) %collective-permute-start.1) | collective-permute-done | bytes 262176 | tf_op jit(solution)/shard_map/ppermute | solution.py:34
  48.8 5.6 %collective-permute-done.2.w3 = bf16[512,256]{1,0:T(8,128)(2,1)} collective-permute-done((bf16[512,256]{1,0:T(8,128)(2,1)S(1)}, bf16[512,256]{1,0:T(8,128)(2,1)}, u32[]{:S(2)}, u32[]{:S(2)}) %collective-permute-start.2) | collective-permute-done | bytes 262176 | tf_op jit(solution)/shard_map/ppermute | solution.py:34
  54.4 0.0 all-to-all-done.1
  54.4 0.0 copy-done.15
  54.4 0.0 copy-done.16
  54.4 2.5 %residual.1 = (bf16[64,1024]{1,0:T(8,128)(2,1)S(1)}, bf16[128,4,256]{2,1,0:T(4,128)(2,1)}, bf16[16,256]{1,0:T(8,128)(2,1)S(1)}) custom-call(s32[1]{0:T(128)} %bitcast.me, s32[1]{0:T(128)} %bitcast.1.place, bf16[4,4,16,384]{3,2,1,0:T(8,128)(2,1)S(1)} %bitcast.27, bf16[512,256]{1,0:T(8,128)(2,1)S(1)} %copy-done.5, ...), custom_call_target="tpu_custom_call" | custom-call | flops 140000000 | bytes 2000000 | tf_op jit(solution)/shard_map/residual/pallas_call | solution.py:165
  57.0 19.4 %all-to-all-start.2 = ((bf16[128,4,256]{2,1,0:T(4,128)(2,1)}), bf16[128,4,256]{2,1,0:T(4,128)(2,1)S(1)}, u32[]{:S(2)}, u32[]{:S(2)}) async-start(bf16[128,4,256]{2,1,0:T(4,128)(2,1)} %get-tuple-element.10), calls=%async_computation.2 | async-start | bytes 524288 | tf_op jit(solution)/shard_map/all_to_all | solution.py:21
  76.4 0.1 copy.24.ids
  76.5 0.0 copy-done.18
  76.5 15.1 %all-to-all-done.2.rows = bf16[128,4,256]{2,1,0:T(4,128)(2,1)S(1)} async-done(((bf16[128,4,256]{2,1,0:T(4,128)(2,1)}), bf16[128,4,256]{2,1,0:T(4,128)(2,1)S(1)}, u32[]{:S(2)}, u32[]{:S(2)}) %all-to-all-start.2) | async-done | bytes 262176 | tf_op jit(solution)/shard_map/all_to_all | solution.py:21
  91.6 0.0 copy-done.2
  91.6 0.0 copy-done.3
  91.6 0.0 copy-done.4
  91.6 2.1 %expert.1 = bf16[128,4,256]{2,1,0:T(4,128)(2,1)} custom-call(bf16[128,4,256]{2,1,0:T(4,128)(2,1)S(1)} %all-to-all-done.2.rows, bf16[352,1024]{1,0:T(8,128)(2,1)S(1)} %bitcast.28, bf16[352,1024]{1,0:T(8,128)(2,1)S(1)} %bitcast.29, bf16[352,1024]{1,0:T(8,128)(2,1)S(1)} %bitcast.30), custom_call_target="tpu_custom_call" | custom-call | flops 277000000 | bytes 2700000 | tf_op jit(solution)/shard_map/expert/pallas_call | solution.py:221
  93.8 5.5 %all-to-all-start.3 = ((bf16[128,4,256]{2,1,0:T(4,128)(2,1)}), bf16[128,4,256]{2,1,0:T(4,128)(2,1)S(1)}, u32[]{:S(2)}, u32[]{:S(2)}) async-start(bf16[128,4,256]{2,1,0:T(4,128)(2,1)} %expert.1), calls=%async_computation.3 | async-start | bytes 524288 | tf_op jit(solution)/shard_map/all_to_all | solution.py:21
  99.3 0.0 all-gather.2.cloned.1.call-done
  99.4 0.0 copy-start
  99.4 1.4 %copy-done = bf16[32,96,256]{2,1,0:T(8,128)(2,1)S(1)} copy-done((bf16[32,96,256]{2,1,0:T(8,128)(2,1)S(1)}, bf16[32,96,256]{2,1,0:T(8,128)(2,1)}, u32[]{:S(2)}) %copy-start) | copy-done | bytes 1572888
  100.8 0.6 dense.1.part
  101.4 13.3 %all-to-all-done.3.returned = bf16[128,4,256]{2,1,0:T(4,128)(2,1)S(1)} async-done(((bf16[128,4,256]{2,1,0:T(4,128)(2,1)}), bf16[128,4,256]{2,1,0:T(4,128)(2,1)S(1)}, u32[]{:S(2)}, u32[]{:S(2)}) %all-to-all-start.3) | async-done | bytes 262176 | tf_op jit(solution)/shard_map/all_to_all | solution.py:21
  114.7 0.6 combine.1
  115.3 9.4 %all_to_all.26 = bf16[16,16,256]{2,1,0:T(8,128)(2,1)S(1)} all-to-all(bf16[16,16,256]{2,1,0:T(8,128)(2,1)S(1)} %combine.1), channel_id=1, replica_groups=mesh['zh'=4,'zl'=2,'yh'=4,'yl'=2,'c'=2,'x'=4] {'zl','yl','x'}, dimensions={0} | all-to-all | bytes 262144 | tf_op jit(solution)/shard_map/all_to_all | solution.py:21
  124.7 0.6 add_convert_fusion
  (5 shorter events, 0.1 us)
Async XLA Ops:
  6.5 92.8 %all-gather.2.cloned.1.call-start = ((), (), s32[]{:S(2)}) async-start(), calls=%async_computation.5 | async-start | bytes 1622016 | tf_op jit(solution)/shard_map/all_gather | solution.py:303
  8.1 26.2 %copy-start.5 = (bf16[512,256]{1,0:T(8,128)(2,1)S(1)}, bf16[512,256]{1,0:T(8,128)(2,1)}, u32[]{:S(2)}) copy-start(bf16[512,256]{1,0:T(8,128)(2,1)} %w0.1) | copy-start | bytes 786436
  8.1 46.3 %copy-start.15 = (f32[1024]{0:T(1024)S(1)}, f32[1024]{0:T(1024)}, u32[]{:S(2)}) copy-start(f32[1024]{0:T(1024)} %param.34) | copy-start | bytes 12292
  8.1 46.3 %copy-start.16 = (s32[16,2]{0,1:T(2,128)S(1)}, s32[16,2]{0,1:T(2,128)}, u32[]{:S(2)}) copy-start(s32[16,2]{0,1:T(2,128)} %param.35) | copy-start | bytes 388
  18.4 1.2 copy-start.1
  19.6 0.9 copy-start.6
  20.5 0.9 copy-start.7
  21.5 0.9 copy-start.8
  22.4 0.9 copy-start.9
  23.4 0.7 copy-start.10
  24.1 0.7 copy-start.11
  24.8 0.7 copy-start.12
  25.5 0.7 copy-start.13
  26.2 0.7 copy-start.14
  26.8 0.7 copy-start.17
  29.0 47.5 %copy-start.18 = (f32[16,2]{0,1:T(2,128)S(1)}, f32[16,2]{0,1:T(2,128)}, u32[]{:S(2)}) copy-start(f32[16,2]{0,1:T(2,128)} %param.36) | copy-start | bytes 388
  29.0 62.6 %copy-start.2 = (bf16[1,1024,352]{1,2,0:T(8,128)(2,1)S(1)}, bf16[1,1024,352]{1,2,0:T(8,128)(2,1)}, u32[]{:S(2)}) copy-start(bf16[1,1024,352]{1,2,0:T(8,128)(2,1)} %param.37) | copy-start | bytes 2162692
  29.0 62.6 %copy-start.3 = (bf16[1,1024,352]{1,2,0:T(8,128)(2,1)S(1)}, bf16[1,1024,352]{1,2,0:T(8,128)(2,1)}, u32[]{:S(2)}) copy-start(bf16[1,1024,352]{1,2,0:T(8,128)(2,1)} %param.38) | copy-start | bytes 2162692
  29.0 62.6 %copy-start.4 = (bf16[1,352,1024]{2,1,0:T(8,128)(2,1)S(1)}, bf16[1,352,1024]{2,1,0:T(8,128)(2,1)}, u32[]{:S(2)}) copy-start(bf16[1,352,1024]{2,1,0:T(8,128)(2,1)} %param.39) | copy-start | bytes 2162692
  29.0 25.4 %all-to-all-start.1 = ((bf16[16,16,384]{2,1,0:T(8,128)(2,1)}), bf16[16,16,384]{2,1,0:T(8,128)(2,1)S(1)}, u32[]{:S(2)}, u32[]{:S(2)}) async-start(bf16[16,16,384]{2,1,0:T(8,128)(2,1)} %cell.1), calls=%async_computation.1 | async-start | bytes 393216 | tf_op jit(solution)/shard_map/all_to_all | solution.py:21
  34.3 9.6 %collective-permute-start = (bf16[512,256]{1,0:T(8,128)(2,1)S(1)}, bf16[512,256]{1,0:T(8,128)(2,1)S(1)}, u32[]{:S(2)}, u32[]{:S(2)}) collective-permute-start(bf16[512,256]{1,0:T(8,128)(2,1)S(1)} %copy-done.5), channel_id=1, source_target_pairs={{0,1},{1,0},{2,3},{3,2},{4,5},{5,4},{6,7},{7,6},{8,9},{9,8},{10,11... | collective-permute-start | bytes 786440 | tf_op jit(solution)/shard_map/ppermute | solution.py:34
  37.5 11.3 %collective-permute-start.1 = (bf16[512,256]{1,0:T(8,128)(2,1)S(1)}, bf16[512,256]{1,0:T(8,128)(2,1)S(1)}, u32[]{:S(2)}, u32[]{:S(2)}) collective-permute-start(bf16[512,256]{1,0:T(8,128)(2,1)S(1)} %copy-done.5), channel_id=1, source_target_pairs={{0,2},{1,3},{2,0},{3,1},{4,6},{5,7},{6,4},{7,5},{8,10},{9,11},{10,... | collective-permute-start | bytes 786440 | tf_op jit(solution)/shard_map/ppermute | solution.py:34
  41.9 12.6 %collective-permute-start.2 = (bf16[512,256]{1,0:T(8,128)(2,1)S(1)}, bf16[512,256]{1,0:T(8,128)(2,1)}, u32[]{:S(2)}, u32[]{:S(2)}) collective-permute-start(bf16[512,256]{1,0:T(8,128)(2,1)S(1)} %copy-done.5), channel_id=1, source_target_pairs={{0,3},{1,2},{2,1},{3,0},{4,7},{5,6},{6,5},{7,4},{8,11},{9,10},{10,... | collective-permute-start | bytes 786440 | tf_op jit(solution)/shard_map/ppermute | solution.py:34
  57.0 34.7 %all-to-all-start.2 = ((bf16[128,4,256]{2,1,0:T(4,128)(2,1)}), bf16[128,4,256]{2,1,0:T(4,128)(2,1)S(1)}, u32[]{:S(2)}, u32[]{:S(2)}) async-start(bf16[128,4,256]{2,1,0:T(4,128)(2,1)} %get-tuple-element.10), calls=%async_computation.2 | async-start | bytes 524288 | tf_op jit(solution)/shard_map/all_to_all | solution.py:21
  93.8 20.9 %all-to-all-start.3 = ((bf16[128,4,256]{2,1,0:T(4,128)(2,1)}), bf16[128,4,256]{2,1,0:T(4,128)(2,1)S(1)}, u32[]{:S(2)}, u32[]{:S(2)}) async-start(bf16[128,4,256]{2,1,0:T(4,128)(2,1)} %expert.1), calls=%async_computation.3 | async-start | bytes 524288 | tf_op jit(solution)/shard_map/all_to_all | solution.py:21
  99.4 1.4 %copy-start = (bf16[32,96,256]{2,1,0:T(8,128)(2,1)S(1)}, bf16[32,96,256]{2,1,0:T(8,128)(2,1)}, u32[]{:S(2)}) copy-start(bf16[32,96,256]{2,1,0:T(8,128)(2,1)} %all-gather.2.cloned.1.call-done) | copy-start | bytes 4718596
Sparse Core Ops, SparseCore 0:
  18.5 67.1 all-gather.1
